TPU v7x, 512 devices: a whole 4x8x8 slice. The times are simulated.
512 devices in a mesh: fs: 64 (over z, y), tp: 8 (over x, core).
Axes of the slice: x: 4, y: 8, z: 8, core: 2. Of those that a mesh axis runs over, the one named last changes fastest.
Arguments:
- tokens: bfloat16 [24576, 2048], P('fs', 'tp'), may hold values from -8 to 8
- w_value: bfloat16 [2048, 1024], P('fs', 'tp'), may hold values from -0.125 to 0.125
- w_gate: bfloat16 [2048, 1024], P('fs', 'tp'), may hold values from -0.125 to 0.125
- conv_kernel: bfloat16 [31, 1024], replicated, may hold values from -1 to 1
- conv_gain: float32 [1024], replicated, may hold values from 0.1 to 1.9
- w_mix_out: bfloat16 [1024, 2048], P('fs', 'tp'), may hold values from -0.1875 to 0.1875
- mix_gain: float32 [2048], replicated, may hold values from 0.1 to 1.9
- w_up: bfloat16 [2048, 8192], P('fs', 'tp'), may hold values from -0.125 to 0.125
- w_down: bfloat16 [8192, 2048], P('tp', 'fs'), may hold values from -0.0625 to 0.0625
- out_gain: float32 [2048], replicated, may hold values from 0.1 to 1.9
Outputs:
- result: bfloat16 [24576, 2048], P('fs', 'tp')
All inputs are finite; a program needn't handle non-finite values.
Results may differ from a plain program's by a relative error of at most 0.013.
Values may be sent and summed in bfloat16 or wider, within the bound.
No kernel may reach another device: no remote copies, remote signals or barrier semaphores. Data moves between devices by JAX's collectives and lax.ppermute only.
A program may use at most 64 MiB of HBM per device.

v0:
```python
import jax
import jax.numpy as jnp
import numpy as np
from jax import lax
from jax.sharding import Mesh
from jax.sharding import PartitionSpec as P


WIDTH = 2048
CHANNELS = 1024
KERNEL = 31
LENGTH = 128
FS = ("z", "y")
TP = ("x", "core")
ALL = ("z", "y", "x", "core")
SIDE = 8


norm_eps = 1e-05
residual_scale = 2.0**0.5
f32 = jnp.float32
bf16 = jnp.bfloat16


def rings(axis_of_core):
    ids = np.arange(SIDE * SIDE * 4 * 2).reshape(SIDE, SIDE, 4, 2)
    out = []
    for x in range(4):
        for core in range(2):
            plane = ids[:, :, x, core]
            out += (plane if axis_of_core[core] == "y" else plane.T).tolist()
    return out


FIRST, SECOND = rings("yz"), rings("zy")


def sent_to_group(shard, groups):
    copies = jnp.broadcast_to(shard, (SIDE, *shard.shape))
    return lax.all_to_all(copies, ALL, 0, 0, axis_index_groups=groups, tiled=True)


def partner_of(a):
    return lax.ppermute(a, "core", [(0, 1), (1, 0)])


def turned(core, a):
    return jnp.where(core == 0, a, jnp.swapaxes(a, 0, 1))


def all_ranks(shard, core):
    copies = jnp.broadcast_to(shard, (4, *shard.shape))
    mine = lax.all_to_all(copies, "x", 0, 0, tiled=True)
    other = partner_of(mine)
    both = jnp.stack([jnp.where(core == 0, mine, other), jnp.where(core == 0, other, mine)], 1)
    return both.reshape(SIDE, *shard.shape)


def joined_columns(parts):
    return jnp.moveaxis(parts, 0, 1).reshape(parts.shape[1], -1)


def causal_filter(gated, kernel):
    sequences = gated.shape[0] // LENGTH
    frames = gated.astype(f32).reshape(sequences, LENGTH, gated.shape[1])
    padded = jnp.pad(frames, ((0, 0), (KERNEL - 1, 0), (0, 0)))
    accumulated = jnp.zeros(frames.shape, f32)
    for offset in range(KERNEL):
        accumulated = (
            accumulated + kernel[offset].astype(f32) * padded[:, offset : offset + LENGTH]
        )
    return accumulated.reshape(gated.shape[0], gated.shape[1])


def row_norm_terms(values, entries):
    average = jnp.sum(values, 1, keepdims=True) / entries
    spread = jnp.maximum(jnp.sum(values * values, 1, keepdims=True) / entries - average * average, 0.0)
    return average, lax.rsqrt(spread + norm_eps)


def layer(
    tokens, w_value, w_gate, conv_kernel, conv_gain, w_mix_out, mix_gain, w_up, w_down, out_gain
):
    tp_rank = lax.axis_index(TP)
    core = lax.axis_index("core")
    frames = tokens.shape[0]
    width_part = tokens.shape[1]
    channel_part = w_value.shape[1]
    units_part = w_up.shape[1]

    def mine_of(vector, size):
        return lax.dynamic_slice_in_dim(vector, tp_rank * size, size, vector.ndim - 1)

    wide = jnp.concatenate([w_up, w_down.T], 1)
    wide = lax.all_gather(wide, ALL, axis=0, tiled=True, axis_index_groups=FIRST)
    wide = lax.all_gather(wide, ALL, axis=0, tiled=True, axis_index_groups=SECOND)

    mix_rows = w_mix_out.shape[0]
    halves = [w_mix_out[:, :channel_part], w_mix_out[:, channel_part:]]
    small = jnp.concatenate([w_value, w_gate, jnp.concatenate(halves, 0)], 1)
    small = sent_to_group(small, FIRST).reshape(-1, small.shape[1])
    small = sent_to_group(small, SECOND)
    value_gate = small[:, :, : 2 * channel_part].reshape(WIDTH, 2 * channel_part)
    mix = small[:, :, 2 * channel_part :].reshape(SIDE, SIDE, 2, mix_rows, channel_part)
    mix = turned(core, mix.transpose(0, 1, 3, 2, 4)).reshape(CHANNELS, width_part)

    ranks = all_ranks(tokens.T, core)
    ranks = turned(core, ranks.reshape(SIDE, SIDE, -1, frames)).reshape(WIDTH, frames)

    both = lax.dot_general(ranks, value_gate, (((0,), (0,)), ((), ())), preferred_element_type=f32)
    values_proj, gate_proj = both[:, :channel_part], both[:, channel_part:]
    gated = (values_proj * jax.nn.sigmoid(gate_proj)).astype(bf16)
    filtered = causal_filter(gated, mine_of(conv_kernel, channel_part))
    filtered_whole = joined_columns(all_ranks(filtered.astype(bf16), core)).astype(f32)
    average, scale = row_norm_terms(filtered_whole, CHANNELS)
    activated = jax.nn.silu((filtered_whole - average) * scale * conv_gain).astype(bf16)

    mixed = jnp.dot(activated, mix, preferred_element_type=f32)
    combined = residual_scale * tokens.astype(f32) + mixed
    combined_whole = all_ranks(combined.astype(bf16).T, core).reshape(WIDTH, frames).astype(f32)
    average = jnp.sum(combined_whole, 0) / WIDTH
    spread = jnp.maximum(jnp.sum(combined_whole * combined_whole, 0) / WIDTH - average * average, 0.0)
    scale = lax.rsqrt(spread + norm_eps)
    middle_whole = ((combined_whole - average) * scale * mix_gain[:, None]).astype(bf16)
    middle_whole = turned(core, middle_whole.reshape(SIDE, SIDE, -1, frames)).reshape(WIDTH, frames)
    middle = ((combined - average[:, None]) * scale[:, None] * mine_of(mix_gain, width_part)).astype(bf16)

    up_proj = lax.dot_general(
        wide[:, :units_part], middle_whole, (((0,), (0,)), ((), ())), preferred_element_type=f32
    )
    hidden = jnp.square(jax.nn.relu(up_proj)).astype(bf16)
    terms = jnp.dot(wide[:, units_part:], hidden, preferred_element_type=f32)
    terms = turned(core, terms.astype(bf16).reshape(SIDE, SIDE, -1, frames))
    terms = terms.reshape(4, 2, width_part, frames)
    kept = lax.dynamic_index_in_dim(terms, core, 1, keepdims=False)
    given = lax.dynamic_index_in_dim(terms, 1 - core, 1, keepdims=False)
    pair = (kept.astype(f32) + partner_of(given).astype(f32)).astype(bf16)
    arrived = lax.all_to_all(pair, "x", 0, 0, tiled=True)
    down_sum = jnp.sum(arrived.astype(f32), 0).T

    final = residual_scale * middle.astype(f32) + down_sum
    sums = jnp.stack([jnp.sum(final, 1), jnp.sum(final * final, 1)])
    copies = jnp.broadcast_to(sums, (SIDE, *sums.shape))
    totals = jnp.sum(lax.all_to_all(copies, TP, 0, 0, tiled=True), 0)
    average = totals[0] / WIDTH
    spread = jnp.maximum(totals[1] / WIDTH - average * average, 0.0)
    scale = lax.rsqrt(spread + norm_eps)
    result = (final - average[:, None]) * scale[:, None] * mine_of(out_gain, width_part)
    return result.astype(bf16)


def solution(mesh):
    split = Mesh(mesh.devices.reshape(8, 8, 4, 2), ALL)
    in_specs = (
        P(FS, TP),
        P(FS, TP),
        P(FS, TP),
        P(),
        P(),
        P(FS, TP),
        P(),
        P(FS, TP),
        P(TP, FS),
        P(),
    )
    return jax.shard_map(layer, mesh=split, in_specs=in_specs, out_specs=P(FS, TP), check_vma=False)
```

profile of v0, /device:TPU:1, one launch (start us, length us, event | category | flops | bytes accessed | tf_op | source)
XLA Modules:
  0.0 212.6 jit_solution(3159996493156462970)
XLA Ops:
  6.5 1.6 pad_maximum_fusion.2
  8.2 43.6 %all-gather.3.cloned.1.call-done = bf16[256,2048]{1,0:T(8,128)(2,1)} async-done(((bf16[32,2048]{1,0:T(8,128)(2,1)}), bf16[256,2048]{1,0:T(8,128)(2,1)}) %all-gather.3.cloned.1.call-update) | async-done | bytes 1048592 | tf_op jit(solution)/shard_map/all_gather | solution.py:95
  51.8 0.7 fusion.128
  52.5 0.7 maximum_maximum_fusion
  53.2 0.7 broadcast_in_dim.13
  53.9 3.5 %all-to-all-start.1 = ((bf16[8,32,384]{2,1,0:T(8,128)(2,1)}), bf16[8,32,384]{2,1,0:T(8,128)(2,1)S(1)}, u32[]{:S(2)}, u32[]{:S(2)}) async-start(bf16[8,32,384]{2,1,0:T(8,128)(2,1)} %broadcast_in_dim.13), calls=%async_computation.1 | async-start | bytes 393216 | tf_op jit(solution)/shard_map/all_to_all | solution.py:40
  57.6 8.5 %all-to-all-done.1 = bf16[8,32,384]{2,1,0:T(8,128)(2,1)S(1)} async-done(((bf16[8,32,384]{2,1,0:T(8,128)(2,1)}), bf16[8,32,384]{2,1,0:T(8,128)(2,1)S(1)}, u32[]{:S(2)}, u32[]{:S(2)}) %all-to-all-start.1) | async-done | bytes 196640 | tf_op jit(solution)/shard_map/all_to_all | solution.py:40
  66.1 12.2 %all_to_all.35 = bf16[4,256,384]{2,1,0:T(8,128)(2,1)S(1)} all-to-all(bf16[4,256,384]{2,1,0:T(8,128)(2,1)S(1)} %broadcast_in_dim.12), channel_id=1, replica_groups=mesh['z'=8,'y'=8,'x'=4,'core'=2] {'x'}, dimensions={0} | all-to-all | bytes 1572864 | tf_op jit(solution)/shard_map/all_to_all | solution.py:53
  78.3 1.4 broadcast_in_dim.14
  79.7 8.6 %all-to-all-start.2 = ((bf16[8,256,384]{2,1,0:T(8,128)(2,1)}), bf16[8,256,384]{2,1,0:T(8,128)(2,1)S(1)}, u32[]{:S(2)}, u32[]{:S(2)}) async-start(bf16[8,256,384]{2,1,0:T(8,128)(2,1)} %broadcast_in_dim.14), calls=%async_computation.2 | async-start | bytes 3145728 | tf_op jit(solution)/shard_map/all_to_all | solution.py:40
  88.3 8.3 %collective-permute-start = (bf16[4,256,384]{2,1,0:T(8,128)(2,1)S(1)}, bf16[4,256,384]{2,1,0:T(8,128)(2,1)S(1)}, u32[]{:S(2)}, u32[]{:S(2)}) collective-permute-start(bf16[4,256,384]{2,1,0:T(8,128)(2,1)S(1)} %all_to_all.35), channel_id=1, source_target_pairs={{0,1},{1,0},{2,3},{3,2},{4,5},{5,4},{6,7},{7,6},{8,9},{9,8},{10,11... | collective-permute-start | bytes 2359304 | tf_op jit(solution)/shard_map/ppermute | solution.py:44
  96.6 1.1 fusion.125
  97.7 1.1 fusion.95
  99.3 20.8 %all-to-all-done.2 = bf16[8,256,384]{2,1,0:T(8,128)(2,1)S(1)} async-done(((bf16[8,256,384]{2,1,0:T(8,128)(2,1)}), bf16[8,256,384]{2,1,0:T(8,128)(2,1)S(1)}, u32[]{:S(2)}, u32[]{:S(2)}) %all-to-all-start.2) | async-done | bytes 1572896 | tf_op jit(solution)/shard_map/all_to_all | solution.py:40
  121.0 0.7 fusion.81
  121.7 8.7 %all_to_all.36 = bf16[4,384,128]{2,1,0:T(8,128)(2,1)S(1)} all-to-all(bf16[4,384,128]{2,1,0:T(8,128)(2,1)S(1)} %broadcast_in_dim.15), channel_id=1, replica_groups=mesh['z'=8,'y'=8,'x'=4,'core'=2] {'x'}, dimensions={0} | all-to-all | bytes 786432 | tf_op jit(solution)/shard_map/all_to_all | solution.py:53
  130.4 10.5 %collective-permute-start.1 = (bf16[4,384,128]{2,1,0:T(8,128)(2,1)S(1)}, bf16[4,384,128]{2,1,0:T(8,128)(2,1)S(1)}, u32[]{:S(2)}, u32[]{:S(2)}) collective-permute-start(bf16[4,384,128]{2,1,0:T(8,128)(2,1)S(1)} %all_to_all.36), channel_id=1, source_target_pairs={{0,1},{1,0},{2,3},{3,2},{4,5},{5,4},{6,7},{7,6},{8,9},{9,8},{10,11... | collective-permute-start | bytes 1179656 | tf_op jit(solution)/shard_map/ppermute | solution.py:44
  142.7 0.6 fusion.17
  144.3 14.4 %all_to_all.37 = bf16[4,256,384]{2,1,0:T(8,128)(2,1)S(1)} all-to-all(bf16[4,256,384]{2,1,0:T(8,128)(2,1)S(1)} %broadcast_in_dim.16), channel_id=1, replica_groups=mesh['z'=8,'y'=8,'x'=4,'core'=2] {'x'}, dimensions={0} | all-to-all | bytes 1572864 | tf_op jit(solution)/shard_map/all_to_all | solution.py:53
  158.8 3.3 %collective-permute-start.2 = (bf16[4,256,384]{2,1,0:T(8,128)(2,1)S(1)}, bf16[4,256,384]{2,1,0:T(8,128)(2,1)S(1)}, u32[]{:S(2)}, u32[]{:S(2)}) collective-permute-start(bf16[4,256,384]{2,1,0:T(8,128)(2,1)S(1)} %all_to_all.37), channel_id=1, source_target_pairs={{0,1},{1,0},{2,3},{3,2},{4,5},{5,4},{6,7},{7,6},{8,9},{9,8},{10,11... | collective-permute-start | bytes 2359304 | tf_op jit(solution)/shard_map/ppermute | solution.py:44
  162.2 1.6 collective-permute-done.2
  165.6 8.0 %fusion.7 = bf16[2048,384]{1,0:T(8,128)(2,1)S(1)} fusion(bf16[2048,2048]{1,0:T(8,128)(2,1)} %all-gather.5.cloned.1.call-done, bf16[2048,384]{1,0:T(8,128)(2,1)S(1)} %bitcast.250), kind=kOutput, calls=%fused_computation.9 | convolution fusion | flops 3223191552 | bytes 11534336 | tf_op jit(solution)/shard_map/dot_general | solution.py:132
  173.9 2.3 %collective-permute-start.3 = (bf16[4,256,384]{2,1,0:T(8,128)(2,1)S(1)}, bf16[4,256,384]{2,1,0:T(8,128)(2,1)S(1)}, u32[]{:S(2)}, u32[]{:S(2)}) collective-permute-start(bf16[4,256,384]{2,1,0:T(8,128)(2,1)S(1)} %dynamic-slice_bitcast_fusion), channel_id=1, source_target_pairs={{0,1},{1,0},{2,3},{3,2},{4,5},{5,4},{6,7},{7,6},{8,9},{9,8},{10,11... | collective-permute-start | bytes 2359304 | tf_op jit(solution)/shard_map/ppermute | solution.py:44
  176.2 1.9 collective-permute-done.3
  178.1 1.1 fusion.10
  179.2 3.5 %all-to-all-start.5 = ((bf16[4,256,384]{2,1,0:T(8,128)(2,1)}), bf16[4,256,384]{2,1,0:T(8,128)(2,1)S(1)}, u32[]{:S(2)}, u32[]{:S(2)}) async-start(bf16[4,256,384]{2,1,0:T(8,128)(2,1)} %fusion.10), calls=%async_computation.5 | async-start | bytes 1572864 | tf_op jit(solution)/shard_map/all_to_all | solution.py:138
  182.8 11.9 %all-to-all-done.5 = bf16[4,256,384]{2,1,0:T(8,128)(2,1)S(1)} async-done(((bf16[4,256,384]{2,1,0:T(8,128)(2,1)}), bf16[4,256,384]{2,1,0:T(8,128)(2,1)S(1)}, u32[]{:S(2)}, u32[]{:S(2)}) %all-to-all-start.5) | async-done | bytes 786464 | tf_op jit(solution)/shard_map/all_to_all | solution.py:138
  195.0 0.6 broadcast_in_dim.17
  195.6 4.5 %all-to-all-start.6 = ((f32[8,2,384]{2,1,0:T(2,128)}), f32[8,2,384]{2,1,0:T(2,128)S(1)}, u32[]{:S(2)}, u32[]{:S(2)}) async-start(f32[8,2,384]{2,1,0:T(2,128)} %broadcast_in_dim.17), calls=%async_computation.6 | async-start | bytes 49152 | tf_op jit(solution)/shard_map/all_to_all | solution.py:144
  200.1 0.8 dynamic_slice.20
  200.8 3.9 %all-to-all-done.6 = f32[8,2,384]{2,1,0:T(2,128)S(1)} async-done(((f32[8,2,384]{2,1,0:T(2,128)}), f32[8,2,384]{2,1,0:T(2,128)S(1)}, u32[]{:S(2)}, u32[]{:S(2)}) %all-to-all-start.6) | async-done | bytes 24608 | tf_op jit(solution)/shard_map/all_to_all | solution.py:144
  204.9 0.8 copy.73
  (56 shorter events, 7.0 us)
Async XLA Ops:
  6.5 50.9 %copy-start = (bf16[384,256]{1,0:T(8,128)(2,1)S(1)}, bf16[384,256]{1,0:T(8,128)(2,1)}, u32[]{:S(2)}) copy-start(bf16[384,256]{1,0:T(8,128)(2,1)} %param.10) | copy-start | bytes 589828
  6.5 45.2 %all-gather.3.cloned.1.call-start = ((), (), s32[]{:S(2)}) async-start(), calls=%async_computation.7 | async-start | bytes 1179648 | tf_op jit(solution)/shard_map/all_gather | solution.py:95
  8.1 157.5 %all-gather.5.cloned.1.call-start = ((), (), s32[]{:S(2)}) async-start(), calls=%async_computation.8 | async-start | bytes 9437184 | tf_op jit(solution)/shard_map/all_gather | solution.py:96
  53.9 12.2 %all-to-all-start.1 = ((bf16[8,32,384]{2,1,0:T(8,128)(2,1)}), bf16[8,32,384]{2,1,0:T(8,128)(2,1)S(1)}, u32[]{:S(2)}, u32[]{:S(2)}) async-start(bf16[8,32,384]{2,1,0:T(8,128)(2,1)} %broadcast_in_dim.13), calls=%async_computation.1 | async-start | bytes 393216 | tf_op jit(solution)/shard_map/all_to_all | solution.py:40
  79.7 40.5 %all-to-all-start.2 = ((bf16[8,256,384]{2,1,0:T(8,128)(2,1)}), bf16[8,256,384]{2,1,0:T(8,128)(2,1)S(1)}, u32[]{:S(2)}, u32[]{:S(2)}) async-start(bf16[8,256,384]{2,1,0:T(8,128)(2,1)} %broadcast_in_dim.14), calls=%async_computation.2 | async-start | bytes 3145728 | tf_op jit(solution)/shard_map/all_to_all | solution.py:40
  88.3 10.5 %collective-permute-start = (bf16[4,256,384]{2,1,0:T(8,128)(2,1)S(1)}, bf16[4,256,384]{2,1,0:T(8,128)(2,1)S(1)}, u32[]{:S(2)}, u32[]{:S(2)}) collective-permute-start(bf16[4,256,384]{2,1,0:T(8,128)(2,1)S(1)} %all_to_all.35), channel_id=1, source_target_pairs={{0,1},{1,0},{2,3},{3,2},{4,5},{5,4},{6,7},{7,6},{8,9},{9,8},{10,11... | collective-permute-start | bytes 2359304 | tf_op jit(solution)/shard_map/ppermute | solution.py:44
  130.4 11.9 %collective-permute-start.1 = (bf16[4,384,128]{2,1,0:T(8,128)(2,1)S(1)}, bf16[4,384,128]{2,1,0:T(8,128)(2,1)S(1)}, u32[]{:S(2)}, u32[]{:S(2)}) collective-permute-start(bf16[4,384,128]{2,1,0:T(8,128)(2,1)S(1)} %all_to_all.36), channel_id=1, source_target_pairs={{0,1},{1,0},{2,3},{3,2},{4,5},{5,4},{6,7},{7,6},{8,9},{9,8},{10,11... | collective-permute-start | bytes 1179656 | tf_op jit(solution)/shard_map/ppermute | solution.py:44
  141.7 1.0 copy-start.2
  144.2 17.9 %copy-start.1 = (f32[2048]{0:T(1024)S(1)}, f32[2048]{0:T(1024)}, u32[]{:S(2)}) copy-start(f32[2048]{0:T(1024)} %param.16) | copy-start | bytes 24580
  158.8 5.0 %collective-permute-start.2 = (bf16[4,256,384]{2,1,0:T(8,128)(2,1)S(1)}, bf16[4,256,384]{2,1,0:T(8,128)(2,1)S(1)}, u32[]{:S(2)}, u32[]{:S(2)}) collective-permute-start(bf16[4,256,384]{2,1,0:T(8,128)(2,1)S(1)} %all_to_all.37), channel_id=1, source_target_pairs={{0,1},{1,0},{2,3},{3,2},{4,5},{5,4},{6,7},{7,6},{8,9},{9,8},{10,11... | collective-permute-start | bytes 2359304 | tf_op jit(solution)/shard_map/ppermute | solution.py:44
  173.9 4.2 %collective-permute-start.3 = (bf16[4,256,384]{2,1,0:T(8,128)(2,1)S(1)}, bf16[4,256,384]{2,1,0:T(8,128)(2,1)S(1)}, u32[]{:S(2)}, u32[]{:S(2)}) collective-permute-start(bf16[4,256,384]{2,1,0:T(8,128)(2,1)S(1)} %dynamic-slice_bitcast_fusion), channel_id=1, source_target_pairs={{0,1},{1,0},{2,3},{3,2},{4,5},{5,4},{6,7},{7,6},{8,9},{9,8},{10,11... | collective-permute-start | bytes 2359304 | tf_op jit(solution)/shard_map/ppermute | solution.py:44
  179.2 15.5 %all-to-all-start.5 = ((bf16[4,256,384]{2,1,0:T(8,128)(2,1)}), bf16[4,256,384]{2,1,0:T(8,128)(2,1)S(1)}, u32[]{:S(2)}, u32[]{:S(2)}) async-start(bf16[4,256,384]{2,1,0:T(8,128)(2,1)} %fusion.10), calls=%async_computation.5 | async-start | bytes 1572864 | tf_op jit(solution)/shard_map/all_to_all | solution.py:138
  195.6 9.2 %all-to-all-start.6 = ((f32[8,2,384]{2,1,0:T(2,128)}), f32[8,2,384]{2,1,0:T(2,128)S(1)}, u32[]{:S(2)}, u32[]{:S(2)}) async-start(f32[8,2,384]{2,1,0:T(2,128)} %broadcast_in_dim.17), calls=%async_computation.6 | async-start | bytes 49152 | tf_op jit(solution)/shard_map/all_to_all | solution.py:144
Sparse Core Ops, SparseCore 0:
  9.4 42.2 all-gather.2
  53.8 76.6 all-gather.4
where the time goes:
time: 213 us
  waiting for transfers between devices  92.8 us (44%)
  starting transfers between devices  44.6 us (21%)
  blocking collectives  35.3 us (17%)
  between operations  13.8 us (6%)
  other arithmetic  10.2 us (5%)
  matrix products  9.11 us (4%)
  local copies, waits for them, and re-layouts  6.93 us (3%)
    all_gather x1, waiting for transfers between devices, layer(): lax.all_gather(wide, ALL, axis=0, tiled=True, axis_index_groups=FIRST)  43.6 us
    all_to_all x3, blocking collectives, all_ranks(): mine = lax.all_to_all(copies, 'x', 0, 0, tiled=True)  35.3 us
    all_to_all x2, waiting for transfers between devices, sent_to_group(): lax.all_to_all(copies, ALL, 0, 0, axis_index_groups=groups, tiled=True)  29.3 us
    ppermute x4, starting transfers between devices, partner_of(): return lax.ppermute(a, 'core', [(0, 1), (1, 0)])  24.4 us
    all_to_all x2, starting transfers between devices, sent_to_group(): lax.all_to_all(copies, ALL, 0, 0, axis_index_groups=groups, tiled=True)  12.2 us
    all_to_all x1, waiting for transfers between devices, layer(): arrived = lax.all_to_all(pair, 'x', 0, 0, tiled=True)  11.9 us
    dot_general x1, matrix products, layer(): terms = jnp.dot(wide[:, units_part:], hidden, preferred_element_type=f32)  8.01 us
    all_to_all x1, starting transfers between devices, layer(): totals = jnp.sum(lax.all_to_all(copies, TP, 0, 0, tiled=True), 0)  4.47 us
  transfers between devices with their start and end apart: 10, of which 8 were waited for; matrix products, arithmetic and copies ran while one was open for 6% of the time, Pallas kernels for 0%

commit v1 on v0

--- a/solution.py
+++ b/solution.py
@@ -38,6 +38,22 @@
 def sent_to_group(shard, groups):
     copies = jnp.broadcast_to(shard, (SIDE, *shard.shape))
     return lax.all_to_all(copies, ALL, 0, 0, axis_index_groups=groups, tiled=True)
+
+
+def second_axis_pairs(by):
+    return [
+        (group[i], group[(i + by) % SIDE]) for group in SECOND for i in range(SIDE)
+    ]
+
+
+def doubled(piece):
+    for by in (1, 2, 4):
+        piece = jnp.concatenate([piece, lax.ppermute(piece, ALL, second_axis_pairs(-by))], 0)
+    return piece
+
+
+def along_x(a, by):
+    return lax.ppermute(a, "x", [(i, (i + by) % 4) for i in range(4)])
 
 
 def partner_of(a):
@@ -91,20 +107,26 @@
     def mine_of(vector, size):
         return lax.dynamic_slice_in_dim(vector, tp_rank * size, size, vector.ndim - 1)
 
-    wide = jnp.concatenate([w_up, w_down.T], 1)
-    wide = lax.all_gather(wide, ALL, axis=0, tiled=True, axis_index_groups=FIRST)
-    wide = lax.all_gather(wide, ALL, axis=0, tiled=True, axis_index_groups=SECOND)
-
+    own_xt = tokens.T
     mix_rows = w_mix_out.shape[0]
     halves = [w_mix_out[:, :channel_part], w_mix_out[:, channel_part:]]
-    small = jnp.concatenate([w_value, w_gate, jnp.concatenate(halves, 0)], 1)
-    small = sent_to_group(small, FIRST).reshape(-1, small.shape[1])
-    small = sent_to_group(small, SECOND)
-    value_gate = small[:, :, : 2 * channel_part].reshape(WIDTH, 2 * channel_part)
-    mix = small[:, :, 2 * channel_part :].reshape(SIDE, SIDE, 2, mix_rows, channel_part)
+    shard = jnp.concatenate([w_up, w_down.T, w_value, w_gate, jnp.concatenate(halves, 0)], 1)
+    shard = sent_to_group(shard, FIRST).reshape(-1, shard.shape[1])
+    at = 2 * units_part
+    wide = lax.all_gather(shard[:, :at], ALL, axis=0, tiled=True, axis_index_groups=SECOND)
+    value_gate = sent_to_group(shard[:, at : at + 2 * channel_part], SECOND)
+    value_gate = value_gate.reshape(WIDTH, 2 * channel_part)
+    mix = doubled(shard[None, :, at + 2 * channel_part :])
+    mix = jnp.roll(mix, jnp.where(core == 0, lax.axis_index("z"), lax.axis_index("y")), 0)
+    mix = mix.reshape(SIDE, SIDE, 2, mix_rows, channel_part)
     mix = turned(core, mix.transpose(0, 1, 3, 2, 4)).reshape(CHANNELS, width_part)
 
-    ranks = all_ranks(tokens.T, core)
+    x_rank = lax.axis_index("x")
+    mine = [own_xt, along_x(own_xt, -1), along_x(own_xt, 2), along_x(own_xt, 1)]
+    mine = jnp.stack(mine)
+    other = partner_of(mine)
+    mine, other = jnp.roll(mine, x_rank, 0), jnp.roll(other, x_rank, 0)
+    ranks = jnp.stack([jnp.where(core == 0, mine, other), jnp.where(core == 0, other, mine)], 1)
     ranks = turned(core, ranks.reshape(SIDE, SIDE, -1, frames)).reshape(WIDTH, frames)
 
     both = lax.dot_general(ranks, value_gate, (((0,), (0,)), ((), ())), preferred_element_type=f32)

time: 213 us -> 211 us (level)
  waiting for transfers between devices: 92.8 us -> 56.7 us
  local copies, waits for them, and re-layouts: 6.93 us -> 17.2 us
  blocking collectives: 35.3 us -> 45 us
  starting transfers between devices: 44.6 us -> 54.2 us
    all_gather x2 -> x1, waiting for transfers between devices: 43.6 us -> 0.02 us  [layer(): lax.all_gather(shard[:, :at], ALL, axis=0, tiled=True, axis_index_groups=...]
    ppermute x0 -> x6, waiting for transfers between devices: none -> 33.1 us  [the longest x3 23.8 us: doubled(): lax.ppermute(piece, ALL, second_axis_pairs(-by))]
    all_to_all x0 -> x1, blocking collectives: none -> 30.5 us  [sent_to_group(): lax.all_to_all(copies, ALL, 0, 0, axis_index_groups=groups, tiled=True)]
    all_to_all x2 -> x1, waiting for transfers between devices: 29.3 us -> 0.01 us  [sent_to_group(): lax.all_to_all(copies, ALL, 0, 0, axis_index_groups=groups, tiled=True)]
    ppermute x0 -> x6, starting transfers between devices: none -> 23.7 us  [the longest x3 14.4 us: doubled(): lax.ppermute(piece, ALL, second_axis_pairs(-by))]
    all_to_all x3 -> x1, blocking collectives: 35.3 us -> 14.5 us  [all_ranks(): mine = lax.all_to_all(copies, 'x', 0, 0, tiled=True)]
    ppermute x4, starting transfers between devices: 24.4 us -> 14.8 us  [partner_of(): return lax.ppermute(a, 'core', [(0, 1), (1, 0)])]
    all_to_all x2 -> x1, starting transfers between devices: 12.2 us -> 4.25 us  [sent_to_group(): lax.all_to_all(copies, ALL, 0, 0, axis_index_groups=groups, tiled=True)]
  transfers between devices with their start and end apart: 10 -> 15, of which waited for: 8 -> 11; matrix products, arithmetic and copies ran while one was open for 6% -> 11% of each run, Pallas kernels for 0% -> 0%
where the time goes in v1:
time: 211 us; the launch traced here: 210 us
  waiting for transfers between devices  56.7 us (27%)
  starting transfers between devices  54.2 us (26%)
  blocking collectives  45 us (21%)
  local copies, waits for them, and re-layouts  17.2 us (8%)
  between operations  14 us (7%)
  other arithmetic  12.2 us (6%)
  matrix products  10.3 us (5%)
    all_to_all x1, blocking collectives, sent_to_group(): lax.all_to_all(copies, ALL, 0, 0, axis_index_groups=groups, tiled=True)  30.5 us
    ppermute x3, waiting for transfers between devices, doubled(): lax.ppermute(piece, ALL, second_axis_pairs(-by))  23.8 us
    ppermute x4, starting transfers between devices, partner_of(): return lax.ppermute(a, 'core', [(0, 1), (1, 0)])  14.8 us
    all_to_all x1, blocking collectives, all_ranks(): mine = lax.all_to_all(copies, 'x', 0, 0, tiled=True)  14.5 us
    ppermute x3, starting transfers between devices, doubled(): lax.ppermute(piece, ALL, second_axis_pairs(-by))  14.4 us
    all_to_all x1, waiting for transfers between devices, layer(): arrived = lax.all_to_all(pair, 'x', 0, 0, tiled=True)  11.9 us
    ppermute x3, starting transfers between devices, along_x(): return lax.ppermute(a, 'x', [(i, (i + by) % 4) for i in range(4)])  9.33 us
    ppermute x3, waiting for transfers between devices, along_x(): return lax.ppermute(a, 'x', [(i, (i + by) % 4) for i in range(4)])  9.31 us
  transfers between devices with their start and end apart: 15, of which 11 were waited for; matrix products, arithmetic and copies ran while one was open for 11% of the time, Pallas kernels for 0%

profile of v1, /device:TPU:1, one launch (start us, length us, event | category | flops | bytes accessed | tf_op | source)
XLA Modules:
  0.0 209.7 jit_solution(14303746528108307607)
XLA Ops:
  10.4 30.5 %all_to_all.30 = bf16[8,32,2432]{2,1,0:T(8,128)(2,1)S(1)} all-to-all(bf16[8,32,2432]{2,1,0:T(8,128)(2,1)S(1)} %broadcast_in_dim.12), channel_id=1, replica_groups={{0,8,16,24,32,40,48,56},{64,72,80,88,96,104,112,120},{128,136,144,152,1..., dimensions={0} | all-to-all | bytes 2490368 | tf_op jit(solution)/shard_map/all_to_all | solution.py:40
  41.0 1.2 slice.293
  42.4 4.4 %collective-permute-start = (bf16[256,384]{1,0:T(8,128)(2,1)S(1)}, bf16[256,384]{1,0:T(8,128)(2,1)S(1)}, u32[]{:S(2)}, u32[]{:S(2)}) collective-permute-start(bf16[256,384]{1,0:T(8,128)(2,1)S(1)} %bitcast.266), channel_id=1, source_target_pairs={{0,6},{2,0},{4,2},{6,4},{1,7},{3,1},{5,3},{7,5},{8,14},{10,8},{12,... | collective-permute-start | bytes 589832 | tf_op jit(solution)/shard_map/ppermute | solution.py:56
  46.7 2.4 %collective-permute-start.1 = (bf16[256,384]{1,0:T(8,128)(2,1)S(1)}, bf16[256,384]{1,0:T(8,128)(2,1)S(1)}, u32[]{:S(2)}, u32[]{:S(2)}) collective-permute-start(bf16[256,384]{1,0:T(8,128)(2,1)S(1)} %bitcast.267), channel_id=1, source_target_pairs={{0,4},{2,6},{4,0},{6,2},{1,5},{3,7},{5,1},{7,3},{8,12},{10,14},{12... | collective-permute-start | bytes 589832 | tf_op jit(solution)/shard_map/ppermute | solution.py:56
  49.2 2.5 %collective-permute-start.2 = (bf16[256,384]{1,0:T(8,128)(2,1)S(1)}, bf16[256,384]{1,0:T(8,128)(2,1)}, u32[]{:S(2)}, u32[]{:S(2)}) collective-permute-start(bf16[256,384]{1,0:T(8,128)(2,1)S(1)} %bitcast.268), channel_id=1, source_target_pairs={{0,2},{2,4},{4,6},{6,0},{1,3},{3,5},{5,7},{7,1},{8,10},{10,12},{12... | collective-permute-start | bytes 589832 | tf_op jit(solution)/shard_map/ppermute | solution.py:56
  51.7 3.3 %collective-permute-done = bf16[256,384]{1,0:T(8,128)(2,1)S(1)} collective-permute-done((bf16[256,384]{1,0:T(8,128)(2,1)S(1)}, bf16[256,384]{1,0:T(8,128)(2,1)S(1)}, u32[]{:S(2)}, u32[]{:S(2)}) %collective-permute-start) | collective-permute-done | bytes 196640 | tf_op jit(solution)/shard_map/ppermute | solution.py:56
  55.0 1.8 collective-permute-done.1
  56.8 4.2 %collective-permute-done.2 = bf16[256,384]{1,0:T(8,128)(2,1)} collective-permute-done((bf16[256,384]{1,0:T(8,128)(2,1)S(1)}, bf16[256,384]{1,0:T(8,128)(2,1)}, u32[]{:S(2)}, u32[]{:S(2)}) %collective-permute-start.2) | collective-permute-done | bytes 196640 | tf_op jit(solution)/shard_map/ppermute | solution.py:56
  62.1 2.3 %collective-permute-start.3 = (bf16[4,256,384]{2,1,0:T(8,128)(2,1)S(1)}, bf16[4,256,384]{2,1,0:T(8,128)(2,1)S(1)}, u32[]{:S(2)}, u32[]{:S(2)}) collective-permute-start(bf16[4,256,384]{2,1,0:T(8,128)(2,1)S(1)} %pad_maximum_fusion.1), channel_id=1, source_target_pairs={{0,1},{1,0},{2,3},{3,2},{4,5},{5,4},{6,7},{7,6},{8,9},{9,8},{10,11... | collective-permute-start | bytes 2359304 | tf_op jit(solution)/shard_map/ppermute | solution.py:60
  64.4 1.7 fusion.133
  68.3 4.3 %all-to-all-start.1 = ((bf16[8,256,256]{2,1,0:T(8,128)(2,1)}), bf16[8,256,256]{2,1,0:T(8,128)(2,1)}, u32[]{:S(2)}, u32[]{:S(2)}) async-start(bf16[8,256,256]{2,1,0:T(8,128)(2,1)} %broadcast_in_dim.13), calls=%async_computation.1 | async-start | bytes 2097152 | tf_op jit(solution)/shard_map/all_to_all | solution.py:40
  72.6 2.3 %select_bitcast_fusion.3 = (bf16[4,1,256,384]{3,2,1,0:T(8,128)(2,1)S(1)}, bf16[4,256,384]{2,1,0:T(8,128)(2,1)S(1)}) fusion(pred[]{:T(512)S(6)} %eq.6, s32[]{:T(128)S(6)} %select_n.117, bf16[4,256,384]{2,1,0:T(8,128)(2,1)S(1)} %collective-permute-done.3, bf16[1,256,384]{2,1,0:T(8,128)(2,1)} %bitcast.5, bf16[1,256,384]{2,1,0:T(8,128)(2,1)S(1)} %bitcast.276, ...), kind=kLoop, calls=%fused_computation.57 | loop fusion | flops 3538944 | bytes 3145733 | tf_op jit(solution)/shard_map/stack | solution.py:129
  75.3 4.5 %collective-permute-start.5 = (bf16[1,256,128]{2,1,0:T(8,128)(2,1)S(1)}, bf16[1,256,128]{2,1,0:T(8,128)(2,1)S(1)}, u32[]{:S(2)}, u32[]{:S(2)}) collective-permute-start(bf16[1,256,128]{2,1,0:T(8,128)(2,1)S(1)} %slice_bitcast_fusion), channel_id=1, source_target_pairs={{0,448},{64,0},{128,64},{192,128},{256,192},{320,256},{384,320},{4... | collective-permute-start | bytes 196616 | tf_op jit(solution)/shard_map/ppermute | solution.py:51
  80.0 13.8 %collective-permute-done.5 = bf16[1,256,128]{2,1,0:T(8,128)(2,1)S(1)} collective-permute-done((bf16[1,256,128]{2,1,0:T(8,128)(2,1)S(1)}, bf16[1,256,128]{2,1,0:T(8,128)(2,1)S(1)}, u32[]{:S(2)}, u32[]{:S(2)}) %collective-permute-start.5) | collective-permute-done | bytes 65568 | tf_op jit(solution)/shard_map/ppermute | solution.py:51
  93.8 4.3 %collective-permute-start.6 = (bf16[2,256,128]{2,1,0:T(8,128)(2,1)S(1)}, bf16[2,256,128]{2,1,0:T(8,128)(2,1)S(1)}, u32[]{:S(2)}, u32[]{:S(2)}) collective-permute-start(bf16[2,256,128]{2,1,0:T(8,128)(2,1)S(1)} %pad_maximum_fusion.4), channel_id=1, source_target_pairs={{0,384},{64,448},{128,0},{192,64},{256,128},{320,192},{384,256},{4... | collective-permute-start | bytes 393224 | tf_op jit(solution)/shard_map/ppermute | solution.py:51
  98.3 5.4 %collective-permute-done.6 = bf16[2,256,128]{2,1,0:T(8,128)(2,1)S(1)} collective-permute-done((bf16[2,256,128]{2,1,0:T(8,128)(2,1)S(1)}, bf16[2,256,128]{2,1,0:T(8,128)(2,1)S(1)}, u32[]{:S(2)}, u32[]{:S(2)}) %collective-permute-start.6) | collective-permute-done | bytes 131104 | tf_op jit(solution)/shard_map/ppermute | solution.py:51
  103.7 5.6 %collective-permute-start.7 = (bf16[4,256,128]{2,1,0:T(8,128)(2,1)S(1)}, bf16[4,256,128]{2,1,0:T(8,128)(2,1)S(1)}, u32[]{:S(2)}, u32[]{:S(2)}) collective-permute-start(bf16[4,256,128]{2,1,0:T(8,128)(2,1)S(1)} %pad_maximum_fusion.3), channel_id=1, source_target_pairs={{0,256},{64,320},{128,384},{192,448},{256,0},{320,64},{384,128},{4... | collective-permute-start | bytes 786440 | tf_op jit(solution)/shard_map/ppermute | solution.py:51
  111.2 4.6 %collective-permute-done.7 = bf16[4,256,128]{2,1,0:T(8,128)(2,1)S(1)} collective-permute-done((bf16[4,256,128]{2,1,0:T(8,128)(2,1)S(1)}, bf16[4,256,128]{2,1,0:T(8,128)(2,1)S(1)}, u32[]{:S(2)}, u32[]{:S(2)}) %collective-permute-start.7) | collective-permute-done | bytes 262176 | tf_op jit(solution)/shard_map/ppermute | solution.py:51
  116.6 1.8 fusion.138
  120.2 3.5 %all-to-all-start.2 = ((bf16[4,384,128]{2,1,0:T(8,128)(2,1)}), bf16[4,384,128]{2,1,0:T(8,128)(2,1)S(1)}, u32[]{:S(2)}, u32[]{:S(2)}) async-start(bf16[4,384,128]{2,1,0:T(8,128)(2,1)} %broadcast_in_dim.14), calls=%async_computation.2 | async-start | bytes 786432 | tf_op jit(solution)/shard_map/all_to_all | solution.py:69
  125.5 4.3 %all-to-all-done.2 = bf16[4,384,128]{2,1,0:T(8,128)(2,1)S(1)} async-done(((bf16[4,384,128]{2,1,0:T(8,128)(2,1)}), bf16[4,384,128]{2,1,0:T(8,128)(2,1)S(1)}, u32[]{:S(2)}, u32[]{:S(2)}) %all-to-all-start.2) | async-done | bytes 393248 | tf_op jit(solution)/shard_map/all_to_all | solution.py:69
  129.8 7.0 %collective-permute-start.4 = (bf16[4,384,128]{2,1,0:T(8,128)(2,1)S(1)}, bf16[4,384,128]{2,1,0:T(8,128)(2,1)S(1)}, u32[]{:S(2)}, u32[]{:S(2)}) collective-permute-start(bf16[4,384,128]{2,1,0:T(8,128)(2,1)S(1)} %all-to-all-done.2), channel_id=1, source_target_pairs={{0,1},{1,0},{2,3},{3,2},{4,5},{5,4},{6,7},{7,6},{8,9},{9,8},{10,11... | collective-permute-start | bytes 1179656 | tf_op jit(solution)/shard_map/ppermute | solution.py:60
  141.4 14.5 %all_to_all.31 = bf16[4,256,384]{2,1,0:T(8,128)(2,1)S(1)} all-to-all(bf16[4,256,384]{2,1,0:T(8,128)(2,1)S(1)} %broadcast_in_dim.16), channel_id=1, replica_groups=mesh['z'=8,'y'=8,'x'=4,'core'=2] {'x'}, dimensions={0} | all-to-all | bytes 1572864 | tf_op jit(solution)/shard_map/all_to_all | solution.py:69
  155.9 3.2 %collective-permute-start.8 = (bf16[4,256,384]{2,1,0:T(8,128)(2,1)S(1)}, bf16[4,256,384]{2,1,0:T(8,128)(2,1)S(1)}, u32[]{:S(2)}, u32[]{:S(2)}) collective-permute-start(bf16[4,256,384]{2,1,0:T(8,128)(2,1)S(1)} %all_to_all.31), channel_id=1, source_target_pairs={{0,1},{1,0},{2,3},{3,2},{4,5},{5,4},{6,7},{7,6},{8,9},{9,8},{10,11... | collective-permute-start | bytes 2359304 | tf_op jit(solution)/shard_map/ppermute | solution.py:60
  159.3 1.6 collective-permute-done.8
  162.8 8.0 %fusion.7 = bf16[2048,384]{1,0:T(8,128)(2,1)S(1)} fusion(bf16[2048,2048]{1,0:T(8,128)(2,1)} %all-gather.2.cloned.1.call-done, bf16[2048,384]{1,0:T(8,128)(2,1)S(1)} %bitcast.271), kind=kOutput, calls=%fused_computation.9 | convolution fusion | flops 3223191552 | bytes 11534336 | tf_op jit(solution)/shard_map/dot_general | solution.py:154
  171.0 2.3 %collective-permute-start.9 = (bf16[4,256,384]{2,1,0:T(8,128)(2,1)S(1)}, bf16[4,256,384]{2,1,0:T(8,128)(2,1)S(1)}, u32[]{:S(2)}, u32[]{:S(2)}) collective-permute-start(bf16[4,256,384]{2,1,0:T(8,128)(2,1)S(1)} %dynamic-slice_bitcast_fusion), channel_id=1, source_target_pairs={{0,1},{1,0},{2,3},{3,2},{4,5},{5,4},{6,7},{7,6},{8,9},{9,8},{10,11... | collective-permute-start | bytes 2359304 | tf_op jit(solution)/shard_map/ppermute | solution.py:60
  173.3 1.9 collective-permute-done.9
  176.3 3.5 %all-to-all-start.4 = ((bf16[4,256,384]{2,1,0:T(8,128)(2,1)}), bf16[4,256,384]{2,1,0:T(8,128)(2,1)S(1)}, u32[]{:S(2)}, u32[]{:S(2)}) async-start(bf16[4,256,384]{2,1,0:T(8,128)(2,1)} %fusion.10), calls=%async_computation.4 | async-start | bytes 1572864 | tf_op jit(solution)/shard_map/all_to_all | solution.py:160
  179.9 11.9 %all-to-all-done.4 = bf16[4,256,384]{2,1,0:T(8,128)(2,1)S(1)} async-done(((bf16[4,256,384]{2,1,0:T(8,128)(2,1)}), bf16[4,256,384]{2,1,0:T(8,128)(2,1)S(1)}, u32[]{:S(2)}, u32[]{:S(2)}) %all-to-all-start.4) | async-done | bytes 786464 | tf_op jit(solution)/shard_map/all_to_all | solution.py:160
  192.7 4.5 %all-to-all-start.5 = ((f32[8,2,384]{2,1,0:T(2,128)}), f32[8,2,384]{2,1,0:T(2,128)S(1)}, u32[]{:S(2)}, u32[]{:S(2)}) async-start(f32[8,2,384]{2,1,0:T(2,128)} %broadcast_in_dim.17), calls=%async_computation.5 | async-start | bytes 49152 | tf_op jit(solution)/shard_map/all_to_all | solution.py:166
  197.9 3.9 %all-to-all-done.5 = f32[8,2,384]{2,1,0:T(2,128)S(1)} async-done(((f32[8,2,384]{2,1,0:T(2,128)}), f32[8,2,384]{2,1,0:T(2,128)S(1)}, u32[]{:S(2)}, u32[]{:S(2)}) %all-to-all-start.5) | async-done | bytes 24608 | tf_op jit(solution)/shard_map/all_to_all | solution.py:166
  (101 shorter events, 24.8 us)
Async XLA Ops:
  6.5 156.2 %all-gather.2.cloned.1.call-start = ((), (), s32[]{:S(2)}) async-start(), calls=%async_computation.6 | async-start | bytes 9437184 | tf_op jit(solution)/shard_map/all_gather | solution.py:116
  41.0 1.2 copy-start
  42.4 12.7 %collective-permute-start = (bf16[256,384]{1,0:T(8,128)(2,1)S(1)}, bf16[256,384]{1,0:T(8,128)(2,1)S(1)}, u32[]{:S(2)}, u32[]{:S(2)}) collective-permute-start(bf16[256,384]{1,0:T(8,128)(2,1)S(1)} %bitcast.266), channel_id=1, source_target_pairs={{0,6},{2,0},{4,2},{6,4},{1,7},{3,1},{5,3},{7,5},{8,14},{10,8},{12,... | collective-permute-start | bytes 589832 | tf_op jit(solution)/shard_map/ppermute | solution.py:56
  46.7 10.0 %collective-permute-start.1 = (bf16[256,384]{1,0:T(8,128)(2,1)S(1)}, bf16[256,384]{1,0:T(8,128)(2,1)S(1)}, u32[]{:S(2)}, u32[]{:S(2)}) collective-permute-start(bf16[256,384]{1,0:T(8,128)(2,1)S(1)} %bitcast.267), channel_id=1, source_target_pairs={{0,4},{2,6},{4,0},{6,2},{1,5},{3,7},{5,1},{7,3},{8,12},{10,14},{12... | collective-permute-start | bytes 589832 | tf_op jit(solution)/shard_map/ppermute | solution.py:56
  49.2 11.8 %collective-permute-start.2 = (bf16[256,384]{1,0:T(8,128)(2,1)S(1)}, bf16[256,384]{1,0:T(8,128)(2,1)}, u32[]{:S(2)}, u32[]{:S(2)}) collective-permute-start(bf16[256,384]{1,0:T(8,128)(2,1)S(1)} %bitcast.268), channel_id=1, source_target_pairs={{0,2},{2,4},{4,6},{6,0},{1,3},{3,5},{5,7},{7,1},{8,10},{10,12},{12... | collective-permute-start | bytes 589832 | tf_op jit(solution)/shard_map/ppermute | solution.py:56
  62.1 10.5 %collective-permute-start.3 = (bf16[4,256,384]{2,1,0:T(8,128)(2,1)S(1)}, bf16[4,256,384]{2,1,0:T(8,128)(2,1)S(1)}, u32[]{:S(2)}, u32[]{:S(2)}) collective-permute-start(bf16[4,256,384]{2,1,0:T(8,128)(2,1)S(1)} %pad_maximum_fusion.1), channel_id=1, source_target_pairs={{0,1},{1,0},{2,3},{3,2},{4,5},{5,4},{6,7},{7,6},{8,9},{9,8},{10,11... | collective-permute-start | bytes 2359304 | tf_op jit(solution)/shard_map/ppermute | solution.py:60
  68.3 48.2 %all-to-all-start.1 = ((bf16[8,256,256]{2,1,0:T(8,128)(2,1)}), bf16[8,256,256]{2,1,0:T(8,128)(2,1)}, u32[]{:S(2)}, u32[]{:S(2)}) async-start(bf16[8,256,256]{2,1,0:T(8,128)(2,1)} %broadcast_in_dim.13), calls=%async_computation.1 | async-start | bytes 2097152 | tf_op jit(solution)/shard_map/all_to_all | solution.py:40
  75.3 18.5 %collective-permute-start.5 = (bf16[1,256,128]{2,1,0:T(8,128)(2,1)S(1)}, bf16[1,256,128]{2,1,0:T(8,128)(2,1)S(1)}, u32[]{:S(2)}, u32[]{:S(2)}) collective-permute-start(bf16[1,256,128]{2,1,0:T(8,128)(2,1)S(1)} %slice_bitcast_fusion), channel_id=1, source_target_pairs={{0,448},{64,0},{128,64},{192,128},{256,192},{320,256},{384,320},{4... | collective-permute-start | bytes 196616 | tf_op jit(solution)/shard_map/ppermute | solution.py:51
  93.8 9.9 %collective-permute-start.6 = (bf16[2,256,128]{2,1,0:T(8,128)(2,1)S(1)}, bf16[2,256,128]{2,1,0:T(8,128)(2,1)S(1)}, u32[]{:S(2)}, u32[]{:S(2)}) collective-permute-start(bf16[2,256,128]{2,1,0:T(8,128)(2,1)S(1)} %pad_maximum_fusion.4), channel_id=1, source_target_pairs={{0,384},{64,448},{128,0},{192,64},{256,128},{320,192},{384,256},{4... | collective-permute-start | bytes 393224 | tf_op jit(solution)/shard_map/ppermute | solution.py:51
  103.7 12.1 %collective-permute-start.7 = (bf16[4,256,128]{2,1,0:T(8,128)(2,1)S(1)}, bf16[4,256,128]{2,1,0:T(8,128)(2,1)S(1)}, u32[]{:S(2)}, u32[]{:S(2)}) collective-permute-start(bf16[4,256,128]{2,1,0:T(8,128)(2,1)S(1)} %pad_maximum_fusion.3), channel_id=1, source_target_pairs={{0,256},{64,320},{128,384},{192,448},{256,0},{320,64},{384,128},{4... | collective-permute-start | bytes 786440 | tf_op jit(solution)/shard_map/ppermute | solution.py:51
  116.6 2.0 copy-start.3
  116.6 2.0 copy-start.4
  116.6 2.0 copy-start.5
  116.6 2.0 copy-start.6
  116.6 2.0 copy-start.7
  116.6 2.0 copy-start.8
  116.6 2.0 copy-start.9
  116.6 2.0 copy-start.10
  116.6 2.0 copy-start.11
  116.6 2.0 copy-start.12
  116.6 2.0 copy-start.13
  120.2 9.7 %all-to-all-start.2 = ((bf16[4,384,128]{2,1,0:T(8,128)(2,1)}), bf16[4,384,128]{2,1,0:T(8,128)(2,1)S(1)}, u32[]{:S(2)}, u32[]{:S(2)}) async-start(bf16[4,384,128]{2,1,0:T(8,128)(2,1)} %broadcast_in_dim.14), calls=%async_computation.2 | async-start | bytes 786432 | tf_op jit(solution)/shard_map/all_to_all | solution.py:69
  129.8 9.3 %collective-permute-start.4 = (bf16[4,384,128]{2,1,0:T(8,128)(2,1)S(1)}, bf16[4,384,128]{2,1,0:T(8,128)(2,1)S(1)}, u32[]{:S(2)}, u32[]{:S(2)}) collective-permute-start(bf16[4,384,128]{2,1,0:T(8,128)(2,1)S(1)} %all-to-all-done.2), channel_id=1, source_target_pairs={{0,1},{1,0},{2,3},{3,2},{4,5},{5,4},{6,7},{7,6},{8,9},{9,8},{10,11... | collective-permute-start | bytes 1179656 | tf_op jit(solution)/shard_map/ppermute | solution.py:60
  139.1 0.7 copy-start.2
  141.3 17.9 %copy-start.1 = (f32[2048]{0:T(1024)S(1)}, f32[2048]{0:T(1024)}, u32[]{:S(2)}) copy-start(f32[2048]{0:T(1024)} %param.18) | copy-start | bytes 24580
  155.9 5.0 %collective-permute-start.8 = (bf16[4,256,384]{2,1,0:T(8,128)(2,1)S(1)}, bf16[4,256,384]{2,1,0:T(8,128)(2,1)S(1)}, u32[]{:S(2)}, u32[]{:S(2)}) collective-permute-start(bf16[4,256,384]{2,1,0:T(8,128)(2,1)S(1)} %all_to_all.31), channel_id=1, source_target_pairs={{0,1},{1,0},{2,3},{3,2},{4,5},{5,4},{6,7},{7,6},{8,9},{9,8},{10,11... | collective-permute-start | bytes 2359304 | tf_op jit(solution)/shard_map/ppermute | solution.py:60
  171.0 4.2 %collective-permute-start.9 = (bf16[4,256,384]{2,1,0:T(8,128)(2,1)S(1)}, bf16[4,256,384]{2,1,0:T(8,128)(2,1)S(1)}, u32[]{:S(2)}, u32[]{:S(2)}) collective-permute-start(bf16[4,256,384]{2,1,0:T(8,128)(2,1)S(1)} %dynamic-slice_bitcast_fusion), channel_id=1, source_target_pairs={{0,1},{1,0},{2,3},{3,2},{4,5},{5,4},{6,7},{7,6},{8,9},{9,8},{10,11... | collective-permute-start | bytes 2359304 | tf_op jit(solution)/shard_map/ppermute | solution.py:60
  176.3 15.5 %all-to-all-start.4 = ((bf16[4,256,384]{2,1,0:T(8,128)(2,1)}), bf16[4,256,384]{2,1,0:T(8,128)(2,1)S(1)}, u32[]{:S(2)}, u32[]{:S(2)}) async-start(bf16[4,256,384]{2,1,0:T(8,128)(2,1)} %fusion.10), calls=%async_computation.4 | async-start | bytes 1572864 | tf_op jit(solution)/shard_map/all_to_all | solution.py:160
  192.7 9.2 %all-to-all-start.5 = ((f32[8,2,384]{2,1,0:T(2,128)}), f32[8,2,384]{2,1,0:T(2,128)S(1)}, u32[]{:S(2)}, u32[]{:S(2)}) async-start(f32[8,2,384]{2,1,0:T(2,128)} %broadcast_in_dim.17), calls=%async_computation.5 | async-start | bytes 49152 | tf_op jit(solution)/shard_map/all_to_all | solution.py:166
Sparse Core Ops, SparseCore 0:
  42.3 68.4 all-gather.1

commit v2 on v0

--- a/solution.py
+++ b/solution.py
@@ -33,11 +33,17 @@
 
 
 FIRST, SECOND = rings("yz"), rings("zy")
+FOURS = [group[parity::2] for group in FIRST for parity in range(2)]
+PAIRS = [(a, group[i ^ 1]) for group in FIRST for i, a in enumerate(group)]
 
 
 def sent_to_group(shard, groups):
     copies = jnp.broadcast_to(shard, (SIDE, *shard.shape))
     return lax.all_to_all(copies, ALL, 0, 0, axis_index_groups=groups, tiled=True)
+
+
+def along_x(a, by):
+    return lax.ppermute(a, "x", [(i, (i + by) % 4) for i in range(4)])
 
 
 def partner_of(a):
@@ -92,7 +98,11 @@
         return lax.dynamic_slice_in_dim(vector, tp_rank * size, size, vector.ndim - 1)
 
     wide = jnp.concatenate([w_up, w_down.T], 1)
-    wide = lax.all_gather(wide, ALL, axis=0, tiled=True, axis_index_groups=FIRST)
+    place = jnp.where(core == 0, lax.axis_index("y"), lax.axis_index("z"))
+    met = lax.ppermute(wide, ALL, PAIRS)
+    even = place % 2 == 0
+    wide = jnp.concatenate([jnp.where(even, wide, met), jnp.where(even, met, wide)], 0)
+    wide = lax.all_gather(wide, ALL, axis=0, tiled=True, axis_index_groups=FOURS)
     wide = lax.all_gather(wide, ALL, axis=0, tiled=True, axis_index_groups=SECOND)
 
     mix_rows = w_mix_out.shape[0]
@@ -104,7 +114,13 @@
     mix = small[:, :, 2 * channel_part :].reshape(SIDE, SIDE, 2, mix_rows, channel_part)
     mix = turned(core, mix.transpose(0, 1, 3, 2, 4)).reshape(CHANNELS, width_part)
 
-    ranks = all_ranks(tokens.T, core)
+    x_rank = lax.axis_index("x")
+    own_xt = tokens.T
+    parts = [own_xt, along_x(own_xt, -1), along_x(own_xt, 2), along_x(own_xt, 1)]
+    mine = jnp.stack(parts)
+    other = partner_of(mine)
+    mine, other = jnp.roll(mine, x_rank, 0), jnp.roll(other, x_rank, 0)
+    ranks = jnp.stack([jnp.where(core == 0, mine, other), jnp.where(core == 0, other, mine)], 1)
     ranks = turned(core, ranks.reshape(SIDE, SIDE, -1, frames)).reshape(WIDTH, frames)
 
     both = lax.dot_general(ranks, value_gate, (((0,), (0,)), ((), ())), preferred_element_type=f32)

time: 213 us -> 198 us (0.930)
  waiting for transfers between devices: 92.8 us -> 70.7 us
  starting transfers between devices: 44.6 us -> 48.2 us
  other arithmetic: 10.2 us -> 13 us
    all_to_all x2 -> x1, waiting for transfers between devices: 29.3 us -> 5.33 us  [sent_to_group(): lax.all_to_all(copies, ALL, 0, 0, axis_index_groups=groups, tiled=True)]
    ppermute x0 -> x4, starting transfers between devices: none -> 13.8 us  [the longest x3 8.99 us: along_x(): return lax.ppermute(a, 'x', [(i, (i + by) % 4) for i in range(4)])]
    all_to_all x0 -> x1, blocking collectives: none -> 12.4 us  [sent_to_group(): lax.all_to_all(copies, ALL, 0, 0, axis_index_groups=groups, tiled=True)]
    all_to_all x3 -> x2, blocking collectives: 35.3 us -> 24.2 us  [all_ranks(): mine = lax.all_to_all(copies, 'x', 0, 0, tiled=True)]
    ppermute x0 -> x4, waiting for transfers between devices: none -> 8.24 us  [the longest x3 5.92 us: along_x(): return lax.ppermute(a, 'x', [(i, (i + by) % 4) for i in range(4)])]
    all_gather x1, waiting for transfers between devices: 43.6 us -> 37.1 us  [layer(): lax.all_gather(wide, ALL, axis=0, tiled=True, axis_index_groups=FOURS)]
    all_to_all x2 -> x1, starting transfers between devices: 12.2 us -> 6.73 us  [sent_to_group(): lax.all_to_all(copies, ALL, 0, 0, axis_index_groups=groups, tiled=True)]
    ppermute x4, starting transfers between devices: 24.4 us -> 19.7 us  [partner_of(): return lax.ppermute(a, 'core', [(0, 1), (1, 0)])]
  transfers between devices with their start and end apart: 10 -> 13, of which waited for: 8 -> 10; matrix products, arithmetic and copies ran while one was open for 6% -> 7% of each run, Pallas kernels for 0% -> 0%
where the time goes in v2:
time: 198 us; the launch traced here: 197 us
  waiting for transfers between devices  70.7 us (36%)
  starting transfers between devices  48.2 us (24%)
  blocking collectives  36.5 us (18%)
  between operations  13.9 us (7%)
  other arithmetic  13 us (7%)
  matrix products  9.11 us (5%)
  local copies, waits for them, and re-layouts  5.3 us (3%)
    all_gather x1, waiting for transfers between devices, layer(): lax.all_gather(wide, ALL, axis=0, tiled=True, axis_index_groups=FOURS)  37.1 us
    all_to_all x2, blocking collectives, all_ranks(): mine = lax.all_to_all(copies, 'x', 0, 0, tiled=True)  24.2 us
    ppermute x4, starting transfers between devices, partner_of(): return lax.ppermute(a, 'core', [(0, 1), (1, 0)])  19.7 us
    all_to_all x1, blocking collectives, sent_to_group(): lax.all_to_all(copies, ALL, 0, 0, axis_index_groups=groups, tiled=True)  12.4 us
    all_to_all x1, waiting for transfers between devices, layer(): arrived = lax.all_to_all(pair, 'x', 0, 0, tiled=True)  11.9 us
    ppermute x3, starting transfers between devices, along_x(): return lax.ppermute(a, 'x', [(i, (i + by) % 4) for i in range(4)])  8.99 us
    dot_general x1, matrix products, layer(): terms = jnp.dot(wide[:, units_part:], hidden, preferred_element_type=f32)  8.01 us
    all_to_all x1, starting transfers between devices, sent_to_group(): lax.all_to_all(copies, ALL, 0, 0, axis_index_groups=groups, tiled=True)  6.73 us
  transfers between devices with their start and end apart: 13, of which 10 were waited for; matrix products, arithmetic and copies ran while one was open for 7% of the time, Pallas kernels for 0%

profile of v2, /device:TPU:1, one launch (start us, length us, event | category | flops | bytes accessed | tf_op | source)
XLA Modules:
  0.0 196.8 jit_solution(2402831299061875664)
XLA Ops:
  6.5 0.9 pad_maximum_fusion.4
  7.5 4.8 %collective-permute-start.6 = (bf16[32,2048]{1,0:T(8,128)(2,1)S(1)}, bf16[32,2048]{1,0:T(8,128)(2,1)S(1)}, u32[]{:S(2)}, u32[]{:S(2)}) collective-permute-start(bf16[32,2048]{1,0:T(8,128)(2,1)S(1)} %pad_maximum_fusion.4), channel_id=1, source_target_pairs={{0,8},{8,0},{16,24},{24,16},{32,40},{40,32},{48,56},{56,48},{64,72... | collective-permute-start | bytes 393224 | tf_op jit(solution)/shard_map/ppermute | solution.py:102
  12.3 2.3 %collective-permute-done.6 = bf16[32,2048]{1,0:T(8,128)(2,1)S(1)} collective-permute-done((bf16[32,2048]{1,0:T(8,128)(2,1)S(1)}, bf16[32,2048]{1,0:T(8,128)(2,1)S(1)}, u32[]{:S(2)}, u32[]{:S(2)}) %collective-permute-start.6) | collective-permute-done | bytes 131104 | tf_op jit(solution)/shard_map/ppermute | solution.py:102
  14.6 0.9 broadcast_select_fusion.1
  16.3 37.1 %all-gather.3.cloned.1.call-done = bf16[256,2048]{1,0:T(8,128)(2,1)} async-done(((bf16[64,2048]{1,0:T(8,128)(2,1)}), bf16[256,2048]{1,0:T(8,128)(2,1)}) %all-gather.3.cloned.1.call-update) | async-done | bytes 1048592 | tf_op jit(solution)/shard_map/all_gather | solution.py:105
  53.5 12.4 %all_to_all.30 = bf16[8,32,384]{2,1,0:T(8,128)(2,1)S(1)} all-to-all(bf16[8,32,384]{2,1,0:T(8,128)(2,1)S(1)} %broadcast_in_dim.10), channel_id=1, replica_groups={{0,8,16,24,32,40,48,56},{64,72,80,88,96,104,112,120},{128,136,144,152,1..., dimensions={0} | all-to-all | bytes 393216 | tf_op jit(solution)/shard_map/all_to_all | solution.py:42
  65.9 1.3 broadcast_in_dim.11
  67.2 6.7 %all-to-all-start.1 = ((bf16[8,256,384]{2,1,0:T(8,128)(2,1)}), bf16[8,256,384]{2,1,0:T(8,128)(2,1)S(1)}, u32[]{:S(2)}, u32[]{:S(2)}) async-start(bf16[8,256,384]{2,1,0:T(8,128)(2,1)} %broadcast_in_dim.11), calls=%async_computation.1 | async-start | bytes 3145728 | tf_op jit(solution)/shard_map/all_to_all | solution.py:42
  74.1 4.3 %collective-permute-start = (bf16[256,384]{1,0:T(8,128)(2,1)S(1)}, bf16[256,384]{1,0:T(8,128)(2,1)S(1)}, u32[]{:S(2)}, u32[]{:S(2)}) collective-permute-start(bf16[256,384]{1,0:T(8,128)(2,1)S(1)} %bitcast.255), channel_id=1, source_target_pairs={{0,6},{2,0},{4,2},{6,4},{1,7},{3,1},{5,3},{7,5},{8,14},{10,8},{12,... | collective-permute-start | bytes 589832 | tf_op jit(solution)/shard_map/ppermute | solution.py:46
  78.4 2.2 %collective-permute-start.1 = (bf16[256,384]{1,0:T(8,128)(2,1)S(1)}, bf16[256,384]{1,0:T(8,128)(2,1)S(1)}, u32[]{:S(2)}, u32[]{:S(2)}) collective-permute-start(bf16[256,384]{1,0:T(8,128)(2,1)S(1)} %bitcast.256), channel_id=1, source_target_pairs={{0,4},{2,6},{4,0},{6,2},{1,5},{3,7},{5,1},{7,3},{8,12},{10,14},{12... | collective-permute-start | bytes 589832 | tf_op jit(solution)/shard_map/ppermute | solution.py:46
  80.6 2.5 %collective-permute-start.2 = (bf16[256,384]{1,0:T(8,128)(2,1)S(1)}, bf16[256,384]{1,0:T(8,128)(2,1)S(1)}, u32[]{:S(2)}, u32[]{:S(2)}) collective-permute-start(bf16[256,384]{1,0:T(8,128)(2,1)S(1)} %bitcast.257), channel_id=1, source_target_pairs={{0,2},{2,4},{4,6},{6,0},{1,3},{3,5},{5,7},{7,1},{8,10},{10,12},{12... | collective-permute-start | bytes 589832 | tf_op jit(solution)/shard_map/ppermute | solution.py:46
  83.1 3.5 %collective-permute-done.1 = bf16[256,384]{1,0:T(8,128)(2,1)S(1)} collective-permute-done((bf16[256,384]{1,0:T(8,128)(2,1)S(1)}, bf16[256,384]{1,0:T(8,128)(2,1)S(1)}, u32[]{:S(2)}, u32[]{:S(2)}) %collective-permute-start.1) | collective-permute-done | bytes 196640 | tf_op jit(solution)/shard_map/ppermute | solution.py:46
  86.7 2.4 %collective-permute-done.2 = bf16[256,384]{1,0:T(8,128)(2,1)S(1)} collective-permute-done((bf16[256,384]{1,0:T(8,128)(2,1)S(1)}, bf16[256,384]{1,0:T(8,128)(2,1)S(1)}, u32[]{:S(2)}, u32[]{:S(2)}) %collective-permute-start.2) | collective-permute-done | bytes 196640 | tf_op jit(solution)/shard_map/ppermute | solution.py:46
  89.1 1.0 pad_maximum_fusion.1
  90.1 6.4 %collective-permute-start.3 = (bf16[4,256,384]{2,1,0:T(8,128)(2,1)}, bf16[4,256,384]{2,1,0:T(8,128)(2,1)S(1)}, u32[]{:S(2)}, u32[]{:S(2)}) collective-permute-start(bf16[4,256,384]{2,1,0:T(8,128)(2,1)} %pad_maximum_fusion.1), channel_id=1, source_target_pairs={{0,1},{1,0},{2,3},{3,2},{4,5},{5,4},{6,7},{7,6},{8,9},{9,8},{10,11... | collective-permute-start | bytes 2359304 | tf_op jit(solution)/shard_map/ppermute | solution.py:50
  96.5 1.1 fusion.133
  97.5 1.1 fusion.103
  98.7 1.3 select_bitcast_fusion.3
  100.8 5.3 %all-to-all-done.1 = bf16[8,256,384]{2,1,0:T(8,128)(2,1)S(1)} async-done(((bf16[8,256,384]{2,1,0:T(8,128)(2,1)}), bf16[8,256,384]{2,1,0:T(8,128)(2,1)S(1)}, u32[]{:S(2)}, u32[]{:S(2)}) %all-to-all-start.1) | async-done | bytes 1572896 | tf_op jit(solution)/shard_map/all_to_all | solution.py:42
  107.6 9.8 %all_to_all.31 = bf16[4,384,128]{2,1,0:T(8,128)(2,1)S(1)} all-to-all(bf16[4,384,128]{2,1,0:T(8,128)(2,1)S(1)} %broadcast_in_dim.12), channel_id=1, replica_groups=mesh['z'=8,'y'=8,'x'=4,'core'=2] {'x'}, dimensions={0} | all-to-all | bytes 786432 | tf_op jit(solution)/shard_map/all_to_all | solution.py:59
  117.4 7.7 %collective-permute-start.4 = (bf16[4,384,128]{2,1,0:T(8,128)(2,1)S(1)}, bf16[4,384,128]{2,1,0:T(8,128)(2,1)S(1)}, u32[]{:S(2)}, u32[]{:S(2)}) collective-permute-start(bf16[4,384,128]{2,1,0:T(8,128)(2,1)S(1)} %all_to_all.31), channel_id=1, source_target_pairs={{0,1},{1,0},{2,3},{3,2},{4,5},{5,4},{6,7},{7,6},{8,9},{9,8},{10,11... | collective-permute-start | bytes 1179656 | tf_op jit(solution)/shard_map/ppermute | solution.py:50
  128.5 14.4 %all_to_all.32 = bf16[4,256,384]{2,1,0:T(8,128)(2,1)S(1)} all-to-all(bf16[4,256,384]{2,1,0:T(8,128)(2,1)S(1)} %broadcast_in_dim.13), channel_id=1, replica_groups=mesh['z'=8,'y'=8,'x'=4,'core'=2] {'x'}, dimensions={0} | all-to-all | bytes 1572864 | tf_op jit(solution)/shard_map/all_to_all | solution.py:59
  142.9 3.3 %collective-permute-start.5 = (bf16[4,256,384]{2,1,0:T(8,128)(2,1)S(1)}, bf16[4,256,384]{2,1,0:T(8,128)(2,1)S(1)}, u32[]{:S(2)}, u32[]{:S(2)}) collective-permute-start(bf16[4,256,384]{2,1,0:T(8,128)(2,1)S(1)} %all_to_all.32), channel_id=1, source_target_pairs={{0,1},{1,0},{2,3},{3,2},{4,5},{5,4},{6,7},{7,6},{8,9},{9,8},{10,11... | collective-permute-start | bytes 2359304 | tf_op jit(solution)/shard_map/ppermute | solution.py:50
  146.3 1.6 collective-permute-done.5
  149.8 8.0 %fusion.7 = bf16[2048,384]{1,0:T(8,128)(2,1)S(1)} fusion(bf16[2048,2048]{1,0:T(8,128)(2,1)} %all-gather.5.cloned.1.call-done, bf16[2048,384]{1,0:T(8,128)(2,1)S(1)} %bitcast.260), kind=kOutput, calls=%fused_computation.9 | convolution fusion | flops 3223191552 | bytes 11534336 | tf_op jit(solution)/shard_map/dot_general | solution.py:148
  158.1 2.3 %collective-permute-start.7 = (bf16[4,256,384]{2,1,0:T(8,128)(2,1)S(1)}, bf16[4,256,384]{2,1,0:T(8,128)(2,1)S(1)}, u32[]{:S(2)}, u32[]{:S(2)}) collective-permute-start(bf16[4,256,384]{2,1,0:T(8,128)(2,1)S(1)} %dynamic-slice_bitcast_fusion), channel_id=1, source_target_pairs={{0,1},{1,0},{2,3},{3,2},{4,5},{5,4},{6,7},{7,6},{8,9},{9,8},{10,11... | collective-permute-start | bytes 2359304 | tf_op jit(solution)/shard_map/ppermute | solution.py:50
  160.4 1.9 collective-permute-done.7
  162.3 1.1 fusion.10
  163.4 3.5 %all-to-all-start.4 = ((bf16[4,256,384]{2,1,0:T(8,128)(2,1)}), bf16[4,256,384]{2,1,0:T(8,128)(2,1)S(1)}, u32[]{:S(2)}, u32[]{:S(2)}) async-start(bf16[4,256,384]{2,1,0:T(8,128)(2,1)} %fusion.10), calls=%async_computation.4 | async-start | bytes 1572864 | tf_op jit(solution)/shard_map/all_to_all | solution.py:154
  166.9 11.9 %all-to-all-done.4 = bf16[4,256,384]{2,1,0:T(8,128)(2,1)S(1)} async-done(((bf16[4,256,384]{2,1,0:T(8,128)(2,1)}), bf16[4,256,384]{2,1,0:T(8,128)(2,1)S(1)}, u32[]{:S(2)}, u32[]{:S(2)}) %all-to-all-start.4) | async-done | bytes 786464 | tf_op jit(solution)/shard_map/all_to_all | solution.py:154
  179.8 4.5 %all-to-all-start.5 = ((f32[8,2,384]{2,1,0:T(2,128)}), f32[8,2,384]{2,1,0:T(2,128)S(1)}, u32[]{:S(2)}, u32[]{:S(2)}) async-start(f32[8,2,384]{2,1,0:T(2,128)} %broadcast_in_dim.14), calls=%async_computation.5 | async-start | bytes 49152 | tf_op jit(solution)/shard_map/all_to_all | solution.py:160
  185.0 3.9 %all-to-all-done.5 = f32[8,2,384]{2,1,0:T(2,128)S(1)} async-done(((f32[8,2,384]{2,1,0:T(2,128)}), f32[8,2,384]{2,1,0:T(2,128)S(1)}, u32[]{:S(2)}, u32[]{:S(2)}) %all-to-all-start.5) | async-done | bytes 24608 | tf_op jit(solution)/shard_map/all_to_all | solution.py:160
  (70 shorter events, 11.4 us)
Async XLA Ops:
  6.5 46.9 %copy-start.2 = (bf16[16,256]{1,0:T(8,128)(2,1)S(1)}, bf16[16,256]{1,0:T(8,128)(2,1)}, u32[]{:S(2)}) copy-start(bf16[16,256]{1,0:T(8,128)(2,1)} %param.17) | copy-start | bytes 24580
  6.5 46.9 %copy-start.4 = (bf16[32,128]{1,0:T(8,128)(2,1)S(1)}, bf16[32,128]{1,0:T(8,128)(2,1)}, u32[]{:S(2)}) copy-start(bf16[32,128]{1,0:T(8,128)(2,1)} %param.13) | copy-start | bytes 24580
  6.5 46.9 %copy-start.3 = (bf16[32,128]{1,0:T(8,128)(2,1)S(1)}, bf16[32,128]{1,0:T(8,128)(2,1)}, u32[]{:S(2)}) copy-start(bf16[32,128]{1,0:T(8,128)(2,1)} %param.14) | copy-start | bytes 24580
  6.5 46.9 %all-gather.3.cloned.1.call-start = ((), (), s32[]{:S(2)}) async-start(), calls=%async_computation.6 | async-start | bytes 1310720 | tf_op jit(solution)/shard_map/all_gather | solution.py:105
  7.5 7.2 %collective-permute-start.6 = (bf16[32,2048]{1,0:T(8,128)(2,1)S(1)}, bf16[32,2048]{1,0:T(8,128)(2,1)S(1)}, u32[]{:S(2)}, u32[]{:S(2)}) collective-permute-start(bf16[32,2048]{1,0:T(8,128)(2,1)S(1)} %pad_maximum_fusion.4), channel_id=1, source_target_pairs={{0,8},{8,0},{16,24},{24,16},{32,40},{40,32},{48,56},{56,48},{64,72... | collective-permute-start | bytes 393224 | tf_op jit(solution)/shard_map/ppermute | solution.py:102
  16.3 133.5 %all-gather.5.cloned.1.call-start = ((), (), s32[]{:S(2)}) async-start(), calls=%async_computation.7 | async-start | bytes 9437184 | tf_op jit(solution)/shard_map/all_gather | solution.py:106
  67.2 6.7 %copy-start = (bf16[384,256]{1,0:T(8,128)(2,1)S(1)}, bf16[384,256]{1,0:T(8,128)(2,1)}, u32[]{:S(2)}) copy-start(bf16[384,256]{1,0:T(8,128)(2,1)} %param.12) | copy-start | bytes 589828
  67.2 38.9 %all-to-all-start.1 = ((bf16[8,256,384]{2,1,0:T(8,128)(2,1)}), bf16[8,256,384]{2,1,0:T(8,128)(2,1)S(1)}, u32[]{:S(2)}, u32[]{:S(2)}) async-start(bf16[8,256,384]{2,1,0:T(8,128)(2,1)} %broadcast_in_dim.11), calls=%async_computation.1 | async-start | bytes 3145728 | tf_op jit(solution)/shard_map/all_to_all | solution.py:42
  74.1 9.0 %collective-permute-start = (bf16[256,384]{1,0:T(8,128)(2,1)S(1)}, bf16[256,384]{1,0:T(8,128)(2,1)S(1)}, u32[]{:S(2)}, u32[]{:S(2)}) collective-permute-start(bf16[256,384]{1,0:T(8,128)(2,1)S(1)} %bitcast.255), channel_id=1, source_target_pairs={{0,6},{2,0},{4,2},{6,4},{1,7},{3,1},{5,3},{7,5},{8,14},{10,8},{12,... | collective-permute-start | bytes 589832 | tf_op jit(solution)/shard_map/ppermute | solution.py:46
  78.4 8.2 %collective-permute-start.1 = (bf16[256,384]{1,0:T(8,128)(2,1)S(1)}, bf16[256,384]{1,0:T(8,128)(2,1)S(1)}, u32[]{:S(2)}, u32[]{:S(2)}) collective-permute-start(bf16[256,384]{1,0:T(8,128)(2,1)S(1)} %bitcast.256), channel_id=1, source_target_pairs={{0,4},{2,6},{4,0},{6,2},{1,5},{3,7},{5,1},{7,3},{8,12},{10,14},{12... | collective-permute-start | bytes 589832 | tf_op jit(solution)/shard_map/ppermute | solution.py:46
  80.6 8.4 %collective-permute-start.2 = (bf16[256,384]{1,0:T(8,128)(2,1)S(1)}, bf16[256,384]{1,0:T(8,128)(2,1)S(1)}, u32[]{:S(2)}, u32[]{:S(2)}) collective-permute-start(bf16[256,384]{1,0:T(8,128)(2,1)S(1)} %bitcast.257), channel_id=1, source_target_pairs={{0,2},{2,4},{4,6},{6,0},{1,3},{3,5},{5,7},{7,1},{8,10},{10,12},{12... | collective-permute-start | bytes 589832 | tf_op jit(solution)/shard_map/ppermute | solution.py:46
  90.1 8.6 %collective-permute-start.3 = (bf16[4,256,384]{2,1,0:T(8,128)(2,1)}, bf16[4,256,384]{2,1,0:T(8,128)(2,1)S(1)}, u32[]{:S(2)}, u32[]{:S(2)}) collective-permute-start(bf16[4,256,384]{2,1,0:T(8,128)(2,1)} %pad_maximum_fusion.1), channel_id=1, source_target_pairs={{0,1},{1,0},{2,3},{3,2},{4,5},{5,4},{6,7},{7,6},{8,9},{9,8},{10,11... | collective-permute-start | bytes 2359304 | tf_op jit(solution)/shard_map/ppermute | solution.py:50
  117.4 9.0 %collective-permute-start.4 = (bf16[4,384,128]{2,1,0:T(8,128)(2,1)S(1)}, bf16[4,384,128]{2,1,0:T(8,128)(2,1)S(1)}, u32[]{:S(2)}, u32[]{:S(2)}) collective-permute-start(bf16[4,384,128]{2,1,0:T(8,128)(2,1)S(1)} %all_to_all.31), channel_id=1, source_target_pairs={{0,1},{1,0},{2,3},{3,2},{4,5},{5,4},{6,7},{7,6},{8,9},{9,8},{10,11... | collective-permute-start | bytes 1179656 | tf_op jit(solution)/shard_map/ppermute | solution.py:50
  125.7 1.2 copy-start.5
  128.4 17.9 %copy-start.1 = (f32[2048]{0:T(1024)S(1)}, f32[2048]{0:T(1024)}, u32[]{:S(2)}) copy-start(f32[2048]{0:T(1024)} %param.18) | copy-start | bytes 24580
  142.9 5.0 %collective-permute-start.5 = (bf16[4,256,384]{2,1,0:T(8,128)(2,1)S(1)}, bf16[4,256,384]{2,1,0:T(8,128)(2,1)S(1)}, u32[]{:S(2)}, u32[]{:S(2)}) collective-permute-start(bf16[4,256,384]{2,1,0:T(8,128)(2,1)S(1)} %all_to_all.32), channel_id=1, source_target_pairs={{0,1},{1,0},{2,3},{3,2},{4,5},{5,4},{6,7},{7,6},{8,9},{9,8},{10,11... | collective-permute-start | bytes 2359304 | tf_op jit(solution)/shard_map/ppermute | solution.py:50
  158.1 4.2 %collective-permute-start.7 = (bf16[4,256,384]{2,1,0:T(8,128)(2,1)S(1)}, bf16[4,256,384]{2,1,0:T(8,128)(2,1)S(1)}, u32[]{:S(2)}, u32[]{:S(2)}) collective-permute-start(bf16[4,256,384]{2,1,0:T(8,128)(2,1)S(1)} %dynamic-slice_bitcast_fusion), channel_id=1, source_target_pairs={{0,1},{1,0},{2,3},{3,2},{4,5},{5,4},{6,7},{7,6},{8,9},{9,8},{10,11... | collective-permute-start | bytes 2359304 | tf_op jit(solution)/shard_map/ppermute | solution.py:50
  163.4 15.5 %all-to-all-start.4 = ((bf16[4,256,384]{2,1,0:T(8,128)(2,1)}), bf16[4,256,384]{2,1,0:T(8,128)(2,1)S(1)}, u32[]{:S(2)}, u32[]{:S(2)}) async-start(bf16[4,256,384]{2,1,0:T(8,128)(2,1)} %fusion.10), calls=%async_computation.4 | async-start | bytes 1572864 | tf_op jit(solution)/shard_map/all_to_all | solution.py:154
  179.8 9.2 %all-to-all-start.5 = ((f32[8,2,384]{2,1,0:T(2,128)}), f32[8,2,384]{2,1,0:T(2,128)S(1)}, u32[]{:S(2)}, u32[]{:S(2)}) async-start(f32[8,2,384]{2,1,0:T(2,128)} %broadcast_in_dim.14), calls=%async_computation.5 | async-start | bytes 49152 | tf_op jit(solution)/shard_map/all_to_all | solution.py:160
Sparse Core Ops, SparseCore 0:
  16.4 36.9 all-gather.2
  55.5 73.2 all-gather.4

commit v3 on v2

--- a/solution.py
+++ b/solution.py
@@ -2,6 +2,8 @@
 import jax.numpy as jnp
 import numpy as np
 from jax import lax
+from jax.experimental import pallas as pl
+from jax.experimental.pallas import tpu as pltpu
 from jax.sharding import Mesh
 from jax.sharding import PartitionSpec as P
 
@@ -33,8 +35,37 @@
 
 
 FIRST, SECOND = rings("yz"), rings("zy")
-FOURS = [group[parity::2] for group in FIRST for parity in range(2)]
-PAIRS = [(a, group[i ^ 1]) for group in FIRST for i, a in enumerate(group)]
+
+
+def pairs(groups, by):
+    return [(group[i], group[(i + by) % SIDE]) for group in groups for i in range(SIDE)]
+
+
+def place_blocks(place_ref, *refs):
+    blocks, out, sems = refs[:SIDE], refs[SIDE], refs[SIDE + 1]
+    rows = blocks[0].shape[0]
+    copies = []
+    for i, block in enumerate(blocks):
+        start = pl.multiple_of(lax.rem(place_ref[0] + i, SIDE) * rows, rows)
+        copies.append(pltpu.make_async_copy(block, out.at[pl.ds(start, rows)], sems.at[i]))
+        copies[-1].start()
+    for copy in copies:
+        copy.wait()
+
+
+def in_place(blocks, place):
+    rows, columns = blocks[0].shape
+    size = SIDE * rows * columns
+    return pl.pallas_call(
+        place_blocks,
+        out_shape=jax.ShapeDtypeStruct((SIDE * rows, columns), blocks[0].dtype),
+        in_specs=[pl.BlockSpec(memory_space=pltpu.SMEM)] + [pl.BlockSpec(memory_space=pl.ANY)] * SIDE,
+        out_specs=pl.BlockSpec(memory_space=pl.ANY),
+        scratch_shapes=[pltpu.SemaphoreType.DMA((SIDE,))],
+        cost_estimate=pl.CostEstimate(flops=size, bytes_accessed=4 * size, transcendentals=0),
+        compiler_params=pltpu.CompilerParams(vmem_limit_bytes=1 << 20),
+        name="place_blocks",
+    )(place.astype(jnp.int32).reshape(1), *blocks)
 
 
 def sent_to_group(shard, groups):
@@ -99,10 +130,8 @@
 
     wide = jnp.concatenate([w_up, w_down.T], 1)
     place = jnp.where(core == 0, lax.axis_index("y"), lax.axis_index("z"))
-    met = lax.ppermute(wide, ALL, PAIRS)
-    even = place % 2 == 0
-    wide = jnp.concatenate([jnp.where(even, wide, met), jnp.where(even, met, wide)], 0)
-    wide = lax.all_gather(wide, ALL, axis=0, tiled=True, axis_index_groups=FOURS)
+    blocks = [wide] + [lax.ppermute(wide, ALL, pairs(FIRST, -by)) for by in range(1, SIDE)]
+    wide = in_place(blocks, place)
     wide = lax.all_gather(wide, ALL, axis=0, tiled=True, axis_index_groups=SECOND)
 
     mix_rows = w_mix_out.shape[0]

time: 198 us -> 194 us (0.980)
  waiting for transfers between devices: 70.7 us -> 35.8 us
  starting transfers between devices: 48.2 us -> 79.7 us
    all_gather x1 -> x0, waiting for transfers between devices: 37.1 us -> none  [layer(): lax.all_gather(wide, ALL, axis=0, tiled=True, axis_index_groups=FOURS)]
    ppermute x1 -> x7, starting transfers between devices: 4.82 us -> 32.4 us  [layer(): lax.ppermute(wide, ALL, pairs(FIRST, -by))]
    ppermute x1 -> x7, waiting for transfers between devices: 2.32 us -> 6.73 us  [layer(): lax.ppermute(wide, ALL, pairs(FIRST, -by))]
    ppermute x4, starting transfers between devices: 19.7 us -> 23.1 us  [partner_of(): return lax.ppermute(a, 'core', [(0, 1), (1, 0)])]
  transfers between devices with their start and end apart: 13 -> 18, of which waited for: 10 -> 9; matrix products, arithmetic and copies ran while one was open for 7% -> 7% of each run, Pallas kernels for 0% -> 0%
where the time goes in v3:
time: 194 us; the launch traced here: 193 us
  starting transfers between devices  79.7 us (41%)
  blocking collectives  36.3 us (19%)
  waiting for transfers between devices  35.8 us (18%)
  between operations  14 us (7%)
  other arithmetic  11.3 us (6%)
  matrix products  9.11 us (5%)
  local copies, waits for them, and re-layouts  5.29 us (3%)
    ppermute x7, starting transfers between devices, layer(): lax.ppermute(wide, ALL, pairs(FIRST, -by))  32.4 us
    all_to_all x2, blocking collectives, all_ranks(): mine = lax.all_to_all(copies, 'x', 0, 0, tiled=True)  24.5 us
    ppermute x4, starting transfers between devices, partner_of(): return lax.ppermute(a, 'core', [(0, 1), (1, 0)])  23.1 us
    all_to_all x1, waiting for transfers between devices, layer(): arrived = lax.all_to_all(pair, 'x', 0, 0, tiled=True)  11.9 us
    all_to_all x1, blocking collectives, sent_to_group(): lax.all_to_all(copies, ALL, 0, 0, axis_index_groups=groups, tiled=True)  11.8 us
    ppermute x3, starting transfers between devices, along_x(): return lax.ppermute(a, 'x', [(i, (i + by) % 4) for i in range(4)])  9.33 us
    dot_general x1, matrix products, layer(): terms = jnp.dot(wide[:, units_part:], hidden, preferred_element_type=f32)  8.01 us
    all_to_all x1, starting transfers between devices, sent_to_group(): lax.all_to_all(copies, ALL, 0, 0, axis_index_groups=groups, tiled=True)  6.95 us
  transfers between devices with their start and end apart: 18, of which 9 were waited for; matrix products, arithmetic and copies ran while one was open for 7% of the time, Pallas kernels for 0%

profile of v3, /device:TPU:1, one launch (start us, length us, event | category | flops | bytes accessed | tf_op | source)
XLA Modules:
  0.0 192.6 jit_solution(16409914769437600010)
XLA Ops:
  7.4 8.4 %collective-permute-start.10 = (bf16[32,2048]{1,0:T(8,128)(2,1)S(1)}, bf16[32,2048]{1,0:T(8,128)(2,1)S(1)}, u32[]{:S(2)}, u32[]{:S(2)}) collective-permute-start(bf16[32,2048]{1,0:T(8,128)(2,1)S(1)} %pad_maximum_fusion.3.refs_0_), channel_id=1, source_target_pairs={{0,24},{8,32},{16,40},{24,48},{32,56},{40,0},{48,8},{56,16},{64,88... | collective-permute-start | bytes 393224 | tf_op jit(solution)/shard_map/ppermute | solution.py:133
  15.9 6.1 %collective-permute-start.11 = (bf16[32,2048]{1,0:T(8,128)(2,1)S(1)}, bf16[32,2048]{1,0:T(8,128)(2,1)S(1)}, u32[]{:S(2)}, u32[]{:S(2)}) collective-permute-start(bf16[32,2048]{1,0:T(8,128)(2,1)S(1)} %pad_maximum_fusion.3.refs_0_), channel_id=1, source_target_pairs={{0,16},{8,24},{16,32},{24,40},{32,48},{40,56},{48,0},{56,8},{64,80... | collective-permute-start | bytes 393224 | tf_op jit(solution)/shard_map/ppermute | solution.py:133
  22.0 3.1 %collective-permute-start.12 = (bf16[32,2048]{1,0:T(8,128)(2,1)S(1)}, bf16[32,2048]{1,0:T(8,128)(2,1)S(1)}, u32[]{:S(2)}, u32[]{:S(2)}) collective-permute-start(bf16[32,2048]{1,0:T(8,128)(2,1)S(1)} %pad_maximum_fusion.3.refs_0_), channel_id=1, source_target_pairs={{0,8},{8,16},{16,24},{24,32},{32,40},{40,48},{48,56},{56,0},{64,72... | collective-permute-start | bytes 393224 | tf_op jit(solution)/shard_map/ppermute | solution.py:133
  25.1 3.4 %collective-permute-start.6 = (bf16[32,2048]{1,0:T(8,128)(2,1)S(1)}, bf16[32,2048]{1,0:T(8,128)(2,1)S(1)}, u32[]{:S(2)}, u32[]{:S(2)}) collective-permute-start(bf16[32,2048]{1,0:T(8,128)(2,1)S(1)} %pad_maximum_fusion.3.refs_0_), channel_id=1, source_target_pairs={{0,56},{8,0},{16,8},{24,16},{32,24},{40,32},{48,40},{56,48},{64,12... | collective-permute-start | bytes 393224 | tf_op jit(solution)/shard_map/ppermute | solution.py:133
  28.5 1.9 collective-permute-start.7
  30.4 4.9 %collective-permute-start.8 = (bf16[32,2048]{1,0:T(8,128)(2,1)S(1)}, bf16[32,2048]{1,0:T(8,128)(2,1)S(1)}, u32[]{:S(2)}, u32[]{:S(2)}) collective-permute-start(bf16[32,2048]{1,0:T(8,128)(2,1)S(1)} %pad_maximum_fusion.3.refs_0_), channel_id=1, source_target_pairs={{0,40},{8,48},{16,56},{24,0},{32,8},{40,16},{48,24},{56,32},{64,10... | collective-permute-start | bytes 393224 | tf_op jit(solution)/shard_map/ppermute | solution.py:133
  35.4 4.5 %collective-permute-start.9 = (bf16[32,2048]{1,0:T(8,128)(2,1)S(1)}, bf16[32,2048]{1,0:T(8,128)(2,1)S(1)}, u32[]{:S(2)}, u32[]{:S(2)}) collective-permute-start(bf16[32,2048]{1,0:T(8,128)(2,1)S(1)} %pad_maximum_fusion.3.refs_0_), channel_id=1, source_target_pairs={{0,32},{8,40},{16,48},{24,56},{32,0},{40,8},{48,16},{56,24},{64,96... | collective-permute-start | bytes 393224 | tf_op jit(solution)/shard_map/ppermute | solution.py:133
  40.0 6.7 %collective-permute-done.9.refs_4_ = bf16[32,2048]{1,0:T(8,128)(2,1)S(1)} collective-permute-done((bf16[32,2048]{1,0:T(8,128)(2,1)S(1)}, bf16[32,2048]{1,0:T(8,128)(2,1)S(1)}, u32[]{:S(2)}, u32[]{:S(2)}) %collective-permute-start.9) | collective-permute-done | bytes 131104 | tf_op jit(solution)/shard_map/ppermute | solution.py:133
  47.9 11.8 %all_to_all.30 = bf16[8,32,384]{2,1,0:T(8,128)(2,1)S(1)} all-to-all(bf16[8,32,384]{2,1,0:T(8,128)(2,1)S(1)} %broadcast_in_dim.10), channel_id=1, replica_groups={{0,8,16,24,32,40,48,56},{64,72,80,88,96,104,112,120},{128,136,144,152,1..., dimensions={0} | all-to-all | bytes 393216 | tf_op jit(solution)/shard_map/all_to_all | solution.py:73
  59.6 1.3 broadcast_in_dim.11
  61.0 7.0 %all-to-all-start.1 = ((bf16[8,256,384]{2,1,0:T(8,128)(2,1)}), bf16[8,256,384]{2,1,0:T(8,128)(2,1)S(1)}, u32[]{:S(2)}, u32[]{:S(2)}) async-start(bf16[8,256,384]{2,1,0:T(8,128)(2,1)} %broadcast_in_dim.11), calls=%async_computation.1 | async-start | bytes 3145728 | tf_op jit(solution)/shard_map/all_to_all | solution.py:73
  68.1 4.4 %collective-permute-start = (bf16[256,384]{1,0:T(8,128)(2,1)S(1)}, bf16[256,384]{1,0:T(8,128)(2,1)S(1)}, u32[]{:S(2)}, u32[]{:S(2)}) collective-permute-start(bf16[256,384]{1,0:T(8,128)(2,1)S(1)} %bitcast.256), channel_id=1, source_target_pairs={{0,6},{2,0},{4,2},{6,4},{1,7},{3,1},{5,3},{7,5},{8,14},{10,8},{12,... | collective-permute-start | bytes 589832 | tf_op jit(solution)/shard_map/ppermute | solution.py:77
  72.5 2.4 %collective-permute-start.1 = (bf16[256,384]{1,0:T(8,128)(2,1)S(1)}, bf16[256,384]{1,0:T(8,128)(2,1)S(1)}, u32[]{:S(2)}, u32[]{:S(2)}) collective-permute-start(bf16[256,384]{1,0:T(8,128)(2,1)S(1)} %bitcast.257), channel_id=1, source_target_pairs={{0,4},{2,6},{4,0},{6,2},{1,5},{3,7},{5,1},{7,3},{8,12},{10,14},{12... | collective-permute-start | bytes 589832 | tf_op jit(solution)/shard_map/ppermute | solution.py:77
  74.9 2.5 %collective-permute-start.2 = (bf16[256,384]{1,0:T(8,128)(2,1)S(1)}, bf16[256,384]{1,0:T(8,128)(2,1)S(1)}, u32[]{:S(2)}, u32[]{:S(2)}) collective-permute-start(bf16[256,384]{1,0:T(8,128)(2,1)S(1)} %bitcast.258), channel_id=1, source_target_pairs={{0,2},{2,4},{4,6},{6,0},{1,3},{3,5},{5,7},{7,1},{8,10},{10,12},{12... | collective-permute-start | bytes 589832 | tf_op jit(solution)/shard_map/ppermute | solution.py:77
  77.5 3.2 %collective-permute-done.1 = bf16[256,384]{1,0:T(8,128)(2,1)S(1)} collective-permute-done((bf16[256,384]{1,0:T(8,128)(2,1)S(1)}, bf16[256,384]{1,0:T(8,128)(2,1)S(1)}, u32[]{:S(2)}, u32[]{:S(2)}) %collective-permute-start.1) | collective-permute-done | bytes 196640 | tf_op jit(solution)/shard_map/ppermute | solution.py:77
  80.7 2.2 %collective-permute-done.2 = bf16[256,384]{1,0:T(8,128)(2,1)S(1)} collective-permute-done((bf16[256,384]{1,0:T(8,128)(2,1)S(1)}, bf16[256,384]{1,0:T(8,128)(2,1)S(1)}, u32[]{:S(2)}, u32[]{:S(2)}) %collective-permute-start.2) | collective-permute-done | bytes 196640 | tf_op jit(solution)/shard_map/ppermute | solution.py:77
  84.0 8.3 %collective-permute-start.3 = (bf16[4,256,384]{2,1,0:T(8,128)(2,1)}, bf16[4,256,384]{2,1,0:T(8,128)(2,1)S(1)}, u32[]{:S(2)}, u32[]{:S(2)}) collective-permute-start(bf16[4,256,384]{2,1,0:T(8,128)(2,1)} %pad_maximum_fusion.1), channel_id=1, source_target_pairs={{0,1},{1,0},{2,3},{3,2},{4,5},{5,4},{6,7},{7,6},{8,9},{9,8},{10,11... | collective-permute-start | bytes 2359304 | tf_op jit(solution)/shard_map/ppermute | solution.py:81
  93.3 1.1 fusion.103
  94.5 1.3 select_bitcast_fusion.3
  96.6 3.5 %all-to-all-done.1 = bf16[8,256,384]{2,1,0:T(8,128)(2,1)S(1)} async-done(((bf16[8,256,384]{2,1,0:T(8,128)(2,1)}), bf16[8,256,384]{2,1,0:T(8,128)(2,1)S(1)}, u32[]{:S(2)}, u32[]{:S(2)}) %all-to-all-start.1) | async-done | bytes 1572896 | tf_op jit(solution)/shard_map/all_to_all | solution.py:73
  101.6 10.1 %all_to_all.31 = bf16[4,384,128]{2,1,0:T(8,128)(2,1)S(1)} all-to-all(bf16[4,384,128]{2,1,0:T(8,128)(2,1)S(1)} %broadcast_in_dim.12), channel_id=1, replica_groups=mesh['z'=8,'y'=8,'x'=4,'core'=2] {'x'}, dimensions={0} | all-to-all | bytes 786432 | tf_op jit(solution)/shard_map/all_to_all | solution.py:90
  111.7 9.2 %collective-permute-start.4 = (bf16[4,384,128]{2,1,0:T(8,128)(2,1)S(1)}, bf16[4,384,128]{2,1,0:T(8,128)(2,1)S(1)}, u32[]{:S(2)}, u32[]{:S(2)}) collective-permute-start(bf16[4,384,128]{2,1,0:T(8,128)(2,1)S(1)} %all_to_all.31), channel_id=1, source_target_pairs={{0,1},{1,0},{2,3},{3,2},{4,5},{5,4},{6,7},{7,6},{8,9},{9,8},{10,11... | collective-permute-start | bytes 1179656 | tf_op jit(solution)/shard_map/ppermute | solution.py:81
  124.3 14.4 %all_to_all.32 = bf16[4,256,384]{2,1,0:T(8,128)(2,1)S(1)} all-to-all(bf16[4,256,384]{2,1,0:T(8,128)(2,1)S(1)} %broadcast_in_dim.13), channel_id=1, replica_groups=mesh['z'=8,'y'=8,'x'=4,'core'=2] {'x'}, dimensions={0} | all-to-all | bytes 1572864 | tf_op jit(solution)/shard_map/all_to_all | solution.py:90
  138.8 3.3 %collective-permute-start.5 = (bf16[4,256,384]{2,1,0:T(8,128)(2,1)S(1)}, bf16[4,256,384]{2,1,0:T(8,128)(2,1)S(1)}, u32[]{:S(2)}, u32[]{:S(2)}) collective-permute-start(bf16[4,256,384]{2,1,0:T(8,128)(2,1)S(1)} %all_to_all.32), channel_id=1, source_target_pairs={{0,1},{1,0},{2,3},{3,2},{4,5},{5,4},{6,7},{7,6},{8,9},{9,8},{10,11... | collective-permute-start | bytes 2359304 | tf_op jit(solution)/shard_map/ppermute | solution.py:81
  142.2 1.6 collective-permute-done.5
  145.6 8.0 %fusion.7 = bf16[2048,384]{1,0:T(8,128)(2,1)S(1)} fusion(bf16[2048,2048]{1,0:T(8,128)(2,1)} %all-gather.2.cloned.1.call-done, bf16[2048,384]{1,0:T(8,128)(2,1)S(1)} %bitcast.261), kind=kOutput, calls=%fused_computation.9 | convolution fusion | flops 3223191552 | bytes 11534336 | tf_op jit(solution)/shard_map/dot_general | solution.py:177
  153.9 2.3 %collective-permute-start.13 = (bf16[4,256,384]{2,1,0:T(8,128)(2,1)S(1)}, bf16[4,256,384]{2,1,0:T(8,128)(2,1)S(1)}, u32[]{:S(2)}, u32[]{:S(2)}) collective-permute-start(bf16[4,256,384]{2,1,0:T(8,128)(2,1)S(1)} %dynamic-slice_bitcast_fusion), channel_id=1, source_target_pairs={{0,1},{1,0},{2,3},{3,2},{4,5},{5,4},{6,7},{7,6},{8,9},{9,8},{10,11... | collective-permute-start | bytes 2359304 | tf_op jit(solution)/shard_map/ppermute | solution.py:81
  156.2 1.9 collective-permute-done.13
  159.2 3.5 %all-to-all-start.4 = ((bf16[4,256,384]{2,1,0:T(8,128)(2,1)}), bf16[4,256,384]{2,1,0:T(8,128)(2,1)S(1)}, u32[]{:S(2)}, u32[]{:S(2)}) async-start(bf16[4,256,384]{2,1,0:T(8,128)(2,1)} %fusion.10), calls=%async_computation.4 | async-start | bytes 1572864 | tf_op jit(solution)/shard_map/all_to_all | solution.py:183
  162.8 11.9 %all-to-all-done.4 = bf16[4,256,384]{2,1,0:T(8,128)(2,1)S(1)} async-done(((bf16[4,256,384]{2,1,0:T(8,128)(2,1)}), bf16[4,256,384]{2,1,0:T(8,128)(2,1)S(1)}, u32[]{:S(2)}, u32[]{:S(2)}) %all-to-all-start.4) | async-done | bytes 786464 | tf_op jit(solution)/shard_map/all_to_all | solution.py:183
  175.6 4.5 %all-to-all-start.5 = ((f32[8,2,384]{2,1,0:T(2,128)}), f32[8,2,384]{2,1,0:T(2,128)S(1)}, u32[]{:S(2)}, u32[]{:S(2)}) async-start(f32[8,2,384]{2,1,0:T(2,128)} %broadcast_in_dim.14), calls=%async_computation.5 | async-start | bytes 49152 | tf_op jit(solution)/shard_map/all_to_all | solution.py:189
  180.8 3.9 %all-to-all-done.5 = f32[8,2,384]{2,1,0:T(2,128)S(1)} async-done(((f32[8,2,384]{2,1,0:T(2,128)}), f32[8,2,384]{2,1,0:T(2,128)S(1)}, u32[]{:S(2)}, u32[]{:S(2)}) %all-to-all-start.5) | async-done | bytes 24608 | tf_op jit(solution)/shard_map/all_to_all | solution.py:189
  (78 shorter events, 15.7 us)
Async XLA Ops:
  6.5 139.1 %all-gather.2.cloned.1.call-start = ((), (), s32[]{:S(2)}) async-start(), calls=%async_computation.6 | async-start | bytes 9437184 | tf_op jit(solution)/shard_map/all_gather | solution.py:135
  7.4 23.0 %collective-permute-start.10 = (bf16[32,2048]{1,0:T(8,128)(2,1)S(1)}, bf16[32,2048]{1,0:T(8,128)(2,1)S(1)}, u32[]{:S(2)}, u32[]{:S(2)}) collective-permute-start(bf16[32,2048]{1,0:T(8,128)(2,1)S(1)} %pad_maximum_fusion.3.refs_0_), channel_id=1, source_target_pairs={{0,24},{8,32},{16,40},{24,48},{32,56},{40,0},{48,8},{56,16},{64,88... | collective-permute-start | bytes 393224 | tf_op jit(solution)/shard_map/ppermute | solution.py:133
  15.9 19.5 %collective-permute-start.11 = (bf16[32,2048]{1,0:T(8,128)(2,1)S(1)}, bf16[32,2048]{1,0:T(8,128)(2,1)S(1)}, u32[]{:S(2)}, u32[]{:S(2)}) collective-permute-start(bf16[32,2048]{1,0:T(8,128)(2,1)S(1)} %pad_maximum_fusion.3.refs_0_), channel_id=1, source_target_pairs={{0,16},{8,24},{16,32},{24,40},{32,48},{40,56},{48,0},{56,8},{64,80... | collective-permute-start | bytes 393224 | tf_op jit(solution)/shard_map/ppermute | solution.py:133
  22.0 17.9 %collective-permute-start.12 = (bf16[32,2048]{1,0:T(8,128)(2,1)S(1)}, bf16[32,2048]{1,0:T(8,128)(2,1)S(1)}, u32[]{:S(2)}, u32[]{:S(2)}) collective-permute-start(bf16[32,2048]{1,0:T(8,128)(2,1)S(1)} %pad_maximum_fusion.3.refs_0_), channel_id=1, source_target_pairs={{0,8},{8,16},{16,24},{24,32},{32,40},{40,48},{48,56},{56,0},{64,72... | collective-permute-start | bytes 393224 | tf_op jit(solution)/shard_map/ppermute | solution.py:133
  25.1 14.8 %collective-permute-start.6 = (bf16[32,2048]{1,0:T(8,128)(2,1)S(1)}, bf16[32,2048]{1,0:T(8,128)(2,1)S(1)}, u32[]{:S(2)}, u32[]{:S(2)}) collective-permute-start(bf16[32,2048]{1,0:T(8,128)(2,1)S(1)} %pad_maximum_fusion.3.refs_0_), channel_id=1, source_target_pairs={{0,56},{8,0},{16,8},{24,16},{32,24},{40,32},{48,40},{56,48},{64,12... | collective-permute-start | bytes 393224 | tf_op jit(solution)/shard_map/ppermute | solution.py:133
  28.5 11.5 %collective-permute-start.7 = (bf16[32,2048]{1,0:T(8,128)(2,1)S(1)}, bf16[32,2048]{1,0:T(8,128)(2,1)S(1)}, u32[]{:S(2)}, u32[]{:S(2)}) collective-permute-start(bf16[32,2048]{1,0:T(8,128)(2,1)S(1)} %pad_maximum_fusion.3.refs_0_), channel_id=1, source_target_pairs={{0,48},{8,56},{16,0},{24,8},{32,16},{40,24},{48,32},{56,40},{64,11... | collective-permute-start | bytes 393224 | tf_op jit(solution)/shard_map/ppermute | solution.py:133
  30.4 9.5 %collective-permute-start.8 = (bf16[32,2048]{1,0:T(8,128)(2,1)S(1)}, bf16[32,2048]{1,0:T(8,128)(2,1)S(1)}, u32[]{:S(2)}, u32[]{:S(2)}) collective-permute-start(bf16[32,2048]{1,0:T(8,128)(2,1)S(1)} %pad_maximum_fusion.3.refs_0_), channel_id=1, source_target_pairs={{0,40},{8,48},{16,56},{24,0},{32,8},{40,16},{48,24},{56,32},{64,10... | collective-permute-start | bytes 393224 | tf_op jit(solution)/shard_map/ppermute | solution.py:133
  35.4 11.3 %collective-permute-start.9 = (bf16[32,2048]{1,0:T(8,128)(2,1)S(1)}, bf16[32,2048]{1,0:T(8,128)(2,1)S(1)}, u32[]{:S(2)}, u32[]{:S(2)}) collective-permute-start(bf16[32,2048]{1,0:T(8,128)(2,1)S(1)} %pad_maximum_fusion.3.refs_0_), channel_id=1, source_target_pairs={{0,32},{8,40},{16,48},{24,56},{32,0},{40,8},{48,16},{56,24},{64,96... | collective-permute-start | bytes 393224 | tf_op jit(solution)/shard_map/ppermute | solution.py:133
  46.7 1.1 copy-start.2
  46.7 1.1 copy-start.3
  46.7 1.1 copy-start.4
  61.0 7.0 %copy-start = (bf16[384,256]{1,0:T(8,128)(2,1)S(1)}, bf16[384,256]{1,0:T(8,128)(2,1)}, u32[]{:S(2)}) copy-start(bf16[384,256]{1,0:T(8,128)(2,1)} %param.12) | copy-start | bytes 589828
  61.0 39.1 %all-to-all-start.1 = ((bf16[8,256,384]{2,1,0:T(8,128)(2,1)}), bf16[8,256,384]{2,1,0:T(8,128)(2,1)S(1)}, u32[]{:S(2)}, u32[]{:S(2)}) async-start(bf16[8,256,384]{2,1,0:T(8,128)(2,1)} %broadcast_in_dim.11), calls=%async_computation.1 | async-start | bytes 3145728 | tf_op jit(solution)/shard_map/all_to_all | solution.py:73
  68.1 9.4 %collective-permute-start = (bf16[256,384]{1,0:T(8,128)(2,1)S(1)}, bf16[256,384]{1,0:T(8,128)(2,1)S(1)}, u32[]{:S(2)}, u32[]{:S(2)}) collective-permute-start(bf16[256,384]{1,0:T(8,128)(2,1)S(1)} %bitcast.256), channel_id=1, source_target_pairs={{0,6},{2,0},{4,2},{6,4},{1,7},{3,1},{5,3},{7,5},{8,14},{10,8},{12,... | collective-permute-start | bytes 589832 | tf_op jit(solution)/shard_map/ppermute | solution.py:77
  72.5 8.2 %collective-permute-start.1 = (bf16[256,384]{1,0:T(8,128)(2,1)S(1)}, bf16[256,384]{1,0:T(8,128)(2,1)S(1)}, u32[]{:S(2)}, u32[]{:S(2)}) collective-permute-start(bf16[256,384]{1,0:T(8,128)(2,1)S(1)} %bitcast.257), channel_id=1, source_target_pairs={{0,4},{2,6},{4,0},{6,2},{1,5},{3,7},{5,1},{7,3},{8,12},{10,14},{12... | collective-permute-start | bytes 589832 | tf_op jit(solution)/shard_map/ppermute | solution.py:77
  74.9 8.0 %collective-permute-start.2 = (bf16[256,384]{1,0:T(8,128)(2,1)S(1)}, bf16[256,384]{1,0:T(8,128)(2,1)S(1)}, u32[]{:S(2)}, u32[]{:S(2)}) collective-permute-start(bf16[256,384]{1,0:T(8,128)(2,1)S(1)} %bitcast.258), channel_id=1, source_target_pairs={{0,2},{2,4},{4,6},{6,0},{1,3},{3,5},{5,7},{7,1},{8,10},{10,12},{12... | collective-permute-start | bytes 589832 | tf_op jit(solution)/shard_map/ppermute | solution.py:77
  84.0 10.5 %collective-permute-start.3 = (bf16[4,256,384]{2,1,0:T(8,128)(2,1)}, bf16[4,256,384]{2,1,0:T(8,128)(2,1)S(1)}, u32[]{:S(2)}, u32[]{:S(2)}) collective-permute-start(bf16[4,256,384]{2,1,0:T(8,128)(2,1)} %pad_maximum_fusion.1), channel_id=1, source_target_pairs={{0,1},{1,0},{2,3},{3,2},{4,5},{5,4},{6,7},{7,6},{8,9},{9,8},{10,11... | collective-permute-start | bytes 2359304 | tf_op jit(solution)/shard_map/ppermute | solution.py:81
  111.7 10.5 %collective-permute-start.4 = (bf16[4,384,128]{2,1,0:T(8,128)(2,1)S(1)}, bf16[4,384,128]{2,1,0:T(8,128)(2,1)S(1)}, u32[]{:S(2)}, u32[]{:S(2)}) collective-permute-start(bf16[4,384,128]{2,1,0:T(8,128)(2,1)S(1)} %all_to_all.31), channel_id=1, source_target_pairs={{0,1},{1,0},{2,3},{3,2},{4,5},{5,4},{6,7},{7,6},{8,9},{9,8},{10,11... | collective-permute-start | bytes 1179656 | tf_op jit(solution)/shard_map/ppermute | solution.py:81
  121.5 1.2 copy-start.5
  124.2 17.9 %copy-start.1 = (f32[2048]{0:T(1024)S(1)}, f32[2048]{0:T(1024)}, u32[]{:S(2)}) copy-start(f32[2048]{0:T(1024)} %param.18) | copy-start | bytes 24580
  138.8 5.0 %collective-permute-start.5 = (bf16[4,256,384]{2,1,0:T(8,128)(2,1)S(1)}, bf16[4,256,384]{2,1,0:T(8,128)(2,1)S(1)}, u32[]{:S(2)}, u32[]{:S(2)}) collective-permute-start(bf16[4,256,384]{2,1,0:T(8,128)(2,1)S(1)} %all_to_all.32), channel_id=1, source_target_pairs={{0,1},{1,0},{2,3},{3,2},{4,5},{5,4},{6,7},{7,6},{8,9},{9,8},{10,11... | collective-permute-start | bytes 2359304 | tf_op jit(solution)/shard_map/ppermute | solution.py:81
  153.9 4.2 %collective-permute-start.13 = (bf16[4,256,384]{2,1,0:T(8,128)(2,1)S(1)}, bf16[4,256,384]{2,1,0:T(8,128)(2,1)S(1)}, u32[]{:S(2)}, u32[]{:S(2)}) collective-permute-start(bf16[4,256,384]{2,1,0:T(8,128)(2,1)S(1)} %dynamic-slice_bitcast_fusion), channel_id=1, source_target_pairs={{0,1},{1,0},{2,3},{3,2},{4,5},{5,4},{6,7},{7,6},{8,9},{9,8},{10,11... | collective-permute-start | bytes 2359304 | tf_op jit(solution)/shard_map/ppermute | solution.py:81
  159.2 15.5 %all-to-all-start.4 = ((bf16[4,256,384]{2,1,0:T(8,128)(2,1)}), bf16[4,256,384]{2,1,0:T(8,128)(2,1)S(1)}, u32[]{:S(2)}, u32[]{:S(2)}) async-start(bf16[4,256,384]{2,1,0:T(8,128)(2,1)} %fusion.10), calls=%async_computation.4 | async-start | bytes 1572864 | tf_op jit(solution)/shard_map/all_to_all | solution.py:183
  175.6 9.2 %all-to-all-start.5 = ((f32[8,2,384]{2,1,0:T(2,128)}), f32[8,2,384]{2,1,0:T(2,128)S(1)}, u32[]{:S(2)}, u32[]{:S(2)}) async-start(f32[8,2,384]{2,1,0:T(2,128)} %broadcast_in_dim.14), calls=%async_computation.5 | async-start | bytes 49152 | tf_op jit(solution)/shard_map/all_to_all | solution.py:189
Sparse Core Ops, SparseCore 0:
  47.9 74.7 all-gather.1

commit v4 on v2

--- a/solution.py
+++ b/solution.py
@@ -33,8 +33,6 @@
 
 
 FIRST, SECOND = rings("yz"), rings("zy")
-FOURS = [group[parity::2] for group in FIRST for parity in range(2)]
-PAIRS = [(a, group[i ^ 1]) for group in FIRST for i, a in enumerate(group)]
 
 
 def sent_to_group(shard, groups):
@@ -98,12 +96,7 @@
         return lax.dynamic_slice_in_dim(vector, tp_rank * size, size, vector.ndim - 1)
 
     wide = jnp.concatenate([w_up, w_down.T], 1)
-    place = jnp.where(core == 0, lax.axis_index("y"), lax.axis_index("z"))
-    met = lax.ppermute(wide, ALL, PAIRS)
-    even = place % 2 == 0
-    wide = jnp.concatenate([jnp.where(even, wide, met), jnp.where(even, met, wide)], 0)
-    wide = lax.all_gather(wide, ALL, axis=0, tiled=True, axis_index_groups=FOURS)
-    wide = lax.all_gather(wide, ALL, axis=0, tiled=True, axis_index_groups=SECOND)
+    wide = lax.all_gather(wide, FS, axis=0, tiled=True)
 
     mix_rows = w_mix_out.shape[0]
     halves = [w_mix_out[:, :channel_part], w_mix_out[:, channel_part:]]
@@ -138,7 +131,6 @@
     spread = jnp.maximum(jnp.sum(combined_whole * combined_whole, 0) / WIDTH - average * average, 0.0)
     scale = lax.rsqrt(spread + norm_eps)
     middle_whole = ((combined_whole - average) * scale * mix_gain[:, None]).astype(bf16)
-    middle_whole = turned(core, middle_whole.reshape(SIDE, SIDE, -1, frames)).reshape(WIDTH, frames)
     middle = ((combined - average[:, None]) * scale[:, None] * mine_of(mix_gain, width_part)).astype(bf16)
 
     up_proj = lax.dot_general(
@@ -146,8 +138,7 @@
     )
     hidden = jnp.square(jax.nn.relu(up_proj)).astype(bf16)
     terms = jnp.dot(wide[:, units_part:], hidden, preferred_element_type=f32)
-    terms = turned(core, terms.astype(bf16).reshape(SIDE, SIDE, -1, frames))
-    terms = terms.reshape(4, 2, width_part, frames)
+    terms = terms.astype(bf16).reshape(4, 2, width_part, frames)
     kept = lax.dynamic_index_in_dim(terms, core, 1, keepdims=False)
     given = lax.dynamic_index_in_dim(terms, 1 - core, 1, keepdims=False)
     pair = (kept.astype(f32) + partner_of(given).astype(f32)).astype(bf16)

time: 198 us -> 171 us (0.86)
  waiting for transfers between devices: 70.7 us -> 42.2 us
  blocking collectives: 36.5 us -> 43.8 us
  starting transfers between devices: 48.2 us -> 42.8 us
    all_gather x2 -> x1, waiting for transfers between devices: 37.1 us -> 15.8 us  [layer(): wide = lax.all_gather(wide, FS, axis=0, tiled=True)]
    all_to_all x1, blocking collectives: 12.4 us -> 19.3 us  [sent_to_group(): lax.all_to_all(copies, ALL, 0, 0, axis_index_groups=groups, tiled=True)]
    all_to_all x1, waiting for transfers between devices: 5.33 us -> 0.01 us  [sent_to_group(): lax.all_to_all(copies, ALL, 0, 0, axis_index_groups=groups, tiled=True)]
    ppermute x1 -> x0, starting transfers between devices: 4.82 us -> none  [layer(): met = lax.ppermute(wide, ALL, PAIRS)]
    ppermute x1 -> x0, waiting for transfers between devices: 2.32 us -> none  [layer(): met = lax.ppermute(wide, ALL, PAIRS)]
  transfers between devices with their start and end apart: 13 -> 11, of which waited for: 10 -> 8; matrix products, arithmetic and copies ran while one was open for 7% -> 9% of each run, Pallas kernels for 0% -> 0%
where the time goes in v4:
time: 171 us; the launch traced here: 170 us
  blocking collectives  43.8 us (26%)
  starting transfers between devices  42.8 us (25%)
  waiting for transfers between devices  42.2 us (25%)
  between operations  13.7 us (8%)
  other arithmetic  12.4 us (7%)
  matrix products  9.1 us (5%)
  local copies, waits for them, and re-layouts  6.05 us (4%)
    all_to_all x2, blocking collectives, all_ranks(): mine = lax.all_to_all(copies, 'x', 0, 0, tiled=True)  24.5 us
    all_to_all x1, blocking collectives, sent_to_group(): lax.all_to_all(copies, ALL, 0, 0, axis_index_groups=groups, tiled=True)  19.3 us
    ppermute x4, starting transfers between devices, partner_of(): return lax.ppermute(a, 'core', [(0, 1), (1, 0)])  17.8 us
    all_gather x1, waiting for transfers between devices, layer(): wide = lax.all_gather(wide, FS, axis=0, tiled=True)  15.8 us
    all_to_all x1, waiting for transfers between devices, layer(): arrived = lax.all_to_all(pair, 'x', 0, 0, tiled=True)  11.7 us
    ppermute x3, starting transfers between devices, along_x(): return lax.ppermute(a, 'x', [(i, (i + by) % 4) for i in range(4)])  9.33 us
    dot_general x1, matrix products, layer(): terms = jnp.dot(wide[:, units_part:], hidden, preferred_element_type=f32)  8.01 us
    all_to_all x1, starting transfers between devices, sent_to_group(): lax.all_to_all(copies, ALL, 0, 0, axis_index_groups=groups, tiled=True)  6.95 us
  transfers between devices with their start and end apart: 11, of which 8 were waited for; matrix products, arithmetic and copies ran while one was open for 9% of the time, Pallas kernels for 0%

profile of v4, /device:TPU:1, one launch (start us, length us, event | category | flops | bytes accessed | tf_op | source)
XLA Modules:
  0.0 170.0 jit_solution(11785377818731685346)
XLA Ops:
  6.5 1.5 pad_maximum_fusion.3
  8.1 0.7 fusion.137
  8.8 0.7 maximum_maximum_fusion
  9.5 19.3 %all_to_all.30 = bf16[8,32,384]{2,1,0:T(8,128)(2,1)S(1)} all-to-all(bf16[8,32,384]{2,1,0:T(8,128)(2,1)S(1)} %broadcast_in_dim.10), channel_id=1, replica_groups={{0,8,16,24,32,40,48,56},{64,72,80,88,96,104,112,120},{128,136,144,152,1..., dimensions={0} | all-to-all | bytes 393216 | tf_op jit(solution)/shard_map/all_to_all | solution.py:40
  28.8 1.4 broadcast_in_dim.11
  30.2 7.0 %all-to-all-start.1 = ((bf16[8,256,384]{2,1,0:T(8,128)(2,1)}), bf16[8,256,384]{2,1,0:T(8,128)(2,1)S(1)}, u32[]{:S(2)}, u32[]{:S(2)}) async-start(bf16[8,256,384]{2,1,0:T(8,128)(2,1)} %broadcast_in_dim.11), calls=%async_computation.1 | async-start | bytes 3145728 | tf_op jit(solution)/shard_map/all_to_all | solution.py:40
  37.3 4.4 %collective-permute-start = (bf16[256,384]{1,0:T(8,128)(2,1)S(1)}, bf16[256,384]{1,0:T(8,128)(2,1)S(1)}, u32[]{:S(2)}, u32[]{:S(2)}) collective-permute-start(bf16[256,384]{1,0:T(8,128)(2,1)S(1)} %bitcast.253), channel_id=1, source_target_pairs={{0,6},{2,0},{4,2},{6,4},{1,7},{3,1},{5,3},{7,5},{8,14},{10,8},{12,... | collective-permute-start | bytes 589832 | tf_op jit(solution)/shard_map/ppermute | solution.py:44
  41.7 2.4 %collective-permute-start.1 = (bf16[256,384]{1,0:T(8,128)(2,1)S(1)}, bf16[256,384]{1,0:T(8,128)(2,1)S(1)}, u32[]{:S(2)}, u32[]{:S(2)}) collective-permute-start(bf16[256,384]{1,0:T(8,128)(2,1)S(1)} %bitcast.254), channel_id=1, source_target_pairs={{0,4},{2,6},{4,0},{6,2},{1,5},{3,7},{5,1},{7,3},{8,12},{10,14},{12... | collective-permute-start | bytes 589832 | tf_op jit(solution)/shard_map/ppermute | solution.py:44
  44.2 2.5 %collective-permute-start.2 = (bf16[256,384]{1,0:T(8,128)(2,1)S(1)}, bf16[256,384]{1,0:T(8,128)(2,1)S(1)}, u32[]{:S(2)}, u32[]{:S(2)}) collective-permute-start(bf16[256,384]{1,0:T(8,128)(2,1)S(1)} %bitcast.255), channel_id=1, source_target_pairs={{0,2},{2,4},{4,6},{6,0},{1,3},{3,5},{5,7},{7,1},{8,10},{10,12},{12... | collective-permute-start | bytes 589832 | tf_op jit(solution)/shard_map/ppermute | solution.py:44
  46.7 3.2 %collective-permute-done.1 = bf16[256,384]{1,0:T(8,128)(2,1)S(1)} collective-permute-done((bf16[256,384]{1,0:T(8,128)(2,1)S(1)}, bf16[256,384]{1,0:T(8,128)(2,1)S(1)}, u32[]{:S(2)}, u32[]{:S(2)}) %collective-permute-start.1) | collective-permute-done | bytes 196640 | tf_op jit(solution)/shard_map/ppermute | solution.py:44
  49.9 3.2 %collective-permute-done.2 = bf16[256,384]{1,0:T(8,128)(2,1)S(1)} collective-permute-done((bf16[256,384]{1,0:T(8,128)(2,1)S(1)}, bf16[256,384]{1,0:T(8,128)(2,1)S(1)}, u32[]{:S(2)}, u32[]{:S(2)}) %collective-permute-start.2) | collective-permute-done | bytes 196640 | tf_op jit(solution)/shard_map/ppermute | solution.py:44
  53.2 1.0 pad_maximum_fusion.1
  54.2 5.4 %collective-permute-start.3 = (bf16[4,256,384]{2,1,0:T(8,128)(2,1)}, bf16[4,256,384]{2,1,0:T(8,128)(2,1)S(1)}, u32[]{:S(2)}, u32[]{:S(2)}) collective-permute-start(bf16[4,256,384]{2,1,0:T(8,128)(2,1)} %pad_maximum_fusion.1), channel_id=1, source_target_pairs={{0,1},{1,0},{2,3},{3,2},{4,5},{5,4},{6,7},{7,6},{8,9},{9,8},{10,11... | collective-permute-start | bytes 2359304 | tf_op jit(solution)/shard_map/ppermute | solution.py:48
  59.6 1.1 fusion.133
  60.7 1.1 fusion.103
  61.9 1.3 select_bitcast_fusion.3
  65.5 10.1 %all_to_all.31 = bf16[4,384,128]{2,1,0:T(8,128)(2,1)S(1)} all-to-all(bf16[4,384,128]{2,1,0:T(8,128)(2,1)S(1)} %broadcast_in_dim.12), channel_id=1, replica_groups=mesh['z'=8,'y'=8,'x'=4,'core'=2] {'x'}, dimensions={0} | all-to-all | bytes 786432 | tf_op jit(solution)/shard_map/all_to_all | solution.py:57
  75.5 6.2 %collective-permute-start.4 = (bf16[4,384,128]{2,1,0:T(8,128)(2,1)S(1)}, bf16[4,384,128]{2,1,0:T(8,128)(2,1)S(1)}, u32[]{:S(2)}, u32[]{:S(2)}) collective-permute-start(bf16[4,384,128]{2,1,0:T(8,128)(2,1)S(1)} %all_to_all.31), channel_id=1, source_target_pairs={{0,1},{1,0},{2,3},{3,2},{4,5},{5,4},{6,7},{7,6},{8,9},{9,8},{10,11... | collective-permute-start | bytes 1179656 | tf_op jit(solution)/shard_map/ppermute | solution.py:48
  85.2 14.4 %all_to_all.32 = bf16[4,256,384]{2,1,0:T(8,128)(2,1)S(1)} all-to-all(bf16[4,256,384]{2,1,0:T(8,128)(2,1)S(1)} %broadcast_in_dim.13), channel_id=1, replica_groups=mesh['z'=8,'y'=8,'x'=4,'core'=2] {'x'}, dimensions={0} | all-to-all | bytes 1572864 | tf_op jit(solution)/shard_map/all_to_all | solution.py:57
  99.6 3.3 %collective-permute-start.5 = (bf16[4,256,384]{2,1,0:T(8,128)(2,1)S(1)}, bf16[4,256,384]{2,1,0:T(8,128)(2,1)S(1)}, u32[]{:S(2)}, u32[]{:S(2)}) collective-permute-start(bf16[4,256,384]{2,1,0:T(8,128)(2,1)S(1)} %all_to_all.32), channel_id=1, source_target_pairs={{0,1},{1,0},{2,3},{3,2},{4,5},{5,4},{6,7},{7,6},{8,9},{9,8},{10,11... | collective-permute-start | bytes 2359304 | tf_op jit(solution)/shard_map/ppermute | solution.py:48
  102.9 1.7 %collective-permute-done.5 = bf16[4,256,384]{2,1,0:T(8,128)(2,1)S(1)} collective-permute-done((bf16[4,256,384]{2,1,0:T(8,128)(2,1)S(1)}, bf16[4,256,384]{2,1,0:T(8,128)(2,1)S(1)}, u32[]{:S(2)}, u32[]{:S(2)}) %collective-permute-start.5) | collective-permute-done | bytes 786464 | tf_op jit(solution)/shard_map/ppermute | solution.py:48
  106.4 15.8 %all-gather.2.cloned.1.call-done = bf16[2048,2048]{1,0:T(8,128)(2,1)} async-done(((bf16[32,2048]{1,0:T(8,128)(2,1)}), bf16[2048,2048]{1,0:T(8,128)(2,1)}) %all-gather.2.cloned.1.call-update) | async-done | bytes 8388624 | tf_op jit(solution)/shard_map/all_gather | solution.py:99
  122.2 8.0 %fusion.7 = bf16[2048,384]{1,0:T(8,128)(2,1)S(1)} fusion(bf16[2048,2048]{1,0:T(8,128)(2,1)} %all-gather.2.cloned.1.call-done, bf16[2048,384]{1,0:T(8,128)(2,1)S(1)} %fusion.6), kind=kOutput, calls=%fused_computation.9 | convolution fusion | flops 3223191552 | bytes 11534336 | tf_op jit(solution)/shard_map/dot_general | solution.py:140
  130.3 2.8 %collective-permute-start.6 = (bf16[4,256,384]{2,1,0:T(8,128)(2,1)S(1)}, bf16[4,256,384]{2,1,0:T(8,128)(2,1)S(1)}, u32[]{:S(2)}, u32[]{:S(2)}) collective-permute-start(bf16[4,256,384]{2,1,0:T(8,128)(2,1)S(1)} %dynamic-slice_bitcast_fusion), channel_id=1, source_target_pairs={{0,1},{1,0},{2,3},{3,2},{4,5},{5,4},{6,7},{7,6},{8,9},{9,8},{10,11... | collective-permute-start | bytes 2359304 | tf_op jit(solution)/shard_map/ppermute | solution.py:48
  133.1 1.9 %collective-permute-done.6 = bf16[4,256,384]{2,1,0:T(8,128)(2,1)S(1)} collective-permute-done((bf16[4,256,384]{2,1,0:T(8,128)(2,1)S(1)}, bf16[4,256,384]{2,1,0:T(8,128)(2,1)S(1)}, u32[]{:S(2)}, u32[]{:S(2)}) %collective-permute-start.6) | collective-permute-done | bytes 786464 | tf_op jit(solution)/shard_map/ppermute | solution.py:48
  135.0 1.1 fusion.10
  136.1 4.0 %all-to-all-start.4 = ((bf16[4,256,384]{2,1,0:T(8,128)(2,1)}), bf16[4,256,384]{2,1,0:T(8,128)(2,1)S(1)}, u32[]{:S(2)}, u32[]{:S(2)}) async-start(bf16[4,256,384]{2,1,0:T(8,128)(2,1)} %fusion.10), calls=%async_computation.4 | async-start | bytes 1572864 | tf_op jit(solution)/shard_map/all_to_all | solution.py:145
  140.1 11.7 %all-to-all-done.4 = bf16[4,256,384]{2,1,0:T(8,128)(2,1)S(1)} async-done(((bf16[4,256,384]{2,1,0:T(8,128)(2,1)}), bf16[4,256,384]{2,1,0:T(8,128)(2,1)S(1)}, u32[]{:S(2)}, u32[]{:S(2)}) %all-to-all-start.4) | async-done | bytes 786464 | tf_op jit(solution)/shard_map/all_to_all | solution.py:145
  152.7 4.8 %all-to-all-start.5 = ((f32[8,2,384]{2,1,0:T(2,128)}), f32[8,2,384]{2,1,0:T(2,128)S(1)}, u32[]{:S(2)}, u32[]{:S(2)}) async-start(f32[8,2,384]{2,1,0:T(2,128)} %broadcast_in_dim.14), calls=%async_computation.5 | async-start | bytes 49152 | tf_op jit(solution)/shard_map/all_to_all | solution.py:151
  157.5 0.8 dynamic_slice.23
  158.2 3.9 %all-to-all-done.5 = f32[8,2,384]{2,1,0:T(2,128)S(1)} async-done(((f32[8,2,384]{2,1,0:T(2,128)}), f32[8,2,384]{2,1,0:T(2,128)S(1)}, u32[]{:S(2)}, u32[]{:S(2)}) %all-to-all-start.5) | async-done | bytes 24608 | tf_op jit(solution)/shard_map/all_to_all | solution.py:151
  162.3 0.8 copy.55
  (53 shorter events, 8.7 us)
Async XLA Ops:
  6.5 115.6 %all-gather.2.cloned.1.call-start = ((), (), s32[]{:S(2)}) async-start(), calls=%async_computation.6 | async-start | bytes 8519680 | tf_op jit(solution)/shard_map/all_gather | solution.py:99
  30.2 7.0 %copy-start = (bf16[384,256]{1,0:T(8,128)(2,1)S(1)}, bf16[384,256]{1,0:T(8,128)(2,1)}, u32[]{:S(2)}) copy-start(bf16[384,256]{1,0:T(8,128)(2,1)} %param.12) | copy-start | bytes 589828
  30.2 33.7 %all-to-all-start.1 = ((bf16[8,256,384]{2,1,0:T(8,128)(2,1)}), bf16[8,256,384]{2,1,0:T(8,128)(2,1)S(1)}, u32[]{:S(2)}, u32[]{:S(2)}) async-start(bf16[8,256,384]{2,1,0:T(8,128)(2,1)} %broadcast_in_dim.11), calls=%async_computation.1 | async-start | bytes 3145728 | tf_op jit(solution)/shard_map/all_to_all | solution.py:40
  37.3 9.4 %collective-permute-start = (bf16[256,384]{1,0:T(8,128)(2,1)S(1)}, bf16[256,384]{1,0:T(8,128)(2,1)S(1)}, u32[]{:S(2)}, u32[]{:S(2)}) collective-permute-start(bf16[256,384]{1,0:T(8,128)(2,1)S(1)} %bitcast.253), channel_id=1, source_target_pairs={{0,6},{2,0},{4,2},{6,4},{1,7},{3,1},{5,3},{7,5},{8,14},{10,8},{12,... | collective-permute-start | bytes 589832 | tf_op jit(solution)/shard_map/ppermute | solution.py:44
  41.7 8.2 %collective-permute-start.1 = (bf16[256,384]{1,0:T(8,128)(2,1)S(1)}, bf16[256,384]{1,0:T(8,128)(2,1)S(1)}, u32[]{:S(2)}, u32[]{:S(2)}) collective-permute-start(bf16[256,384]{1,0:T(8,128)(2,1)S(1)} %bitcast.254), channel_id=1, source_target_pairs={{0,4},{2,6},{4,0},{6,2},{1,5},{3,7},{5,1},{7,3},{8,12},{10,14},{12... | collective-permute-start | bytes 589832 | tf_op jit(solution)/shard_map/ppermute | solution.py:44
  44.2 9.0 %collective-permute-start.2 = (bf16[256,384]{1,0:T(8,128)(2,1)S(1)}, bf16[256,384]{1,0:T(8,128)(2,1)S(1)}, u32[]{:S(2)}, u32[]{:S(2)}) collective-permute-start(bf16[256,384]{1,0:T(8,128)(2,1)S(1)} %bitcast.255), channel_id=1, source_target_pairs={{0,2},{2,4},{4,6},{6,0},{1,3},{3,5},{5,7},{7,1},{8,10},{10,12},{12... | collective-permute-start | bytes 589832 | tf_op jit(solution)/shard_map/ppermute | solution.py:44
  54.2 7.7 %collective-permute-start.3 = (bf16[4,256,384]{2,1,0:T(8,128)(2,1)}, bf16[4,256,384]{2,1,0:T(8,128)(2,1)S(1)}, u32[]{:S(2)}, u32[]{:S(2)}) collective-permute-start(bf16[4,256,384]{2,1,0:T(8,128)(2,1)} %pad_maximum_fusion.1), channel_id=1, source_target_pairs={{0,1},{1,0},{2,3},{3,2},{4,5},{5,4},{6,7},{7,6},{8,9},{9,8},{10,11... | collective-permute-start | bytes 2359304 | tf_op jit(solution)/shard_map/ppermute | solution.py:48
  75.5 7.5 %collective-permute-start.4 = (bf16[4,384,128]{2,1,0:T(8,128)(2,1)S(1)}, bf16[4,384,128]{2,1,0:T(8,128)(2,1)S(1)}, u32[]{:S(2)}, u32[]{:S(2)}) collective-permute-start(bf16[4,384,128]{2,1,0:T(8,128)(2,1)S(1)} %all_to_all.31), channel_id=1, source_target_pairs={{0,1},{1,0},{2,3},{3,2},{4,5},{5,4},{6,7},{7,6},{8,9},{9,8},{10,11... | collective-permute-start | bytes 1179656 | tf_op jit(solution)/shard_map/ppermute | solution.py:48
  82.4 1.2 copy-start.2
  99.6 5.0 %collective-permute-start.5 = (bf16[4,256,384]{2,1,0:T(8,128)(2,1)S(1)}, bf16[4,256,384]{2,1,0:T(8,128)(2,1)S(1)}, u32[]{:S(2)}, u32[]{:S(2)}) collective-permute-start(bf16[4,256,384]{2,1,0:T(8,128)(2,1)S(1)} %all_to_all.32), channel_id=1, source_target_pairs={{0,1},{1,0},{2,3},{3,2},{4,5},{5,4},{6,7},{7,6},{8,9},{9,8},{10,11... | collective-permute-start | bytes 2359304 | tf_op jit(solution)/shard_map/ppermute | solution.py:48
  105.2 0.7 copy-start.1
  130.3 4.7 %collective-permute-start.6 = (bf16[4,256,384]{2,1,0:T(8,128)(2,1)S(1)}, bf16[4,256,384]{2,1,0:T(8,128)(2,1)S(1)}, u32[]{:S(2)}, u32[]{:S(2)}) collective-permute-start(bf16[4,256,384]{2,1,0:T(8,128)(2,1)S(1)} %dynamic-slice_bitcast_fusion), channel_id=1, source_target_pairs={{0,1},{1,0},{2,3},{3,2},{4,5},{5,4},{6,7},{7,6},{8,9},{9,8},{10,11... | collective-permute-start | bytes 2359304 | tf_op jit(solution)/shard_map/ppermute | solution.py:48
  136.1 15.7 %all-to-all-start.4 = ((bf16[4,256,384]{2,1,0:T(8,128)(2,1)}), bf16[4,256,384]{2,1,0:T(8,128)(2,1)S(1)}, u32[]{:S(2)}, u32[]{:S(2)}) async-start(bf16[4,256,384]{2,1,0:T(8,128)(2,1)} %fusion.10), calls=%async_computation.4 | async-start | bytes 1572864 | tf_op jit(solution)/shard_map/all_to_all | solution.py:145
  152.7 9.5 %all-to-all-start.5 = ((f32[8,2,384]{2,1,0:T(2,128)}), f32[8,2,384]{2,1,0:T(2,128)S(1)}, u32[]{:S(2)}, u32[]{:S(2)}) async-start(f32[8,2,384]{2,1,0:T(2,128)} %broadcast_in_dim.14), calls=%async_computation.5 | async-start | bytes 49152 | tf_op jit(solution)/shard_map/all_to_all | solution.py:151
Sparse Core Ops, SparseCore 0:
  10.4 111.7 all-gather.1

commit v5 on v1

--- a/solution.py
+++ b/solution.py
@@ -38,18 +38,6 @@
 def sent_to_group(shard, groups):
     copies = jnp.broadcast_to(shard, (SIDE, *shard.shape))
     return lax.all_to_all(copies, ALL, 0, 0, axis_index_groups=groups, tiled=True)
-
-
-def second_axis_pairs(by):
-    return [
-        (group[i], group[(i + by) % SIDE]) for group in SECOND for i in range(SIDE)
-    ]
-
-
-def doubled(piece):
-    for by in (1, 2, 4):
-        piece = jnp.concatenate([piece, lax.ppermute(piece, ALL, second_axis_pairs(-by))], 0)
-    return piece
 
 
 def along_x(a, by):
@@ -107,6 +95,8 @@
     def mine_of(vector, size):
         return lax.dynamic_slice_in_dim(vector, tp_rank * size, size, vector.ndim - 1)
 
+    own_mix_gain = mine_of(mix_gain, width_part)
+    own_out_gain = mine_of(out_gain, width_part)
     own_xt = tokens.T
     mix_rows = w_mix_out.shape[0]
     halves = [w_mix_out[:, :channel_part], w_mix_out[:, channel_part:]]
@@ -114,11 +104,9 @@
     shard = sent_to_group(shard, FIRST).reshape(-1, shard.shape[1])
     at = 2 * units_part
     wide = lax.all_gather(shard[:, :at], ALL, axis=0, tiled=True, axis_index_groups=SECOND)
-    value_gate = sent_to_group(shard[:, at : at + 2 * channel_part], SECOND)
-    value_gate = value_gate.reshape(WIDTH, 2 * channel_part)
-    mix = doubled(shard[None, :, at + 2 * channel_part :])
-    mix = jnp.roll(mix, jnp.where(core == 0, lax.axis_index("z"), lax.axis_index("y")), 0)
-    mix = mix.reshape(SIDE, SIDE, 2, mix_rows, channel_part)
+    small = sent_to_group(shard[:, at:], SECOND)
+    value_gate = small[:, :, : 2 * channel_part].reshape(WIDTH, 2 * channel_part)
+    mix = small[:, :, 2 * channel_part :].reshape(SIDE, SIDE, 2, mix_rows, channel_part)
     mix = turned(core, mix.transpose(0, 1, 3, 2, 4)).reshape(CHANNELS, width_part)
 
     x_rank = lax.axis_index("x")
@@ -145,7 +133,7 @@
     scale = lax.rsqrt(spread + norm_eps)
     middle_whole = ((combined_whole - average) * scale * mix_gain[:, None]).astype(bf16)
     middle_whole = turned(core, middle_whole.reshape(SIDE, SIDE, -1, frames)).reshape(WIDTH, frames)
-    middle = ((combined - average[:, None]) * scale[:, None] * mine_of(mix_gain, width_part)).astype(bf16)
+    middle = ((combined - average[:, None]) * scale[:, None] * own_mix_gain).astype(bf16)
 
     up_proj = lax.dot_general(
         wide[:, :units_part], middle_whole, (((0,), (0,)), ((), ())), preferred_element_type=f32
@@ -167,7 +155,7 @@
     average = totals[0] / WIDTH
     spread = jnp.maximum(totals[1] / WIDTH - average * average, 0.0)
     scale = lax.rsqrt(spread + norm_eps)
-    result = (final - average[:, None]) * scale[:, None] * mine_of(out_gain, width_part)
+    result = (final - average[:, None]) * scale[:, None] * own_out_gain
     return result.astype(bf16)
 
 

time: 211 us -> 173 us (0.82)
  waiting for transfers between devices: 56.7 us -> 31.9 us
  starting transfers between devices: 54.2 us -> 41.5 us
  blocking collectives: 45 us -> 55 us
  local copies, waits for them, and re-layouts: 17.2 us -> 10.3 us
    ppermute x3 -> x0, waiting for transfers between devices: 23.8 us -> none  [doubled(): lax.ppermute(piece, ALL, second_axis_pairs(-by))]
    ppermute x3 -> x0, starting transfers between devices: 14.4 us -> none  [doubled(): lax.ppermute(piece, ALL, second_axis_pairs(-by))]
    all_to_all x1 -> x2, blocking collectives: 14.5 us -> 24.5 us  [all_ranks(): mine = lax.all_to_all(copies, 'x', 0, 0, tiled=True)]
    all_to_all x1, waiting for transfers between devices: 0.01 us -> 5.21 us  [sent_to_group(): lax.all_to_all(copies, ALL, 0, 0, axis_index_groups=groups, tiled=True)]
    unnamed x40 -> x11, local copies, waits for them, and re-layouts: 8.05 us -> 3.27 us
    all_to_all x1 -> x0, waiting for transfers between devices: 4.28 us -> none  [all_ranks(): mine = lax.all_to_all(copies, 'x', 0, 0, tiled=True)]
    all_to_all x1 -> x0, starting transfers between devices: 3.46 us -> none  [all_ranks(): mine = lax.all_to_all(copies, 'x', 0, 0, tiled=True)]
    ppermute x3, waiting for transfers between devices: 9.31 us -> 6.59 us  [along_x(): return lax.ppermute(a, 'x', [(i, (i + by) % 4) for i in range(4)])]
  transfers between devices with their start and end apart: 15 -> 11, of which waited for: 11 -> 8; matrix products, arithmetic and copies ran while one was open for 11% -> 8% of each run, Pallas kernels for 0% -> 0%
where the time goes in v5:
time: 173 us; the launch traced here: 172 us
  blocking collectives  55 us (32%)
  starting transfers between devices  41.5 us (24%)
  waiting for transfers between devices  31.9 us (18%)
  between operations  13.8 us (8%)
  other arithmetic  10.5 us (6%)
  local copies, waits for them, and re-layouts  10.3 us (6%)
  matrix products  9.11 us (5%)
    all_to_all x1, blocking collectives, sent_to_group(): lax.all_to_all(copies, ALL, 0, 0, axis_index_groups=groups, tiled=True)  30.5 us
    all_to_all x2, blocking collectives, all_ranks(): mine = lax.all_to_all(copies, 'x', 0, 0, tiled=True)  24.5 us
    ppermute x4, starting transfers between devices, partner_of(): return lax.ppermute(a, 'core', [(0, 1), (1, 0)])  17.2 us
    all_to_all x1, waiting for transfers between devices, layer(): arrived = lax.all_to_all(pair, 'x', 0, 0, tiled=True)  11.9 us
    ppermute x3, starting transfers between devices, along_x(): return lax.ppermute(a, 'x', [(i, (i + by) % 4) for i in range(4)])  9.33 us
    dot_general x1, matrix products, layer(): terms = jnp.dot(wide[:, units_part:], hidden, preferred_element_type=f32)  8.01 us
    all_to_all x1, starting transfers between devices, sent_to_group(): lax.all_to_all(copies, ALL, 0, 0, axis_index_groups=groups, tiled=True)  6.95 us
    ppermute x3, waiting for transfers between devices, along_x(): return lax.ppermute(a, 'x', [(i, (i + by) % 4) for i in range(4)])  6.59 us
  transfers between devices with their start and end apart: 11, of which 8 were waited for; matrix products, arithmetic and copies ran while one was open for 8% of the time, Pallas kernels for 0%

profile of v5, /device:TPU:1, one launch (start us, length us, event | category | flops | bytes accessed | tf_op | source)
XLA Modules:
  0.0 172.1 jit_solution(14191455275945771130)
XLA Ops:
  7.2 0.8 constant_dynamic-update-slice_fusion.3
  8.1 0.8 bitcast_dynamic-update-slice_fusion
  10.4 30.5 %all_to_all.30 = bf16[8,32,2432]{2,1,0:T(8,128)(2,1)S(1)} all-to-all(bf16[8,32,2432]{2,1,0:T(8,128)(2,1)S(1)} %broadcast_in_dim.10), channel_id=1, replica_groups={{0,8,16,24,32,40,48,56},{64,72,80,88,96,104,112,120},{128,136,144,152,1..., dimensions={0} | all-to-all | bytes 2490368 | tf_op jit(solution)/shard_map/all_to_all | solution.py:40
  41.0 1.1 slice.298
  42.1 1.4 broadcast_in_dim.11
  43.5 7.0 %all-to-all-start.1 = ((bf16[8,256,384]{2,1,0:T(8,128)(2,1)}), bf16[8,256,384]{2,1,0:T(8,128)(2,1)S(1)}, u32[]{:S(2)}, u32[]{:S(2)}) async-start(bf16[8,256,384]{2,1,0:T(8,128)(2,1)} %broadcast_in_dim.11), calls=%async_computation.1 | async-start | bytes 3145728 | tf_op jit(solution)/shard_map/all_to_all | solution.py:40
  50.6 4.4 %collective-permute-start = (bf16[256,384]{1,0:T(8,128)(2,1)S(1)}, bf16[256,384]{1,0:T(8,128)(2,1)S(1)}, u32[]{:S(2)}, u32[]{:S(2)}) collective-permute-start(bf16[256,384]{1,0:T(8,128)(2,1)S(1)} %bitcast.258), channel_id=1, source_target_pairs={{0,6},{2,0},{4,2},{6,4},{1,7},{3,1},{5,3},{7,5},{8,14},{10,8},{12,... | collective-permute-start | bytes 589832 | tf_op jit(solution)/shard_map/ppermute | solution.py:44
  55.0 2.4 %collective-permute-start.1 = (bf16[256,384]{1,0:T(8,128)(2,1)S(1)}, bf16[256,384]{1,0:T(8,128)(2,1)S(1)}, u32[]{:S(2)}, u32[]{:S(2)}) collective-permute-start(bf16[256,384]{1,0:T(8,128)(2,1)S(1)} %bitcast.259), channel_id=1, source_target_pairs={{0,4},{2,6},{4,0},{6,2},{1,5},{3,7},{5,1},{7,3},{8,12},{10,14},{12... | collective-permute-start | bytes 589832 | tf_op jit(solution)/shard_map/ppermute | solution.py:44
  57.5 2.5 %collective-permute-start.2 = (bf16[256,384]{1,0:T(8,128)(2,1)S(1)}, bf16[256,384]{1,0:T(8,128)(2,1)S(1)}, u32[]{:S(2)}, u32[]{:S(2)}) collective-permute-start(bf16[256,384]{1,0:T(8,128)(2,1)S(1)} %bitcast.260), channel_id=1, source_target_pairs={{0,2},{2,4},{4,6},{6,0},{1,3},{3,5},{5,7},{7,1},{8,10},{10,12},{12... | collective-permute-start | bytes 589832 | tf_op jit(solution)/shard_map/ppermute | solution.py:44
  60.0 3.2 %collective-permute-done.1 = bf16[256,384]{1,0:T(8,128)(2,1)S(1)} collective-permute-done((bf16[256,384]{1,0:T(8,128)(2,1)S(1)}, bf16[256,384]{1,0:T(8,128)(2,1)S(1)}, u32[]{:S(2)}, u32[]{:S(2)}) %collective-permute-start.1) | collective-permute-done | bytes 196640 | tf_op jit(solution)/shard_map/ppermute | solution.py:44
  63.2 3.3 %collective-permute-done.2 = bf16[256,384]{1,0:T(8,128)(2,1)S(1)} collective-permute-done((bf16[256,384]{1,0:T(8,128)(2,1)S(1)}, bf16[256,384]{1,0:T(8,128)(2,1)S(1)}, u32[]{:S(2)}, u32[]{:S(2)}) %collective-permute-start.2) | collective-permute-done | bytes 196640 | tf_op jit(solution)/shard_map/ppermute | solution.py:44
  66.6 1.0 pad_maximum_fusion.1
  67.6 5.3 %collective-permute-start.3 = (bf16[4,256,384]{2,1,0:T(8,128)(2,1)}, bf16[4,256,384]{2,1,0:T(8,128)(2,1)S(1)}, u32[]{:S(2)}, u32[]{:S(2)}) collective-permute-start(bf16[4,256,384]{2,1,0:T(8,128)(2,1)} %pad_maximum_fusion.1), channel_id=1, source_target_pairs={{0,1},{1,0},{2,3},{3,2},{4,5},{5,4},{6,7},{7,6},{8,9},{9,8},{10,11... | collective-permute-start | bytes 2359304 | tf_op jit(solution)/shard_map/ppermute | solution.py:48
  72.9 1.1 fusion.133
  74.0 1.1 fusion.103
  75.2 1.3 select_bitcast_fusion.3
  77.3 5.2 %all-to-all-done.1 = bf16[8,256,384]{2,1,0:T(8,128)(2,1)S(1)} async-done(((bf16[8,256,384]{2,1,0:T(8,128)(2,1)}), bf16[8,256,384]{2,1,0:T(8,128)(2,1)S(1)}, u32[]{:S(2)}, u32[]{:S(2)}) %all-to-all-start.1) | async-done | bytes 1572896 | tf_op jit(solution)/shard_map/all_to_all | solution.py:40
  84.0 10.1 %all_to_all.31 = bf16[4,384,128]{2,1,0:T(8,128)(2,1)S(1)} all-to-all(bf16[4,384,128]{2,1,0:T(8,128)(2,1)S(1)} %broadcast_in_dim.12), channel_id=1, replica_groups=mesh['z'=8,'y'=8,'x'=4,'core'=2] {'x'}, dimensions={0} | all-to-all | bytes 786432 | tf_op jit(solution)/shard_map/all_to_all | solution.py:57
  94.1 6.3 %collective-permute-start.4 = (bf16[4,384,128]{2,1,0:T(8,128)(2,1)S(1)}, bf16[4,384,128]{2,1,0:T(8,128)(2,1)S(1)}, u32[]{:S(2)}, u32[]{:S(2)}) collective-permute-start(bf16[4,384,128]{2,1,0:T(8,128)(2,1)S(1)} %all_to_all.31), channel_id=1, source_target_pairs={{0,1},{1,0},{2,3},{3,2},{4,5},{5,4},{6,7},{7,6},{8,9},{9,8},{10,11... | collective-permute-start | bytes 1179656 | tf_op jit(solution)/shard_map/ppermute | solution.py:48
  103.8 14.4 %all_to_all.32 = bf16[4,256,384]{2,1,0:T(8,128)(2,1)S(1)} all-to-all(bf16[4,256,384]{2,1,0:T(8,128)(2,1)S(1)} %broadcast_in_dim.13), channel_id=1, replica_groups=mesh['z'=8,'y'=8,'x'=4,'core'=2] {'x'}, dimensions={0} | all-to-all | bytes 1572864 | tf_op jit(solution)/shard_map/all_to_all | solution.py:57
  118.3 3.3 %collective-permute-start.5 = (bf16[4,256,384]{2,1,0:T(8,128)(2,1)S(1)}, bf16[4,256,384]{2,1,0:T(8,128)(2,1)S(1)}, u32[]{:S(2)}, u32[]{:S(2)}) collective-permute-start(bf16[4,256,384]{2,1,0:T(8,128)(2,1)S(1)} %all_to_all.32), channel_id=1, source_target_pairs={{0,1},{1,0},{2,3},{3,2},{4,5},{5,4},{6,7},{7,6},{8,9},{9,8},{10,11... | collective-permute-start | bytes 2359304 | tf_op jit(solution)/shard_map/ppermute | solution.py:48
  121.7 1.6 collective-permute-done.5
  125.1 8.0 %fusion.7 = bf16[2048,384]{1,0:T(8,128)(2,1)S(1)} fusion(bf16[2048,2048]{1,0:T(8,128)(2,1)} %all-gather.2.cloned.1.call-done, bf16[2048,384]{1,0:T(8,128)(2,1)S(1)} %bitcast.263), kind=kOutput, calls=%fused_computation.9 | convolution fusion | flops 3223191552 | bytes 11534336 | tf_op jit(solution)/shard_map/dot_general | solution.py:142
  133.4 2.3 %collective-permute-start.6 = (bf16[4,256,384]{2,1,0:T(8,128)(2,1)S(1)}, bf16[4,256,384]{2,1,0:T(8,128)(2,1)S(1)}, u32[]{:S(2)}, u32[]{:S(2)}) collective-permute-start(bf16[4,256,384]{2,1,0:T(8,128)(2,1)S(1)} %dynamic-slice_bitcast_fusion), channel_id=1, source_target_pairs={{0,1},{1,0},{2,3},{3,2},{4,5},{5,4},{6,7},{7,6},{8,9},{9,8},{10,11... | collective-permute-start | bytes 2359304 | tf_op jit(solution)/shard_map/ppermute | solution.py:48
  135.7 1.9 %collective-permute-done.6 = bf16[4,256,384]{2,1,0:T(8,128)(2,1)S(1)} collective-permute-done((bf16[4,256,384]{2,1,0:T(8,128)(2,1)S(1)}, bf16[4,256,384]{2,1,0:T(8,128)(2,1)S(1)}, u32[]{:S(2)}, u32[]{:S(2)}) %collective-permute-start.6) | collective-permute-done | bytes 786464 | tf_op jit(solution)/shard_map/ppermute | solution.py:48
  137.6 1.1 fusion.10
  138.7 3.5 %all-to-all-start.4 = ((bf16[4,256,384]{2,1,0:T(8,128)(2,1)}), bf16[4,256,384]{2,1,0:T(8,128)(2,1)S(1)}, u32[]{:S(2)}, u32[]{:S(2)}) async-start(bf16[4,256,384]{2,1,0:T(8,128)(2,1)} %fusion.10), calls=%async_computation.4 | async-start | bytes 1572864 | tf_op jit(solution)/shard_map/all_to_all | solution.py:148
  142.3 11.9 %all-to-all-done.4 = bf16[4,256,384]{2,1,0:T(8,128)(2,1)S(1)} async-done(((bf16[4,256,384]{2,1,0:T(8,128)(2,1)}), bf16[4,256,384]{2,1,0:T(8,128)(2,1)S(1)}, u32[]{:S(2)}, u32[]{:S(2)}) %all-to-all-start.4) | async-done | bytes 786464 | tf_op jit(solution)/shard_map/all_to_all | solution.py:148
  155.1 4.5 %all-to-all-start.5 = ((f32[8,2,384]{2,1,0:T(2,128)}), f32[8,2,384]{2,1,0:T(2,128)S(1)}, u32[]{:S(2)}, u32[]{:S(2)}) async-start(f32[8,2,384]{2,1,0:T(2,128)} %broadcast_in_dim.14), calls=%async_computation.5 | async-start | bytes 49152 | tf_op jit(solution)/shard_map/all_to_all | solution.py:154
  159.6 0.8 dynamic_slice.23
  160.3 3.9 %all-to-all-done.5 = f32[8,2,384]{2,1,0:T(2,128)S(1)} async-done(((f32[8,2,384]{2,1,0:T(2,128)}), f32[8,2,384]{2,1,0:T(2,128)S(1)}, u32[]{:S(2)}, u32[]{:S(2)}) %all-to-all-start.5) | async-done | bytes 24608 | tf_op jit(solution)/shard_map/all_to_all | solution.py:154
  164.4 0.8 copy.73
  (62 shorter events, 11.3 us)
Async XLA Ops:
  6.5 118.6 %all-gather.2.cloned.1.call-start = ((), (), s32[]{:S(2)}) async-start(), calls=%async_computation.6 | async-start | bytes 9437184 | tf_op jit(solution)/shard_map/all_gather | solution.py:106
  43.5 7.0 %copy-start = (bf16[384,256]{1,0:T(8,128)(2,1)S(1)}, bf16[384,256]{1,0:T(8,128)(2,1)}, u32[]{:S(2)}) copy-start(bf16[384,256]{1,0:T(8,128)(2,1)} %param.12) | copy-start | bytes 589828
  43.5 38.9 %all-to-all-start.1 = ((bf16[8,256,384]{2,1,0:T(8,128)(2,1)}), bf16[8,256,384]{2,1,0:T(8,128)(2,1)S(1)}, u32[]{:S(2)}, u32[]{:S(2)}) async-start(bf16[8,256,384]{2,1,0:T(8,128)(2,1)} %broadcast_in_dim.11), calls=%async_computation.1 | async-start | bytes 3145728 | tf_op jit(solution)/shard_map/all_to_all | solution.py:40
  50.6 9.4 %collective-permute-start = (bf16[256,384]{1,0:T(8,128)(2,1)S(1)}, bf16[256,384]{1,0:T(8,128)(2,1)S(1)}, u32[]{:S(2)}, u32[]{:S(2)}) collective-permute-start(bf16[256,384]{1,0:T(8,128)(2,1)S(1)} %bitcast.258), channel_id=1, source_target_pairs={{0,6},{2,0},{4,2},{6,4},{1,7},{3,1},{5,3},{7,5},{8,14},{10,8},{12,... | collective-permute-start | bytes 589832 | tf_op jit(solution)/shard_map/ppermute | solution.py:44
  55.0 8.2 %collective-permute-start.1 = (bf16[256,384]{1,0:T(8,128)(2,1)S(1)}, bf16[256,384]{1,0:T(8,128)(2,1)S(1)}, u32[]{:S(2)}, u32[]{:S(2)}) collective-permute-start(bf16[256,384]{1,0:T(8,128)(2,1)S(1)} %bitcast.259), channel_id=1, source_target_pairs={{0,4},{2,6},{4,0},{6,2},{1,5},{3,7},{5,1},{7,3},{8,12},{10,14},{12... | collective-permute-start | bytes 589832 | tf_op jit(solution)/shard_map/ppermute | solution.py:44
  57.5 9.1 %collective-permute-start.2 = (bf16[256,384]{1,0:T(8,128)(2,1)S(1)}, bf16[256,384]{1,0:T(8,128)(2,1)S(1)}, u32[]{:S(2)}, u32[]{:S(2)}) collective-permute-start(bf16[256,384]{1,0:T(8,128)(2,1)S(1)} %bitcast.260), channel_id=1, source_target_pairs={{0,2},{2,4},{4,6},{6,0},{1,3},{3,5},{5,7},{7,1},{8,10},{10,12},{12... | collective-permute-start | bytes 589832 | tf_op jit(solution)/shard_map/ppermute | solution.py:44
  67.6 7.6 %collective-permute-start.3 = (bf16[4,256,384]{2,1,0:T(8,128)(2,1)}, bf16[4,256,384]{2,1,0:T(8,128)(2,1)S(1)}, u32[]{:S(2)}, u32[]{:S(2)}) collective-permute-start(bf16[4,256,384]{2,1,0:T(8,128)(2,1)} %pad_maximum_fusion.1), channel_id=1, source_target_pairs={{0,1},{1,0},{2,3},{3,2},{4,5},{5,4},{6,7},{7,6},{8,9},{9,8},{10,11... | collective-permute-start | bytes 2359304 | tf_op jit(solution)/shard_map/ppermute | solution.py:48
  94.1 7.7 %collective-permute-start.4 = (bf16[4,384,128]{2,1,0:T(8,128)(2,1)S(1)}, bf16[4,384,128]{2,1,0:T(8,128)(2,1)S(1)}, u32[]{:S(2)}, u32[]{:S(2)}) collective-permute-start(bf16[4,384,128]{2,1,0:T(8,128)(2,1)S(1)} %all_to_all.31), channel_id=1, source_target_pairs={{0,1},{1,0},{2,3},{3,2},{4,5},{5,4},{6,7},{7,6},{8,9},{9,8},{10,11... | collective-permute-start | bytes 1179656 | tf_op jit(solution)/shard_map/ppermute | solution.py:48
  101.0 1.2 copy-start.2
  103.7 17.9 %copy-start.1 = (f32[2048]{0:T(1024)S(1)}, f32[2048]{0:T(1024)}, u32[]{:S(2)}) copy-start(f32[2048]{0:T(1024)} %param.18) | copy-start | bytes 24580
  118.3 5.0 %collective-permute-start.5 = (bf16[4,256,384]{2,1,0:T(8,128)(2,1)S(1)}, bf16[4,256,384]{2,1,0:T(8,128)(2,1)S(1)}, u32[]{:S(2)}, u32[]{:S(2)}) collective-permute-start(bf16[4,256,384]{2,1,0:T(8,128)(2,1)S(1)} %all_to_all.32), channel_id=1, source_target_pairs={{0,1},{1,0},{2,3},{3,2},{4,5},{5,4},{6,7},{7,6},{8,9},{9,8},{10,11... | collective-permute-start | bytes 2359304 | tf_op jit(solution)/shard_map/ppermute | solution.py:48
  133.4 4.2 %collective-permute-start.6 = (bf16[4,256,384]{2,1,0:T(8,128)(2,1)S(1)}, bf16[4,256,384]{2,1,0:T(8,128)(2,1)S(1)}, u32[]{:S(2)}, u32[]{:S(2)}) collective-permute-start(bf16[4,256,384]{2,1,0:T(8,128)(2,1)S(1)} %dynamic-slice_bitcast_fusion), channel_id=1, source_target_pairs={{0,1},{1,0},{2,3},{3,2},{4,5},{5,4},{6,7},{7,6},{8,9},{9,8},{10,11... | collective-permute-start | bytes 2359304 | tf_op jit(solution)/shard_map/ppermute | solution.py:48
  138.7 15.5 %all-to-all-start.4 = ((bf16[4,256,384]{2,1,0:T(8,128)(2,1)}), bf16[4,256,384]{2,1,0:T(8,128)(2,1)S(1)}, u32[]{:S(2)}, u32[]{:S(2)}) async-start(bf16[4,256,384]{2,1,0:T(8,128)(2,1)} %fusion.10), calls=%async_computation.4 | async-start | bytes 1572864 | tf_op jit(solution)/shard_map/all_to_all | solution.py:148
  155.1 9.2 %all-to-all-start.5 = ((f32[8,2,384]{2,1,0:T(2,128)}), f32[8,2,384]{2,1,0:T(2,128)S(1)}, u32[]{:S(2)}, u32[]{:S(2)}) async-start(f32[8,2,384]{2,1,0:T(2,128)} %broadcast_in_dim.14), calls=%async_computation.5 | async-start | bytes 49152 | tf_op jit(solution)/shard_map/all_to_all | solution.py:154
Sparse Core Ops, SparseCore 0:
  42.2 68.9 all-gather.1

commit v6 on v5

--- a/solution.py
+++ b/solution.py
@@ -2,6 +2,8 @@
 import jax.numpy as jnp
 import numpy as np
 from jax import lax
+from jax.experimental import pallas as pl
+from jax.experimental.pallas import tpu as pltpu
 from jax.sharding import Mesh
 from jax.sharding import PartitionSpec as P
 
@@ -38,6 +40,52 @@
 def sent_to_group(shard, groups):
     copies = jnp.broadcast_to(shard, (SIDE, *shard.shape))
     return lax.all_to_all(copies, ALL, 0, 0, axis_index_groups=groups, tiled=True)
+
+
+def pairs(groups, by):
+    return [(group[i], group[(i + by) % SIDE]) for group in groups for i in range(SIDE)]
+
+
+def start_whole(place_ref, block, out, sem):
+    rows = block.shape[0]
+    at = pl.multiple_of(place_ref[0] * rows, rows)
+    copy = pltpu.make_async_copy(block, out.at[pl.ds(at, rows)], sem)
+    copy.start()
+    copy.wait()
+
+
+def whole_with(block, place):
+    rows, columns = block.shape
+    size = rows * columns
+    return pl.pallas_call(
+        start_whole,
+        out_shape=jax.ShapeDtypeStruct((SIDE * rows, columns), block.dtype),
+        in_specs=[pl.BlockSpec(memory_space=pltpu.SMEM), pl.BlockSpec(memory_space=pl.ANY)],
+        out_specs=pl.BlockSpec(memory_space=pl.ANY),
+        scratch_shapes=[pltpu.SemaphoreType.DMA],
+        cost_estimate=pl.CostEstimate(flops=size, bytes_accessed=4 * size, transcendentals=0),
+        compiler_params=pltpu.CompilerParams(vmem_limit_bytes=1 << 20),
+        name="start_whole",
+    )(place.astype(jnp.int32).reshape(1), block)
+
+
+def ring_gathered(block, place):
+    rows = block.shape[0]
+    half = rows // 2
+    whole = whole_with(block, place)
+
+    def put(whole, piece, distance, row=0):
+        at = lax.rem(place + distance, SIDE) * rows + row
+        return lax.dynamic_update_slice_in_dim(whole, piece, at, 0)
+
+    above = below = block
+    for step in range(1, 4):
+        above = lax.ppermute(above, ALL, pairs(SECOND, -1))
+        below = lax.ppermute(below, ALL, pairs(SECOND, 1))
+        whole = put(put(whole, above, step), below, SIDE - step)
+    low = lax.ppermute(above[:half], ALL, pairs(SECOND, -1))
+    high = lax.ppermute(below[half:], ALL, pairs(SECOND, 1))
+    return put(put(whole, low, 4), high, 4, half)
 
 
 def along_x(a, by):
@@ -103,7 +151,7 @@
     shard = jnp.concatenate([w_up, w_down.T, w_value, w_gate, jnp.concatenate(halves, 0)], 1)
     shard = sent_to_group(shard, FIRST).reshape(-1, shard.shape[1])
     at = 2 * units_part
-    wide = lax.all_gather(shard[:, :at], ALL, axis=0, tiled=True, axis_index_groups=SECOND)
+    wide = ring_gathered(shard[:, :at], jnp.where(core == 0, lax.axis_index("z"), lax.axis_index("y")))
     small = sent_to_group(shard[:, at:], SECOND)
     value_gate = small[:, :, : 2 * channel_part].reshape(WIDTH, 2 * channel_part)
     mix = small[:, :, 2 * channel_part :].reshape(SIDE, SIDE, 2, mix_rows, channel_part)

time: 173 us -> 206 us (1.19)
  starting transfers between devices: 41.5 us -> 76.9 us
  local copies, waits for them, and re-layouts: 10.3 us -> 37.4 us
  blocking collectives: 55 us -> 30.5 us
  between operations: 13.8 us -> 0.55 us
  other arithmetic: 10.5 us -> 16.1 us
  matrix products: 9.11 us -> 11.7 us
    all_to_all x2 -> x0, blocking collectives: 24.5 us -> none  [all_ranks(): mine = lax.all_to_all(copies, 'x', 0, 0, tiled=True)]
    ppermute x0 -> x8, starting transfers between devices: none -> 21.1 us  [the longest x3 8.67 us: ring_gathered(): below = lax.ppermute(below, ALL, pairs(SECOND, 1))]
    dynamic_update_slice x0 -> x8, local copies, waits for them, and re-layouts: none -> 16.6 us  [put(): return lax.dynamic_update_slice_in_dim(whole, piece, at, 0)]
    all_to_all x0 -> x2, starting transfers between devices: none -> 7.15 us  [all_ranks(): mine = lax.all_to_all(copies, 'x', 0, 0, tiled=True)]
    all_to_all x1, waiting for transfers between devices: 5.21 us -> 0.01 us  [sent_to_group(): lax.all_to_all(copies, ALL, 0, 0, axis_index_groups=groups, tiled=True)]
    ppermute x0 -> x8, waiting for transfers between devices: none -> 5.03 us  [the longest x3 5.01 us: ring_gathered(): above = lax.ppermute(above, ALL, pairs(SECOND, -1))]
    unnamed x11 -> x27, local copies, waits for them, and re-layouts: 3.27 us -> 8.13 us
    ppermute x4, starting transfers between devices: 17.2 us -> 22 us  [partner_of(): return lax.ppermute(a, 'core', [(0, 1), (1, 0)])]
  transfers between devices with their start and end apart: 11 -> 20, of which waited for: 8 -> 7; matrix products, arithmetic and copies ran while one was open for 8% -> 18% of each run, Pallas kernels for 0% -> 0%
where the time goes in v6:
time: 206 us; the launch traced here: 204 us
  starting transfers between devices  76.9 us (37%)
  local copies, waits for them, and re-layouts  37.4 us (18%)
  waiting for transfers between devices  30.7 us (15%)
  blocking collectives  30.5 us (15%)
  other arithmetic  16.1 us (8%)
  matrix products  11.7 us (6%)
    all_to_all x1, blocking collectives, sent_to_group(): lax.all_to_all(copies, ALL, 0, 0, axis_index_groups=groups, tiled=True)  30.5 us
    ppermute x4, starting transfers between devices, partner_of(): return lax.ppermute(a, 'core', [(0, 1), (1, 0)])  22 us
    dynamic_update_slice x8, local copies, waits for them, and re-layouts, put(): return lax.dynamic_update_slice_in_dim(whole, piece, at, 0)  16.6 us
    all_to_all x1, waiting for transfers between devices, layer(): arrived = lax.all_to_all(pair, 'x', 0, 0, tiled=True)  11.7 us
    ppermute x3, starting transfers between devices, along_x(): return lax.ppermute(a, 'x', [(i, (i + by) % 4) for i in range(4)])  10.5 us
    dot_general x1, matrix products, layer(): terms = jnp.dot(wide[:, units_part:], hidden, preferred_element_type=f32)  9.57 us
    ppermute x3, starting transfers between devices, ring_gathered(): below = lax.ppermute(below, ALL, pairs(SECOND, 1))  8.67 us
    unnamed x27, local copies, waits for them, and re-layouts  8.13 us
  transfers between devices with their start and end apart: 20, of which 7 were waited for; matrix products, arithmetic and copies ran while one was open for 18% of the time, Pallas kernels for 0%

profile of v6, /device:TPU:1, one launch (start us, length us, event | category | flops | bytes accessed | tf_op | source)
XLA Modules:
  0.0 203.9 jit_solution(2620039524082739230)
XLA Ops:
  3.9 30.5 %all_to_all.30 = bf16[8,32,2432]{2,1,0:T(8,128)(2,1)S(1)} all-to-all(bf16[8,32,2432]{2,1,0:T(8,128)(2,1)S(1)} %broadcast_in_dim.10), channel_id=1, replica_groups={{0,8,16,24,32,40,48,56},{64,72,80,88,96,104,112,120},{128,136,144,152,1..., dimensions={0} | all-to-all | bytes 2490368 | tf_op jit(solution)/shard_map/all_to_all | solution.py:42
  36.0 6.8 %all-to-all-start.1 = ((bf16[8,256,384]{2,1,0:T(8,128)(2,1)}), bf16[8,256,384]{2,1,0:T(8,128)(2,1)S(1)}, u32[]{:S(2)}, u32[]{:S(2)}) async-start(bf16[8,256,384]{2,1,0:T(8,128)(2,1)} %broadcast_in_dim.11), calls=%async_computation.1 | async-start | bytes 3145728 | tf_op jit(solution)/shard_map/all_to_all | solution.py:42
  43.0 3.1 %collective-permute-start.2 = (bf16[256,384]{1,0:T(8,128)(2,1)S(1)}, bf16[256,384]{1,0:T(8,128)(2,1)S(1)}, u32[]{:S(2)}, u32[]{:S(2)}) collective-permute-start(bf16[256,384]{1,0:T(8,128)(2,1)S(1)} %bitcast.259), channel_id=1, source_target_pairs={{0,2},{2,4},{4,6},{6,0},{1,3},{3,5},{5,7},{7,1},{8,10},{10,12},{12... | collective-permute-start | bytes 589832 | tf_op jit(solution)/shard_map/ppermute | solution.py:92
  46.1 4.4 %collective-permute-start.1 = (bf16[256,384]{1,0:T(8,128)(2,1)S(1)}, bf16[256,384]{1,0:T(8,128)(2,1)S(1)}, u32[]{:S(2)}, u32[]{:S(2)}) collective-permute-start(bf16[256,384]{1,0:T(8,128)(2,1)S(1)} %bitcast.260), channel_id=1, source_target_pairs={{0,4},{2,6},{4,0},{6,2},{1,5},{3,7},{5,1},{7,3},{8,12},{10,14},{12... | collective-permute-start | bytes 589832 | tf_op jit(solution)/shard_map/ppermute | solution.py:92
  50.5 3.1 %collective-permute-start = (bf16[256,384]{1,0:T(8,128)(2,1)S(1)}, bf16[256,384]{1,0:T(8,128)(2,1)S(1)}, u32[]{:S(2)}, u32[]{:S(2)}) collective-permute-start(bf16[256,384]{1,0:T(8,128)(2,1)S(1)} %bitcast.261), channel_id=1, source_target_pairs={{0,6},{2,0},{4,2},{6,4},{1,7},{3,1},{5,3},{7,5},{8,14},{10,8},{12,... | collective-permute-start | bytes 589832 | tf_op jit(solution)/shard_map/ppermute | solution.py:92
  53.6 2.4 %collective-permute-done.1 = bf16[256,384]{1,0:T(8,128)(2,1)S(1)} collective-permute-done((bf16[256,384]{1,0:T(8,128)(2,1)S(1)}, bf16[256,384]{1,0:T(8,128)(2,1)S(1)}, u32[]{:S(2)}, u32[]{:S(2)}) %collective-permute-start.1) | collective-permute-done | bytes 196640 | tf_op jit(solution)/shard_map/ppermute | solution.py:92
  56.0 2.7 %collective-permute-done = bf16[256,384]{1,0:T(8,128)(2,1)S(1)} collective-permute-done((bf16[256,384]{1,0:T(8,128)(2,1)S(1)}, bf16[256,384]{1,0:T(8,128)(2,1)S(1)}, u32[]{:S(2)}, u32[]{:S(2)}) %collective-permute-start) | collective-permute-done | bytes 196640 | tf_op jit(solution)/shard_map/ppermute | solution.py:92
  59.8 4.3 %collective-permute-start.3 = (bf16[4,256,384]{2,1,0:T(8,128)(2,1)}, bf16[4,256,384]{2,1,0:T(8,128)(2,1)S(1)}, u32[]{:S(2)}, u32[]{:S(2)}) collective-permute-start(bf16[4,256,384]{2,1,0:T(8,128)(2,1)} %pad_maximum_fusion.1), channel_id=1, source_target_pairs={{0,1},{1,0},{2,3},{3,2},{4,5},{5,4},{6,7},{7,6},{8,9},{9,8},{10,11... | collective-permute-start | bytes 2359304 | tf_op jit(solution)/shard_map/ppermute | solution.py:96
  68.5 3.4 %collective-permute-start.7 = (bf16[256,2048]{1,0:T(8,128)(2,1)S(1)}, bf16[256,2048]{1,0:T(8,128)(2,1)}, u32[]{:S(2)}, u32[]{:S(2)}) collective-permute-start(bf16[256,2048]{1,0:T(8,128)(2,1)S(1)} %slice.306.block), channel_id=1, source_target_pairs={{0,64},{64,128},{128,192},{192,256},{256,320},{320,384},{384,448},... | collective-permute-start | bytes 3145736 | tf_op jit(solution)/shard_map/ppermute | solution.py:84
  72.9 2.7 %select_bitcast_fusion.3 = (bf16[4,1,256,384]{3,2,1,0:T(8,128)(2,1)S(1)}, bf16[4,256,384]{2,1,0:T(8,128)(2,1)S(1)}) fusion(pred[]{:T(512)S(6)} %eq.4, s32[]{:T(128)S(6)} %select_n.137, bf16[4,256,384]{2,1,0:T(8,128)(2,1)S(1)} %collective-permute-done.3, bf16[1,256,384]{2,1,0:T(8,128)(2,1)} %bitcast.267, bf16[1,256,384]{2,1,0:T(8,128)(2,1)} %bitcast.269, ...), kind=kLoop, calls=%fused_computation.57 | loop fusion | flops 3538944 | bytes 3145733 | tf_op jit(solution)/shard_map/stack | solution.py:165
  77.5 5.0 %collective-permute-done.6 = bf16[256,2048]{1,0:T(8,128)(2,1)} collective-permute-done((bf16[256,2048]{1,0:T(8,128)(2,1)S(1)}, bf16[256,2048]{1,0:T(8,128)(2,1)}, u32[]{:S(2)}, u32[]{:S(2)}) %collective-permute-start.6) | collective-permute-done | bytes 1048608 | tf_op jit(solution)/shard_map/ppermute | solution.py:83
  82.5 3.1 %collective-permute-start.8 = (bf16[256,2048]{1,0:T(8,128)(2,1)}, bf16[256,2048]{1,0:T(8,128)(2,1)}, u32[]{:S(2)}, u32[]{:S(2)}) collective-permute-start(bf16[256,2048]{1,0:T(8,128)(2,1)} %collective-permute-done.6), channel_id=1, source_target_pairs={{0,448},{64,0},{128,64},{192,128},{256,192},{320,256},{384,320},{4... | collective-permute-start | bytes 3145736 | tf_op jit(solution)/shard_map/ppermute | solution.py:83
  85.6 2.2 %collective-permute-start.9 = (bf16[256,2048]{1,0:T(8,128)(2,1)}, bf16[256,2048]{1,0:T(8,128)(2,1)}, u32[]{:S(2)}, u32[]{:S(2)}) collective-permute-start(bf16[256,2048]{1,0:T(8,128)(2,1)} %collective-permute-done.7), channel_id=1, source_target_pairs={{0,64},{64,128},{128,192},{192,256},{256,320},{320,384},{384,448},... | collective-permute-start | bytes 3145736 | tf_op jit(solution)/shard_map/ppermute | solution.py:84
  91.4 3.7 %all-to-all-start.2 = ((bf16[4,384,128]{2,1,0:T(8,128)(2,1)}), bf16[4,384,128]{2,1,0:T(8,128)(2,1)S(1)}, u32[]{:S(2)}, u32[]{:S(2)}) async-start(bf16[4,384,128]{2,1,0:T(8,128)(2,1)} %broadcast_in_dim.12), calls=%async_computation.2 | async-start | bytes 786432 | tf_op jit(solution)/shard_map/all_to_all | solution.py:105
  95.3 3.2 %copy-done = bf16[2048,2048]{1,0:T(8,128)(2,1)} copy-done((bf16[2048,2048]{1,0:T(8,128)(2,1)}, bf16[2048,2048]{1,0:T(8,128)(2,1)S(1)}, u32[]{:S(2)}) %copy-start) | copy-done | bytes 8388632
  98.5 2.8 %all-to-all-done.2 = bf16[4,384,128]{2,1,0:T(8,128)(2,1)S(1)} async-done(((bf16[4,384,128]{2,1,0:T(8,128)(2,1)}), bf16[4,384,128]{2,1,0:T(8,128)(2,1)S(1)}, u32[]{:S(2)}, u32[]{:S(2)}) %all-to-all-start.2) | async-done | bytes 393248 | tf_op jit(solution)/shard_map/all_to_all | solution.py:105
  101.3 7.0 %collective-permute-start.4 = (bf16[4,384,128]{2,1,0:T(8,128)(2,1)S(1)}, bf16[4,384,128]{2,1,0:T(8,128)(2,1)S(1)}, u32[]{:S(2)}, u32[]{:S(2)}) collective-permute-start(bf16[4,384,128]{2,1,0:T(8,128)(2,1)S(1)} %all-to-all-done.2), channel_id=1, source_target_pairs={{0,1},{1,0},{2,3},{3,2},{4,5},{5,4},{6,7},{7,6},{8,9},{9,8},{10,11... | collective-permute-start | bytes 1179656 | tf_op jit(solution)/shard_map/ppermute | solution.py:96
  108.3 2.3 %constant_dynamic-update-slice_fusion.11 = bf16[2048,2048]{1,0:T(8,128)(2,1)} fusion(bf16[2048,2048]{1,0:T(8,128)(2,1)} %copy-done, bf16[256,2048]{1,0:T(8,128)(2,1)} %collective-permute-done.6, s32[]{:T(128)S(6)} %select_n.122), kind=kLoop, calls=%fused_computation.179 | loop fusion | bytes 2097156 | tf_op jit(solution)/shard_map/dynamic_update_slice | solution.py:79
  112.8 3.2 %collective-permute-start.11 = (bf16[256,2048]{1,0:T(8,128)(2,1)}, bf16[256,2048]{1,0:T(8,128)(2,1)}, u32[]{:S(2)}, u32[]{:S(2)}) collective-permute-start(bf16[256,2048]{1,0:T(8,128)(2,1)} %collective-permute-done.9), channel_id=1, source_target_pairs={{0,64},{64,128},{128,192},{192,256},{256,320},{320,384},{384,448},... | collective-permute-start | bytes 3145736 | tf_op jit(solution)/shard_map/ppermute | solution.py:84
  121.7 3.5 %all-to-all-start.3 = ((bf16[4,256,384]{2,1,0:T(8,128)(2,1)}), bf16[4,256,384]{2,1,0:T(8,128)(2,1)S(1)}, u32[]{:S(2)}, u32[]{:S(2)}) async-start(bf16[4,256,384]{2,1,0:T(8,128)(2,1)} %broadcast_in_dim.13), calls=%async_computation.3 | async-start | bytes 1572864 | tf_op jit(solution)/shard_map/all_to_all | solution.py:105
  125.2 2.4 %constant_dynamic-update-slice_fusion.10 = bf16[2048,2048]{1,0:T(8,128)(2,1)} fusion(bf16[2048,2048]{1,0:T(8,128)(2,1)} %constant_dynamic-update-slice_fusion.11, bf16[256,2048]{1,0:T(8,128)(2,1)} %collective-permute-done.7, s32[]{:T(128)S(6)} %select_n.123), kind=kLoop, calls=%fused_computation.178 | loop fusion | bytes 2097156 | tf_op jit(solution)/shard_map/dynamic_update_slice | solution.py:79
  127.5 2.3 %constant_dynamic-update-slice_fusion.9 = bf16[2048,2048]{1,0:T(8,128)(2,1)} fusion(bf16[2048,2048]{1,0:T(8,128)(2,1)} %constant_dynamic-update-slice_fusion.10, bf16[256,2048]{1,0:T(8,128)(2,1)} %collective-permute-done.8, s32[]{:T(128)S(6)} %select_n.124), kind=kLoop, calls=%fused_computation.177 | loop fusion | bytes 2097156 | tf_op jit(solution)/shard_map/dynamic_update_slice | solution.py:79
  129.9 3.3 %collective-permute-start.12 = (bf16[128,2048]{1,0:T(8,128)(2,1)S(1)}, bf16[128,2048]{1,0:T(8,128)(2,1)}, u32[]{:S(2)}, u32[]{:S(2)}) collective-permute-start(bf16[128,2048]{1,0:T(8,128)(2,1)S(1)} %slice.307), channel_id=1, source_target_pairs={{0,448},{64,0},{128,64},{192,128},{256,192},{320,256},{384,320},{4... | collective-permute-start | bytes 1572872 | tf_op jit(solution)/shard_map/ppermute | solution.py:86
  133.2 2.3 %constant_dynamic-update-slice_fusion.8 = bf16[2048,2048]{1,0:T(8,128)(2,1)} fusion(bf16[2048,2048]{1,0:T(8,128)(2,1)} %constant_dynamic-update-slice_fusion.9, bf16[256,2048]{1,0:T(8,128)(2,1)} %collective-permute-done.9, s32[]{:T(128)S(6)} %select_n.125), kind=kLoop, calls=%fused_computation.176 | loop fusion | bytes 2097156 | tf_op jit(solution)/shard_map/dynamic_update_slice | solution.py:79
  139.5 5.6 %collective-permute-start.5 = (bf16[4,256,384]{2,1,0:T(8,128)(2,1)S(1)}, bf16[4,256,384]{2,1,0:T(8,128)(2,1)S(1)}, u32[]{:S(2)}, u32[]{:S(2)}) collective-permute-start(bf16[4,256,384]{2,1,0:T(8,128)(2,1)S(1)} %all-to-all-done.3), channel_id=1, source_target_pairs={{0,1},{1,0},{2,3},{3,2},{4,5},{5,4},{6,7},{7,6},{8,9},{9,8},{10,11... | collective-permute-start | bytes 2359304 | tf_op jit(solution)/shard_map/ppermute | solution.py:96
  146.2 2.3 %constant_dynamic-update-slice_fusion.6 = bf16[2048,2048]{1,0:T(8,128)(2,1)} fusion(bf16[2048,2048]{1,0:T(8,128)(2,1)} %constant_dynamic-update-slice_fusion.7, bf16[256,2048]{1,0:T(8,128)(2,1)} %collective-permute-done.11, s32[]{:T(128)S(6)} %select_n.127), kind=kLoop, calls=%fused_computation.174 | loop fusion | bytes 2097156 | tf_op jit(solution)/shard_map/dynamic_update_slice | solution.py:79
  155.3 9.6 %fusion.7 = bf16[2048,384]{1,0:T(8,128)(2,1)} fusion(bf16[2048,2048]{1,0:T(8,128)(2,1)} %constant_dynamic-update-slice_fusion.4, bf16[2048,384]{1,0:T(8,128)(2,1)} %bitcast.265), kind=kOutput, calls=%fused_computation.9 | convolution fusion | flops 3223191552 | bytes 11534336 | tf_op jit(solution)/shard_map/dot_general | solution.py:190
  168.0 5.1 %collective-permute-start.14 = (bf16[4,256,384]{2,1,0:T(8,128)(2,1)}, bf16[4,256,384]{2,1,0:T(8,128)(2,1)S(1)}, u32[]{:S(2)}, u32[]{:S(2)}) collective-permute-start(bf16[4,256,384]{2,1,0:T(8,128)(2,1)} %dynamic-slice_bitcast_fusion), channel_id=1, source_target_pairs={{0,1},{1,0},{2,3},{3,2},{4,5},{5,4},{6,7},{7,6},{8,9},{9,8},{10,11... | collective-permute-start | bytes 2359304 | tf_op jit(solution)/shard_map/ppermute | solution.py:96
  176.3 4.5 %all-to-all-start.4 = ((bf16[4,256,384]{2,1,0:T(8,128)(2,1)}), bf16[4,256,384]{2,1,0:T(8,128)(2,1)S(1)}, u32[]{:S(2)}, u32[]{:S(2)}) async-start(bf16[4,256,384]{2,1,0:T(8,128)(2,1)} %fusion.10), calls=%async_computation.4 | async-start | bytes 1572864 | tf_op jit(solution)/shard_map/all_to_all | solution.py:196
  180.9 11.7 %all-to-all-done.4 = bf16[4,256,384]{2,1,0:T(8,128)(2,1)S(1)} async-done(((bf16[4,256,384]{2,1,0:T(8,128)(2,1)}), bf16[4,256,384]{2,1,0:T(8,128)(2,1)S(1)}, u32[]{:S(2)}, u32[]{:S(2)}) %all-to-all-start.4) | async-done | bytes 786464 | tf_op jit(solution)/shard_map/all_to_all | solution.py:196
  193.5 4.8 %all-to-all-start.5 = ((f32[8,2,384]{2,1,0:T(2,128)}), f32[8,2,384]{2,1,0:T(2,128)S(1)}, u32[]{:S(2)}, u32[]{:S(2)}) async-start(f32[8,2,384]{2,1,0:T(2,128)} %broadcast_in_dim.14), calls=%async_computation.5 | async-start | bytes 49152 | tf_op jit(solution)/shard_map/all_to_all | solution.py:202
  199.0 3.9 %all-to-all-done.5 = f32[8,2,384]{2,1,0:T(2,128)S(1)} async-done(((f32[8,2,384]{2,1,0:T(2,128)}), f32[8,2,384]{2,1,0:T(2,128)S(1)}, u32[]{:S(2)}, u32[]{:S(2)}) %all-to-all-start.5) | async-done | bytes 24608 | tf_op jit(solution)/shard_map/all_to_all | solution.py:202
  (104 shorter events, 46.3 us)
Async XLA Ops:
  34.4 1.6 copy-start.2
  35.9 6.9 %copy-start.8 = (bf16[384,256]{1,0:T(8,128)(2,1)S(1)}, bf16[384,256]{1,0:T(8,128)(2,1)}, u32[]{:S(2)}) copy-start(bf16[384,256]{1,0:T(8,128)(2,1)} %param.12) | copy-start | bytes 589828
  36.0 51.8 %all-to-all-start.1 = ((bf16[8,256,384]{2,1,0:T(8,128)(2,1)}), bf16[8,256,384]{2,1,0:T(8,128)(2,1)S(1)}, u32[]{:S(2)}, u32[]{:S(2)}) async-start(bf16[8,256,384]{2,1,0:T(8,128)(2,1)} %broadcast_in_dim.11), calls=%async_computation.1 | async-start | bytes 3145728 | tf_op jit(solution)/shard_map/all_to_all | solution.py:42
  43.0 21.1 %copy-start.3 = (bf16[384,256]{0,1:T(8,128)(2,1)}, bf16[384,256]{0,1:T(8,128)(2,1)S(1)}, u32[]{:S(2)}) copy-start(bf16[384,256]{0,1:T(8,128)(2,1)S(1)} %copy.59) | copy-start | bytes 589828
  43.0 10.6 %collective-permute-start.2 = (bf16[256,384]{1,0:T(8,128)(2,1)S(1)}, bf16[256,384]{1,0:T(8,128)(2,1)S(1)}, u32[]{:S(2)}, u32[]{:S(2)}) collective-permute-start(bf16[256,384]{1,0:T(8,128)(2,1)S(1)} %bitcast.259), channel_id=1, source_target_pairs={{0,2},{2,4},{4,6},{6,0},{1,3},{3,5},{5,7},{7,1},{8,10},{10,12},{12... | collective-permute-start | bytes 589832 | tf_op jit(solution)/shard_map/ppermute | solution.py:92
  46.1 9.9 %collective-permute-start.1 = (bf16[256,384]{1,0:T(8,128)(2,1)S(1)}, bf16[256,384]{1,0:T(8,128)(2,1)S(1)}, u32[]{:S(2)}, u32[]{:S(2)}) collective-permute-start(bf16[256,384]{1,0:T(8,128)(2,1)S(1)} %bitcast.260), channel_id=1, source_target_pairs={{0,4},{2,6},{4,0},{6,2},{1,5},{3,7},{5,1},{7,3},{8,12},{10,14},{12... | collective-permute-start | bytes 589832 | tf_op jit(solution)/shard_map/ppermute | solution.py:92
  50.5 8.3 %collective-permute-start = (bf16[256,384]{1,0:T(8,128)(2,1)S(1)}, bf16[256,384]{1,0:T(8,128)(2,1)S(1)}, u32[]{:S(2)}, u32[]{:S(2)}) collective-permute-start(bf16[256,384]{1,0:T(8,128)(2,1)S(1)} %bitcast.261), channel_id=1, source_target_pairs={{0,6},{2,0},{4,2},{6,4},{1,7},{3,1},{5,3},{7,5},{8,14},{10,8},{12,... | collective-permute-start | bytes 589832 | tf_op jit(solution)/shard_map/ppermute | solution.py:92
  53.6 5.2 %copy-start.5 = (bf16[256,384]{1,0:T(8,128)(2,1)}, bf16[256,384]{1,0:T(8,128)(2,1)S(1)}, u32[]{:S(2)}) copy-start(bf16[256,384]{1,0:T(8,128)(2,1)S(1)} %collective-permute-done.2) | copy-start | bytes 589828
  56.0 3.8 %copy-start.6 = (bf16[256,384]{1,0:T(8,128)(2,1)}, bf16[256,384]{1,0:T(8,128)(2,1)S(1)}, u32[]{:S(2)}) copy-start(bf16[256,384]{1,0:T(8,128)(2,1)S(1)} %collective-permute-done.1) | copy-start | bytes 589828
  58.8 5.3 %copy-start.7 = (bf16[256,384]{1,0:T(8,128)(2,1)}, bf16[256,384]{1,0:T(8,128)(2,1)S(1)}, u32[]{:S(2)}) copy-start(bf16[256,384]{1,0:T(8,128)(2,1)S(1)} %collective-permute-done) | copy-start | bytes 589828
  59.8 13.1 %collective-permute-start.3 = (bf16[4,256,384]{2,1,0:T(8,128)(2,1)}, bf16[4,256,384]{2,1,0:T(8,128)(2,1)S(1)}, u32[]{:S(2)}, u32[]{:S(2)}) collective-permute-start(bf16[4,256,384]{2,1,0:T(8,128)(2,1)} %pad_maximum_fusion.1), channel_id=1, source_target_pairs={{0,1},{1,0},{2,3},{3,2},{4,5},{5,4},{6,7},{7,6},{8,9},{9,8},{10,11... | collective-permute-start | bytes 2359304 | tf_op jit(solution)/shard_map/ppermute | solution.py:96
  66.5 15.9 %collective-permute-start.6 = (bf16[256,2048]{1,0:T(8,128)(2,1)S(1)}, bf16[256,2048]{1,0:T(8,128)(2,1)}, u32[]{:S(2)}, u32[]{:S(2)}) collective-permute-start(bf16[256,2048]{1,0:T(8,128)(2,1)S(1)} %slice.306.block), channel_id=1, source_target_pairs={{0,448},{64,0},{128,64},{192,128},{256,192},{320,256},{384,320},{4... | collective-permute-start | bytes 3145736 | tf_op jit(solution)/shard_map/ppermute | solution.py:83
  68.5 17.2 %collective-permute-start.7 = (bf16[256,2048]{1,0:T(8,128)(2,1)S(1)}, bf16[256,2048]{1,0:T(8,128)(2,1)}, u32[]{:S(2)}, u32[]{:S(2)}) collective-permute-start(bf16[256,2048]{1,0:T(8,128)(2,1)S(1)} %slice.306.block), channel_id=1, source_target_pairs={{0,64},{64,128},{128,192},{192,256},{256,320},{320,384},{384,448},... | collective-permute-start | bytes 3145736 | tf_op jit(solution)/shard_map/ppermute | solution.py:84
  82.5 28.2 %collective-permute-start.8 = (bf16[256,2048]{1,0:T(8,128)(2,1)}, bf16[256,2048]{1,0:T(8,128)(2,1)}, u32[]{:S(2)}, u32[]{:S(2)}) collective-permute-start(bf16[256,2048]{1,0:T(8,128)(2,1)} %collective-permute-done.6), channel_id=1, source_target_pairs={{0,448},{64,0},{128,64},{192,128},{256,192},{320,256},{384,320},{4... | collective-permute-start | bytes 3145736 | tf_op jit(solution)/shard_map/ppermute | solution.py:83
  85.6 27.2 %collective-permute-start.9 = (bf16[256,2048]{1,0:T(8,128)(2,1)}, bf16[256,2048]{1,0:T(8,128)(2,1)}, u32[]{:S(2)}, u32[]{:S(2)}) collective-permute-start(bf16[256,2048]{1,0:T(8,128)(2,1)} %collective-permute-done.7), channel_id=1, source_target_pairs={{0,64},{64,128},{128,192},{192,256},{256,320},{320,384},{384,448},... | collective-permute-start | bytes 3145736 | tf_op jit(solution)/shard_map/ppermute | solution.py:84
  87.8 1.4 copy-start.1
  89.8 5.3 %copy-start.9 = (f32[2048]{0:T(1024)S(1)}, f32[2048]{0:T(1024)}, u32[]{:S(2)}) copy-start(f32[2048]{0:T(1024)} %param.18) | copy-start | bytes 24580
  91.4 9.9 %all-to-all-start.2 = ((bf16[4,384,128]{2,1,0:T(8,128)(2,1)}), bf16[4,384,128]{2,1,0:T(8,128)(2,1)S(1)}, u32[]{:S(2)}, u32[]{:S(2)}) async-start(bf16[4,384,128]{2,1,0:T(8,128)(2,1)} %broadcast_in_dim.12), calls=%async_computation.2 | async-start | bytes 786432 | tf_op jit(solution)/shard_map/all_to_all | solution.py:105
  95.3 3.2 %copy-start = (bf16[2048,2048]{1,0:T(8,128)(2,1)}, bf16[2048,2048]{1,0:T(8,128)(2,1)S(1)}, u32[]{:S(2)}) copy-start(bf16[2048,2048]{1,0:T(8,128)(2,1)S(1)} %start_whole.1) | copy-start | bytes 25165828
  101.3 16.1 %collective-permute-start.4 = (bf16[4,384,128]{2,1,0:T(8,128)(2,1)S(1)}, bf16[4,384,128]{2,1,0:T(8,128)(2,1)S(1)}, u32[]{:S(2)}, u32[]{:S(2)}) collective-permute-start(bf16[4,384,128]{2,1,0:T(8,128)(2,1)S(1)} %all-to-all-done.2), channel_id=1, source_target_pairs={{0,1},{1,0},{2,3},{3,2},{4,5},{5,4},{6,7},{7,6},{8,9},{9,8},{10,11... | collective-permute-start | bytes 1179656 | tf_op jit(solution)/shard_map/ppermute | solution.py:96
  110.6 19.2 %collective-permute-start.10 = (bf16[256,2048]{1,0:T(8,128)(2,1)}, bf16[256,2048]{1,0:T(8,128)(2,1)S(1)}, u32[]{:S(2)}, u32[]{:S(2)}) collective-permute-start(bf16[256,2048]{1,0:T(8,128)(2,1)} %collective-permute-done.8), channel_id=1, source_target_pairs={{0,448},{64,0},{128,64},{192,128},{256,192},{320,256},{384,320},{4... | collective-permute-start | bytes 3145736 | tf_op jit(solution)/shard_map/ppermute | solution.py:83
  112.8 22.8 %collective-permute-start.11 = (bf16[256,2048]{1,0:T(8,128)(2,1)}, bf16[256,2048]{1,0:T(8,128)(2,1)}, u32[]{:S(2)}, u32[]{:S(2)}) collective-permute-start(bf16[256,2048]{1,0:T(8,128)(2,1)} %collective-permute-done.9), channel_id=1, source_target_pairs={{0,64},{64,128},{128,192},{192,256},{256,320},{320,384},{384,448},... | collective-permute-start | bytes 3145736 | tf_op jit(solution)/shard_map/ppermute | solution.py:84
  117.4 0.7 copy-start.10
  118.1 1.0 copy-start.4
  121.7 17.8 %all-to-all-start.3 = ((bf16[4,256,384]{2,1,0:T(8,128)(2,1)}), bf16[4,256,384]{2,1,0:T(8,128)(2,1)S(1)}, u32[]{:S(2)}, u32[]{:S(2)}) async-start(bf16[4,256,384]{2,1,0:T(8,128)(2,1)} %broadcast_in_dim.13), calls=%async_computation.3 | async-start | bytes 1572864 | tf_op jit(solution)/shard_map/all_to_all | solution.py:105
  129.9 18.6 %collective-permute-start.12 = (bf16[128,2048]{1,0:T(8,128)(2,1)S(1)}, bf16[128,2048]{1,0:T(8,128)(2,1)}, u32[]{:S(2)}, u32[]{:S(2)}) collective-permute-start(bf16[128,2048]{1,0:T(8,128)(2,1)S(1)} %slice.307), channel_id=1, source_target_pairs={{0,448},{64,0},{128,64},{192,128},{256,192},{320,256},{384,320},{4... | collective-permute-start | bytes 1572872 | tf_op jit(solution)/shard_map/ppermute | solution.py:86
  137.5 12.9 %collective-permute-start.13 = (bf16[128,2048]{1,0:T(8,128)(2,1)}, bf16[128,2048]{1,0:T(8,128)(2,1)}, u32[]{:S(2)}, u32[]{:S(2)}) collective-permute-start(bf16[128,2048]{1,0:T(8,128)(2,1)} %slice.308), channel_id=1, source_target_pairs={{0,64},{64,128},{128,192},{192,256},{256,320},{320,384},{384,448},... | collective-permute-start | bytes 1572872 | tf_op jit(solution)/shard_map/ppermute | solution.py:87
  139.5 12.8 %collective-permute-start.5 = (bf16[4,256,384]{2,1,0:T(8,128)(2,1)S(1)}, bf16[4,256,384]{2,1,0:T(8,128)(2,1)S(1)}, u32[]{:S(2)}, u32[]{:S(2)}) collective-permute-start(bf16[4,256,384]{2,1,0:T(8,128)(2,1)S(1)} %all-to-all-done.3), channel_id=1, source_target_pairs={{0,1},{1,0},{2,3},{3,2},{4,5},{5,4},{6,7},{7,6},{8,9},{9,8},{10,11... | collective-permute-start | bytes 2359304 | tf_op jit(solution)/shard_map/ppermute | solution.py:96
  168.0 7.2 %collective-permute-start.14 = (bf16[4,256,384]{2,1,0:T(8,128)(2,1)}, bf16[4,256,384]{2,1,0:T(8,128)(2,1)S(1)}, u32[]{:S(2)}, u32[]{:S(2)}) collective-permute-start(bf16[4,256,384]{2,1,0:T(8,128)(2,1)} %dynamic-slice_bitcast_fusion), channel_id=1, source_target_pairs={{0,1},{1,0},{2,3},{3,2},{4,5},{5,4},{6,7},{7,6},{8,9},{9,8},{10,11... | collective-permute-start | bytes 2359304 | tf_op jit(solution)/shard_map/ppermute | solution.py:96
  176.3 16.2 %all-to-all-start.4 = ((bf16[4,256,384]{2,1,0:T(8,128)(2,1)}), bf16[4,256,384]{2,1,0:T(8,128)(2,1)S(1)}, u32[]{:S(2)}, u32[]{:S(2)}) async-start(bf16[4,256,384]{2,1,0:T(8,128)(2,1)} %fusion.10), calls=%async_computation.4 | async-start | bytes 1572864 | tf_op jit(solution)/shard_map/all_to_all | solution.py:196
  193.5 9.5 %all-to-all-start.5 = ((f32[8,2,384]{2,1,0:T(2,128)}), f32[8,2,384]{2,1,0:T(2,128)S(1)}, u32[]{:S(2)}, u32[]{:S(2)}) async-start(f32[8,2,384]{2,1,0:T(2,128)} %broadcast_in_dim.14), calls=%async_computation.5 | async-start | bytes 49152 | tf_op jit(solution)/shard_map/all_to_all | solution.py:202

commit v7 on v4

--- a/solution.py
+++ b/solution.py
@@ -96,7 +96,8 @@
         return lax.dynamic_slice_in_dim(vector, tp_rank * size, size, vector.ndim - 1)
 
     wide = jnp.concatenate([w_up, w_down.T], 1)
-    wide = lax.all_gather(wide, FS, axis=0, tiled=True)
+    wide = lax.all_gather(wide, ALL, axis=0, tiled=True, axis_index_groups=FIRST)
+    wide = lax.all_gather(wide, ALL, axis=0, tiled=True, axis_index_groups=SECOND)
 
     mix_rows = w_mix_out.shape[0]
     halves = [w_mix_out[:, :channel_part], w_mix_out[:, channel_part:]]
@@ -108,6 +109,8 @@
     mix = turned(core, mix.transpose(0, 1, 3, 2, 4)).reshape(CHANNELS, width_part)
 
     x_rank = lax.axis_index("x")
+    own_mix_gain = mine_of(mix_gain, width_part)
+    own_out_gain = mine_of(out_gain, width_part)
     own_xt = tokens.T
     parts = [own_xt, along_x(own_xt, -1), along_x(own_xt, 2), along_x(own_xt, 1)]
     mine = jnp.stack(parts)
@@ -131,14 +134,16 @@
     spread = jnp.maximum(jnp.sum(combined_whole * combined_whole, 0) / WIDTH - average * average, 0.0)
     scale = lax.rsqrt(spread + norm_eps)
     middle_whole = ((combined_whole - average) * scale * mix_gain[:, None]).astype(bf16)
-    middle = ((combined - average[:, None]) * scale[:, None] * mine_of(mix_gain, width_part)).astype(bf16)
+    middle_whole = turned(core, middle_whole.reshape(SIDE, SIDE, -1, frames)).reshape(WIDTH, frames)
+    middle = ((combined - average[:, None]) * scale[:, None] * own_mix_gain).astype(bf16)
 
     up_proj = lax.dot_general(
         wide[:, :units_part], middle_whole, (((0,), (0,)), ((), ())), preferred_element_type=f32
     )
     hidden = jnp.square(jax.nn.relu(up_proj)).astype(bf16)
     terms = jnp.dot(wide[:, units_part:], hidden, preferred_element_type=f32)
-    terms = terms.astype(bf16).reshape(4, 2, width_part, frames)
+    terms = turned(core, terms.astype(bf16).reshape(SIDE, SIDE, -1, frames))
+    terms = terms.reshape(4, 2, width_part, frames)
     kept = lax.dynamic_index_in_dim(terms, core, 1, keepdims=False)
     given = lax.dynamic_index_in_dim(terms, 1 - core, 1, keepdims=False)
     pair = (kept.astype(f32) + partner_of(given).astype(f32)).astype(bf16)
@@ -152,7 +157,7 @@
     average = totals[0] / WIDTH
     spread = jnp.maximum(totals[1] / WIDTH - average * average, 0.0)
     scale = lax.rsqrt(spread + norm_eps)
-    result = (final - average[:, None]) * scale[:, None] * mine_of(out_gain, width_part)
+    result = (final - average[:, None]) * scale[:, None] * own_out_gain
     return result.astype(bf16)
 
 

time: 171 us -> 201 us (1.18)
  waiting for transfers between devices: 42.2 us -> 70.3 us
  starting transfers between devices: 42.8 us -> 51.6 us
  blocking collectives: 43.8 us -> 36.4 us
    all_gather x1 -> x2, waiting for transfers between devices: 15.8 us -> 43.6 us  [the longest x1 43.6 us: layer(): lax.all_gather(wide, ALL, axis=0, tiled=True, axis_index_groups=FIRST)]
    ppermute x4, starting transfers between devices: 17.8 us -> 27.8 us  [partner_of(): return lax.ppermute(a, 'core', [(0, 1), (1, 0)])]
    all_to_all x1, blocking collectives: 19.3 us -> 12 us  [sent_to_group(): lax.all_to_all(copies, ALL, 0, 0, axis_index_groups=groups, tiled=True)]
  transfers between devices with their start and end apart: 11 -> 12, of which waited for: 8 -> 9; matrix products, arithmetic and copies ran while one was open for 9% -> 8% of each run, Pallas kernels for 0% -> 0%
where the time goes in v7:
time: 201 us; the launch traced here: 200 us
  waiting for transfers between devices  70.3 us (35%)
  starting transfers between devices  51.6 us (26%)
  blocking collectives  36.4 us (18%)
  between operations  13.8 us (7%)
  other arithmetic  12.7 us (6%)
  matrix products  9.1 us (5%)
  local copies, waits for them, and re-layouts  6.03 us (3%)
    all_gather x1, waiting for transfers between devices, layer(): lax.all_gather(wide, ALL, axis=0, tiled=True, axis_index_groups=FIRST)  43.6 us
    ppermute x4, starting transfers between devices, partner_of(): return lax.ppermute(a, 'core', [(0, 1), (1, 0)])  27.8 us
    all_to_all x2, blocking collectives, all_ranks(): mine = lax.all_to_all(copies, 'x', 0, 0, tiled=True)  24.5 us
    all_to_all x1, blocking collectives, sent_to_group(): lax.all_to_all(copies, ALL, 0, 0, axis_index_groups=groups, tiled=True)  12 us
    all_to_all x1, waiting for transfers between devices, layer(): arrived = lax.all_to_all(pair, 'x', 0, 0, tiled=True)  11.9 us
    ppermute x3, starting transfers between devices, along_x(): return lax.ppermute(a, 'x', [(i, (i + by) % 4) for i in range(4)])  9.28 us
    dot_general x1, matrix products, layer(): terms = jnp.dot(wide[:, units_part:], hidden, preferred_element_type=f32)  8.01 us
    all_to_all x1, starting transfers between devices, sent_to_group(): lax.all_to_all(copies, ALL, 0, 0, axis_index_groups=groups, tiled=True)  6.51 us
  transfers between devices with their start and end apart: 12, of which 9 were waited for; matrix products, arithmetic and copies ran while one was open for 8% of the time, Pallas kernels for 0%

profile of v7, /device:TPU:1, one launch (start us, length us, event | category | flops | bytes accessed | tf_op | source)
XLA Modules:
  0.0 199.9 jit_solution(15068640784791123215)
XLA Ops:
  6.5 1.5 pad_maximum_fusion.3
  8.1 43.6 %all-gather.3.cloned.1.call-done = bf16[256,2048]{1,0:T(8,128)(2,1)} async-done(((bf16[32,2048]{1,0:T(8,128)(2,1)}), bf16[256,2048]{1,0:T(8,128)(2,1)}) %all-gather.3.cloned.1.call-update) | async-done | bytes 1048592 | tf_op jit(solution)/shard_map/all_gather | solution.py:99
  52.5 0.7 maximum_maximum_fusion
  53.2 12.0 %all_to_all.30 = bf16[8,32,384]{2,1,0:T(8,128)(2,1)S(1)} all-to-all(bf16[8,32,384]{2,1,0:T(8,128)(2,1)S(1)} %broadcast_in_dim.10), channel_id=1, replica_groups={{0,8,16,24,32,40,48,56},{64,72,80,88,96,104,112,120},{128,136,144,152,1..., dimensions={0} | all-to-all | bytes 393216 | tf_op jit(solution)/shard_map/all_to_all | solution.py:40
  65.2 1.4 broadcast_in_dim.11
  66.6 6.5 %all-to-all-start.1 = ((bf16[8,256,384]{2,1,0:T(8,128)(2,1)}), bf16[8,256,384]{2,1,0:T(8,128)(2,1)S(1)}, u32[]{:S(2)}, u32[]{:S(2)}) async-start(bf16[8,256,384]{2,1,0:T(8,128)(2,1)} %broadcast_in_dim.11), calls=%async_computation.1 | async-start | bytes 3145728 | tf_op jit(solution)/shard_map/all_to_all | solution.py:40
  73.2 4.3 %collective-permute-start = (bf16[256,384]{1,0:T(8,128)(2,1)S(1)}, bf16[256,384]{1,0:T(8,128)(2,1)S(1)}, u32[]{:S(2)}, u32[]{:S(2)}) collective-permute-start(bf16[256,384]{1,0:T(8,128)(2,1)S(1)} %bitcast.255), channel_id=1, source_target_pairs={{0,6},{2,0},{4,2},{6,4},{1,7},{3,1},{5,3},{7,5},{8,14},{10,8},{12,... | collective-permute-start | bytes 589832 | tf_op jit(solution)/shard_map/ppermute | solution.py:44
  77.6 2.5 %collective-permute-start.1 = (bf16[256,384]{1,0:T(8,128)(2,1)S(1)}, bf16[256,384]{1,0:T(8,128)(2,1)S(1)}, u32[]{:S(2)}, u32[]{:S(2)}) collective-permute-start(bf16[256,384]{1,0:T(8,128)(2,1)S(1)} %bitcast.256), channel_id=1, source_target_pairs={{0,4},{2,6},{4,0},{6,2},{1,5},{3,7},{5,1},{7,3},{8,12},{10,14},{12... | collective-permute-start | bytes 589832 | tf_op jit(solution)/shard_map/ppermute | solution.py:44
  80.1 2.5 %collective-permute-start.2 = (bf16[256,384]{1,0:T(8,128)(2,1)S(1)}, bf16[256,384]{1,0:T(8,128)(2,1)S(1)}, u32[]{:S(2)}, u32[]{:S(2)}) collective-permute-start(bf16[256,384]{1,0:T(8,128)(2,1)S(1)} %bitcast.257), channel_id=1, source_target_pairs={{0,2},{2,4},{4,6},{6,0},{1,3},{3,5},{5,7},{7,1},{8,10},{10,12},{12... | collective-permute-start | bytes 589832 | tf_op jit(solution)/shard_map/ppermute | solution.py:44
  82.6 3.0 %collective-permute-done.1 = bf16[256,384]{1,0:T(8,128)(2,1)S(1)} collective-permute-done((bf16[256,384]{1,0:T(8,128)(2,1)S(1)}, bf16[256,384]{1,0:T(8,128)(2,1)S(1)}, u32[]{:S(2)}, u32[]{:S(2)}) %collective-permute-start.1) | collective-permute-done | bytes 196640 | tf_op jit(solution)/shard_map/ppermute | solution.py:44
  85.5 2.5 %collective-permute-done.2 = bf16[256,384]{1,0:T(8,128)(2,1)S(1)} collective-permute-done((bf16[256,384]{1,0:T(8,128)(2,1)S(1)}, bf16[256,384]{1,0:T(8,128)(2,1)S(1)}, u32[]{:S(2)}, u32[]{:S(2)}) %collective-permute-start.2) | collective-permute-done | bytes 196640 | tf_op jit(solution)/shard_map/ppermute | solution.py:44
  88.1 1.0 pad_maximum_fusion.1
  89.1 10.5 %collective-permute-start.3 = (bf16[4,256,384]{2,1,0:T(8,128)(2,1)}, bf16[4,256,384]{2,1,0:T(8,128)(2,1)S(1)}, u32[]{:S(2)}, u32[]{:S(2)}) collective-permute-start(bf16[4,256,384]{2,1,0:T(8,128)(2,1)} %pad_maximum_fusion.1), channel_id=1, source_target_pairs={{0,1},{1,0},{2,3},{3,2},{4,5},{5,4},{6,7},{7,6},{8,9},{9,8},{10,11... | collective-permute-start | bytes 2359304 | tf_op jit(solution)/shard_map/ppermute | solution.py:48
  99.6 1.1 fusion.133
  100.6 1.1 fusion.103
  101.8 1.3 select_bitcast_fusion.3
  103.9 1.1 all-to-all-done.1
  106.4 10.1 %all_to_all.31 = bf16[4,384,128]{2,1,0:T(8,128)(2,1)S(1)} all-to-all(bf16[4,384,128]{2,1,0:T(8,128)(2,1)S(1)} %broadcast_in_dim.12), channel_id=1, replica_groups=mesh['z'=8,'y'=8,'x'=4,'core'=2] {'x'}, dimensions={0} | all-to-all | bytes 786432 | tf_op jit(solution)/shard_map/all_to_all | solution.py:57
  116.5 11.7 %collective-permute-start.4 = (bf16[4,384,128]{2,1,0:T(8,128)(2,1)S(1)}, bf16[4,384,128]{2,1,0:T(8,128)(2,1)S(1)}, u32[]{:S(2)}, u32[]{:S(2)}) collective-permute-start(bf16[4,384,128]{2,1,0:T(8,128)(2,1)S(1)} %all_to_all.31), channel_id=1, source_target_pairs={{0,1},{1,0},{2,3},{3,2},{4,5},{5,4},{6,7},{7,6},{8,9},{9,8},{10,11... | collective-permute-start | bytes 1179656 | tf_op jit(solution)/shard_map/ppermute | solution.py:48
  131.6 14.4 %all_to_all.32 = bf16[4,256,384]{2,1,0:T(8,128)(2,1)S(1)} all-to-all(bf16[4,256,384]{2,1,0:T(8,128)(2,1)S(1)} %broadcast_in_dim.13), channel_id=1, replica_groups=mesh['z'=8,'y'=8,'x'=4,'core'=2] {'x'}, dimensions={0} | all-to-all | bytes 1572864 | tf_op jit(solution)/shard_map/all_to_all | solution.py:57
  146.1 3.3 %collective-permute-start.5 = (bf16[4,256,384]{2,1,0:T(8,128)(2,1)S(1)}, bf16[4,256,384]{2,1,0:T(8,128)(2,1)S(1)}, u32[]{:S(2)}, u32[]{:S(2)}) collective-permute-start(bf16[4,256,384]{2,1,0:T(8,128)(2,1)S(1)} %all_to_all.32), channel_id=1, source_target_pairs={{0,1},{1,0},{2,3},{3,2},{4,5},{5,4},{6,7},{7,6},{8,9},{9,8},{10,11... | collective-permute-start | bytes 2359304 | tf_op jit(solution)/shard_map/ppermute | solution.py:48
  149.5 1.6 collective-permute-done.5
  152.9 8.0 %fusion.7 = bf16[2048,384]{1,0:T(8,128)(2,1)S(1)} fusion(bf16[2048,2048]{1,0:T(8,128)(2,1)} %all-gather.5.cloned.1.call-done, bf16[2048,384]{1,0:T(8,128)(2,1)S(1)} %bitcast.260), kind=kOutput, calls=%fused_computation.9 | convolution fusion | flops 3223191552 | bytes 11534336 | tf_op jit(solution)/shard_map/dot_general | solution.py:144
  161.2 2.3 %collective-permute-start.6 = (bf16[4,256,384]{2,1,0:T(8,128)(2,1)S(1)}, bf16[4,256,384]{2,1,0:T(8,128)(2,1)S(1)}, u32[]{:S(2)}, u32[]{:S(2)}) collective-permute-start(bf16[4,256,384]{2,1,0:T(8,128)(2,1)S(1)} %dynamic-slice_bitcast_fusion), channel_id=1, source_target_pairs={{0,1},{1,0},{2,3},{3,2},{4,5},{5,4},{6,7},{7,6},{8,9},{9,8},{10,11... | collective-permute-start | bytes 2359304 | tf_op jit(solution)/shard_map/ppermute | solution.py:48
  163.5 1.9 collective-permute-done.6
  165.4 1.1 fusion.10
  166.5 3.5 %all-to-all-start.4 = ((bf16[4,256,384]{2,1,0:T(8,128)(2,1)}), bf16[4,256,384]{2,1,0:T(8,128)(2,1)S(1)}, u32[]{:S(2)}, u32[]{:S(2)}) async-start(bf16[4,256,384]{2,1,0:T(8,128)(2,1)} %fusion.10), calls=%async_computation.4 | async-start | bytes 1572864 | tf_op jit(solution)/shard_map/all_to_all | solution.py:150
  170.1 11.9 %all-to-all-done.4 = bf16[4,256,384]{2,1,0:T(8,128)(2,1)S(1)} async-done(((bf16[4,256,384]{2,1,0:T(8,128)(2,1)}), bf16[4,256,384]{2,1,0:T(8,128)(2,1)S(1)}, u32[]{:S(2)}, u32[]{:S(2)}) %all-to-all-start.4) | async-done | bytes 786464 | tf_op jit(solution)/shard_map/all_to_all | solution.py:150
  182.9 4.5 %all-to-all-start.5 = ((f32[8,2,384]{2,1,0:T(2,128)}), f32[8,2,384]{2,1,0:T(2,128)S(1)}, u32[]{:S(2)}, u32[]{:S(2)}) async-start(f32[8,2,384]{2,1,0:T(2,128)} %broadcast_in_dim.14), calls=%async_computation.5 | async-start | bytes 49152 | tf_op jit(solution)/shard_map/all_to_all | solution.py:156
  187.4 0.8 dynamic_slice.23
  188.1 3.9 %all-to-all-done.5 = f32[8,2,384]{2,1,0:T(2,128)S(1)} async-done(((f32[8,2,384]{2,1,0:T(2,128)}), f32[8,2,384]{2,1,0:T(2,128)S(1)}, u32[]{:S(2)}, u32[]{:S(2)}) %all-to-all-start.5) | async-done | bytes 24608 | tf_op jit(solution)/shard_map/all_to_all | solution.py:156
  192.2 0.8 copy.73
  (60 shorter events, 9.8 us)
Async XLA Ops:
  6.5 45.2 %all-gather.3.cloned.1.call-start = ((), (), s32[]{:S(2)}) async-start(), calls=%async_computation.6 | async-start | bytes 1179648 | tf_op jit(solution)/shard_map/all_gather | solution.py:99
  8.1 144.8 %all-gather.5.cloned.1.call-start = ((), (), s32[]{:S(2)}) async-start(), calls=%async_computation.7 | async-start | bytes 9437184 | tf_op jit(solution)/shard_map/all_gather | solution.py:100
  66.6 6.5 %copy-start = (bf16[384,256]{1,0:T(8,128)(2,1)S(1)}, bf16[384,256]{1,0:T(8,128)(2,1)}, u32[]{:S(2)}) copy-start(bf16[384,256]{1,0:T(8,128)(2,1)} %param.12) | copy-start | bytes 589828
  66.6 38.4 %all-to-all-start.1 = ((bf16[8,256,384]{2,1,0:T(8,128)(2,1)}), bf16[8,256,384]{2,1,0:T(8,128)(2,1)S(1)}, u32[]{:S(2)}, u32[]{:S(2)}) async-start(bf16[8,256,384]{2,1,0:T(8,128)(2,1)} %broadcast_in_dim.11), calls=%async_computation.1 | async-start | bytes 3145728 | tf_op jit(solution)/shard_map/all_to_all | solution.py:40
  73.2 9.3 %collective-permute-start = (bf16[256,384]{1,0:T(8,128)(2,1)S(1)}, bf16[256,384]{1,0:T(8,128)(2,1)S(1)}, u32[]{:S(2)}, u32[]{:S(2)}) collective-permute-start(bf16[256,384]{1,0:T(8,128)(2,1)S(1)} %bitcast.255), channel_id=1, source_target_pairs={{0,6},{2,0},{4,2},{6,4},{1,7},{3,1},{5,3},{7,5},{8,14},{10,8},{12,... | collective-permute-start | bytes 589832 | tf_op jit(solution)/shard_map/ppermute | solution.py:44
  77.6 8.0 %collective-permute-start.1 = (bf16[256,384]{1,0:T(8,128)(2,1)S(1)}, bf16[256,384]{1,0:T(8,128)(2,1)S(1)}, u32[]{:S(2)}, u32[]{:S(2)}) collective-permute-start(bf16[256,384]{1,0:T(8,128)(2,1)S(1)} %bitcast.256), channel_id=1, source_target_pairs={{0,4},{2,6},{4,0},{6,2},{1,5},{3,7},{5,1},{7,3},{8,12},{10,14},{12... | collective-permute-start | bytes 589832 | tf_op jit(solution)/shard_map/ppermute | solution.py:44
  80.1 8.0 %collective-permute-start.2 = (bf16[256,384]{1,0:T(8,128)(2,1)S(1)}, bf16[256,384]{1,0:T(8,128)(2,1)S(1)}, u32[]{:S(2)}, u32[]{:S(2)}) collective-permute-start(bf16[256,384]{1,0:T(8,128)(2,1)S(1)} %bitcast.257), channel_id=1, source_target_pairs={{0,2},{2,4},{4,6},{6,0},{1,3},{3,5},{5,7},{7,1},{8,10},{10,12},{12... | collective-permute-start | bytes 589832 | tf_op jit(solution)/shard_map/ppermute | solution.py:44
  89.1 12.7 %collective-permute-start.3 = (bf16[4,256,384]{2,1,0:T(8,128)(2,1)}, bf16[4,256,384]{2,1,0:T(8,128)(2,1)S(1)}, u32[]{:S(2)}, u32[]{:S(2)}) collective-permute-start(bf16[4,256,384]{2,1,0:T(8,128)(2,1)} %pad_maximum_fusion.1), channel_id=1, source_target_pairs={{0,1},{1,0},{2,3},{3,2},{4,5},{5,4},{6,7},{7,6},{8,9},{9,8},{10,11... | collective-permute-start | bytes 2359304 | tf_op jit(solution)/shard_map/ppermute | solution.py:48
  116.5 13.0 %collective-permute-start.4 = (bf16[4,384,128]{2,1,0:T(8,128)(2,1)S(1)}, bf16[4,384,128]{2,1,0:T(8,128)(2,1)S(1)}, u32[]{:S(2)}, u32[]{:S(2)}) collective-permute-start(bf16[4,384,128]{2,1,0:T(8,128)(2,1)S(1)} %all_to_all.31), channel_id=1, source_target_pairs={{0,1},{1,0},{2,3},{3,2},{4,5},{5,4},{6,7},{7,6},{8,9},{9,8},{10,11... | collective-permute-start | bytes 1179656 | tf_op jit(solution)/shard_map/ppermute | solution.py:48
  128.8 1.2 copy-start.2
  131.5 17.9 %copy-start.1 = (f32[2048]{0:T(1024)S(1)}, f32[2048]{0:T(1024)}, u32[]{:S(2)}) copy-start(f32[2048]{0:T(1024)} %param.18) | copy-start | bytes 24580
  146.1 5.0 %collective-permute-start.5 = (bf16[4,256,384]{2,1,0:T(8,128)(2,1)S(1)}, bf16[4,256,384]{2,1,0:T(8,128)(2,1)S(1)}, u32[]{:S(2)}, u32[]{:S(2)}) collective-permute-start(bf16[4,256,384]{2,1,0:T(8,128)(2,1)S(1)} %all_to_all.32), channel_id=1, source_target_pairs={{0,1},{1,0},{2,3},{3,2},{4,5},{5,4},{6,7},{7,6},{8,9},{9,8},{10,11... | collective-permute-start | bytes 2359304 | tf_op jit(solution)/shard_map/ppermute | solution.py:48
  161.2 4.2 %collective-permute-start.6 = (bf16[4,256,384]{2,1,0:T(8,128)(2,1)S(1)}, bf16[4,256,384]{2,1,0:T(8,128)(2,1)S(1)}, u32[]{:S(2)}, u32[]{:S(2)}) collective-permute-start(bf16[4,256,384]{2,1,0:T(8,128)(2,1)S(1)} %dynamic-slice_bitcast_fusion), channel_id=1, source_target_pairs={{0,1},{1,0},{2,3},{3,2},{4,5},{5,4},{6,7},{7,6},{8,9},{9,8},{10,11... | collective-permute-start | bytes 2359304 | tf_op jit(solution)/shard_map/ppermute | solution.py:48
  166.5 15.5 %all-to-all-start.4 = ((bf16[4,256,384]{2,1,0:T(8,128)(2,1)}), bf16[4,256,384]{2,1,0:T(8,128)(2,1)S(1)}, u32[]{:S(2)}, u32[]{:S(2)}) async-start(bf16[4,256,384]{2,1,0:T(8,128)(2,1)} %fusion.10), calls=%async_computation.4 | async-start | bytes 1572864 | tf_op jit(solution)/shard_map/all_to_all | solution.py:150
  182.9 9.2 %all-to-all-start.5 = ((f32[8,2,384]{2,1,0:T(2,128)}), f32[8,2,384]{2,1,0:T(2,128)S(1)}, u32[]{:S(2)}, u32[]{:S(2)}) async-start(f32[8,2,384]{2,1,0:T(2,128)} %broadcast_in_dim.14), calls=%async_computation.5 | async-start | bytes 49152 | tf_op jit(solution)/shard_map/all_to_all | solution.py:156
Sparse Core Ops, SparseCore 0:
  9.4 42.2 all-gather.2
  53.8 76.6 all-gather.4

commit v8 on v5

--- a/solution.py
+++ b/solution.py
@@ -35,9 +35,12 @@
 FIRST, SECOND = rings("yz"), rings("zy")
 
 
+def exchanged(copies, groups):
+    return lax.all_to_all(copies, ALL, 0, 0, axis_index_groups=groups, tiled=True)
+
+
 def sent_to_group(shard, groups):
-    copies = jnp.broadcast_to(shard, (SIDE, *shard.shape))
-    return lax.all_to_all(copies, ALL, 0, 0, axis_index_groups=groups, tiled=True)
+    return exchanged(jnp.broadcast_to(shard, (SIDE, *shard.shape)), groups)
 
 
 def along_x(a, by):
@@ -100,8 +103,12 @@
     own_xt = tokens.T
     mix_rows = w_mix_out.shape[0]
     halves = [w_mix_out[:, :channel_part], w_mix_out[:, channel_part:]]
-    shard = jnp.concatenate([w_up, w_down.T, w_value, w_gate, jnp.concatenate(halves, 0)], 1)
-    shard = sent_to_group(shard, FIRST).reshape(-1, shard.shape[1])
+    wide = jnp.concatenate([w_up, w_down.T], 1)
+    small = jnp.concatenate([w_value, w_gate, jnp.concatenate(halves, 0)], 1)
+    wide, small = lax.optimization_barrier((wide, small))
+    copies = [jnp.broadcast_to(a, (SIDE, *a.shape)) for a in (wide, small)]
+    shard = exchanged(jnp.concatenate(copies, 2), FIRST)
+    shard = shard.reshape(-1, shard.shape[2])
     at = 2 * units_part
     wide = lax.all_gather(shard[:, :at], ALL, axis=0, tiled=True, axis_index_groups=SECOND)
     small = sent_to_group(shard[:, at:], SECOND)

time: 173 us -> 172 us (level)
  local copies, waits for them, and re-layouts: 10.3 us -> 7.28 us
    unnamed x11 -> x7, local copies, waits for them, and re-layouts: 3.27 us -> 0.18 us
where the time goes in v8:
time: 172 us; the launch traced here: 171 us
  blocking collectives  55 us (32%)
  starting transfers between devices  41.5 us (24%)
  waiting for transfers between devices  31.9 us (19%)
  between operations  13.8 us (8%)
  other arithmetic  12.2 us (7%)
  matrix products  9.11 us (5%)
  local copies, waits for them, and re-layouts  7.28 us (4%)
    all_to_all x1, blocking collectives, exchanged(): lax.all_to_all(copies, ALL, 0, 0, axis_index_groups=groups, tiled=True)  30.5 us
    all_to_all x2, blocking collectives, all_ranks(): mine = lax.all_to_all(copies, 'x', 0, 0, tiled=True)  24.5 us
    ppermute x4, starting transfers between devices, partner_of(): return lax.ppermute(a, 'core', [(0, 1), (1, 0)])  17.2 us
    all_to_all x1, waiting for transfers between devices, layer(): arrived = lax.all_to_all(pair, 'x', 0, 0, tiled=True)  11.9 us
    ppermute x3, starting transfers between devices, along_x(): return lax.ppermute(a, 'x', [(i, (i + by) % 4) for i in range(4)])  9.33 us
    dot_general x1, matrix products, layer(): terms = jnp.dot(wide[:, units_part:], hidden, preferred_element_type=f32)  8.01 us
    all_to_all x1, starting transfers between devices, exchanged(): lax.all_to_all(copies, ALL, 0, 0, axis_index_groups=groups, tiled=True)  6.95 us
    ppermute x3, waiting for transfers between devices, along_x(): return lax.ppermute(a, 'x', [(i, (i + by) % 4) for i in range(4)])  6.59 us
  transfers between devices with their start and end apart: 11, of which 8 were waited for; matrix products, arithmetic and copies ran while one was open for 8% of the time, Pallas kernels for 0%

profile of v8, /device:TPU:1, one launch (start us, length us, event | category | flops | bytes accessed | tf_op | source)
XLA Modules:
  0.0 170.8 jit_solution(10501250497972736845)
XLA Ops:
  7.2 0.9 pad_maximum_fusion.4
  8.1 0.7 maximum_maximum_fusion
  9.1 30.5 %all_to_all.30 = bf16[8,32,2432]{2,1,0:T(8,128)(2,1)S(1)} all-to-all(bf16[8,32,2432]{2,1,0:T(8,128)(2,1)S(1)} %pad_maximum_fusion.1), channel_id=1, replica_groups={{0,8,16,24,32,40,48,56},{64,72,80,88,96,104,112,120},{128,136,144,152,1..., dimensions={0} | all-to-all | bytes 2490368 | tf_op jit(solution)/shard_map/all_to_all | solution.py:39
  39.6 1.1 slice.298
  40.8 1.4 broadcast_in_dim.14
  42.2 7.0 %all-to-all-start.1 = ((bf16[8,256,384]{2,1,0:T(8,128)(2,1)}), bf16[8,256,384]{2,1,0:T(8,128)(2,1)S(1)}, u32[]{:S(2)}, u32[]{:S(2)}) async-start(bf16[8,256,384]{2,1,0:T(8,128)(2,1)} %broadcast_in_dim.14), calls=%async_computation.1 | async-start | bytes 3145728 | tf_op jit(solution)/shard_map/all_to_all | solution.py:39
  49.3 4.4 %collective-permute-start = (bf16[256,384]{1,0:T(8,128)(2,1)S(1)}, bf16[256,384]{1,0:T(8,128)(2,1)S(1)}, u32[]{:S(2)}, u32[]{:S(2)}) collective-permute-start(bf16[256,384]{1,0:T(8,128)(2,1)S(1)} %bitcast.257), channel_id=1, source_target_pairs={{0,6},{2,0},{4,2},{6,4},{1,7},{3,1},{5,3},{7,5},{8,14},{10,8},{12,... | collective-permute-start | bytes 589832 | tf_op jit(solution)/shard_map/ppermute | solution.py:47
  53.7 2.4 %collective-permute-start.1 = (bf16[256,384]{1,0:T(8,128)(2,1)S(1)}, bf16[256,384]{1,0:T(8,128)(2,1)S(1)}, u32[]{:S(2)}, u32[]{:S(2)}) collective-permute-start(bf16[256,384]{1,0:T(8,128)(2,1)S(1)} %bitcast.258), channel_id=1, source_target_pairs={{0,4},{2,6},{4,0},{6,2},{1,5},{3,7},{5,1},{7,3},{8,12},{10,14},{12... | collective-permute-start | bytes 589832 | tf_op jit(solution)/shard_map/ppermute | solution.py:47
  56.1 2.5 %collective-permute-start.2 = (bf16[256,384]{1,0:T(8,128)(2,1)S(1)}, bf16[256,384]{1,0:T(8,128)(2,1)S(1)}, u32[]{:S(2)}, u32[]{:S(2)}) collective-permute-start(bf16[256,384]{1,0:T(8,128)(2,1)S(1)} %bitcast.259), channel_id=1, source_target_pairs={{0,2},{2,4},{4,6},{6,0},{1,3},{3,5},{5,7},{7,1},{8,10},{10,12},{12... | collective-permute-start | bytes 589832 | tf_op jit(solution)/shard_map/ppermute | solution.py:47
  58.7 3.2 %collective-permute-done.1 = bf16[256,384]{1,0:T(8,128)(2,1)S(1)} collective-permute-done((bf16[256,384]{1,0:T(8,128)(2,1)S(1)}, bf16[256,384]{1,0:T(8,128)(2,1)S(1)}, u32[]{:S(2)}, u32[]{:S(2)}) %collective-permute-start.1) | collective-permute-done | bytes 196640 | tf_op jit(solution)/shard_map/ppermute | solution.py:47
  61.9 3.3 %collective-permute-done.2 = bf16[256,384]{1,0:T(8,128)(2,1)S(1)} collective-permute-done((bf16[256,384]{1,0:T(8,128)(2,1)S(1)}, bf16[256,384]{1,0:T(8,128)(2,1)S(1)}, u32[]{:S(2)}, u32[]{:S(2)}) %collective-permute-start.2) | collective-permute-done | bytes 196640 | tf_op jit(solution)/shard_map/ppermute | solution.py:47
  65.3 1.0 pad_maximum_fusion.2
  66.3 5.3 %collective-permute-start.3 = (bf16[4,256,384]{2,1,0:T(8,128)(2,1)}, bf16[4,256,384]{2,1,0:T(8,128)(2,1)S(1)}, u32[]{:S(2)}, u32[]{:S(2)}) collective-permute-start(bf16[4,256,384]{2,1,0:T(8,128)(2,1)} %pad_maximum_fusion.2), channel_id=1, source_target_pairs={{0,1},{1,0},{2,3},{3,2},{4,5},{5,4},{6,7},{7,6},{8,9},{9,8},{10,11... | collective-permute-start | bytes 2359304 | tf_op jit(solution)/shard_map/ppermute | solution.py:51
  71.6 1.1 fusion.133
  72.7 1.1 fusion.103
  73.8 1.3 select_bitcast_fusion.3
  75.9 5.2 %all-to-all-done.1 = bf16[8,256,384]{2,1,0:T(8,128)(2,1)S(1)} async-done(((bf16[8,256,384]{2,1,0:T(8,128)(2,1)}), bf16[8,256,384]{2,1,0:T(8,128)(2,1)S(1)}, u32[]{:S(2)}, u32[]{:S(2)}) %all-to-all-start.1) | async-done | bytes 1572896 | tf_op jit(solution)/shard_map/all_to_all | solution.py:39
  82.6 10.1 %all_to_all.31 = bf16[4,384,128]{2,1,0:T(8,128)(2,1)S(1)} all-to-all(bf16[4,384,128]{2,1,0:T(8,128)(2,1)S(1)} %broadcast_in_dim.15), channel_id=1, replica_groups=mesh['z'=8,'y'=8,'x'=4,'core'=2] {'x'}, dimensions={0} | all-to-all | bytes 786432 | tf_op jit(solution)/shard_map/all_to_all | solution.py:60
  92.7 6.3 %collective-permute-start.4 = (bf16[4,384,128]{2,1,0:T(8,128)(2,1)S(1)}, bf16[4,384,128]{2,1,0:T(8,128)(2,1)S(1)}, u32[]{:S(2)}, u32[]{:S(2)}) collective-permute-start(bf16[4,384,128]{2,1,0:T(8,128)(2,1)S(1)} %all_to_all.31), channel_id=1, source_target_pairs={{0,1},{1,0},{2,3},{3,2},{4,5},{5,4},{6,7},{7,6},{8,9},{9,8},{10,11... | collective-permute-start | bytes 1179656 | tf_op jit(solution)/shard_map/ppermute | solution.py:51
  102.5 14.4 %all_to_all.32 = bf16[4,256,384]{2,1,0:T(8,128)(2,1)S(1)} all-to-all(bf16[4,256,384]{2,1,0:T(8,128)(2,1)S(1)} %broadcast_in_dim.16), channel_id=1, replica_groups=mesh['z'=8,'y'=8,'x'=4,'core'=2] {'x'}, dimensions={0} | all-to-all | bytes 1572864 | tf_op jit(solution)/shard_map/all_to_all | solution.py:60
  116.9 3.3 %collective-permute-start.5 = (bf16[4,256,384]{2,1,0:T(8,128)(2,1)S(1)}, bf16[4,256,384]{2,1,0:T(8,128)(2,1)S(1)}, u32[]{:S(2)}, u32[]{:S(2)}) collective-permute-start(bf16[4,256,384]{2,1,0:T(8,128)(2,1)S(1)} %all_to_all.32), channel_id=1, source_target_pairs={{0,1},{1,0},{2,3},{3,2},{4,5},{5,4},{6,7},{7,6},{8,9},{9,8},{10,11... | collective-permute-start | bytes 2359304 | tf_op jit(solution)/shard_map/ppermute | solution.py:51
  120.3 1.6 collective-permute-done.5
  123.8 8.0 %fusion.7 = bf16[2048,384]{1,0:T(8,128)(2,1)S(1)} fusion(bf16[2048,2048]{1,0:T(8,128)(2,1)} %all-gather.2.cloned.1.call-done, bf16[2048,384]{1,0:T(8,128)(2,1)S(1)} %bitcast.262), kind=kOutput, calls=%fused_computation.9 | convolution fusion | flops 3223191552 | bytes 11534336 | tf_op jit(solution)/shard_map/dot_general | solution.py:149
  132.1 2.3 %collective-permute-start.6 = (bf16[4,256,384]{2,1,0:T(8,128)(2,1)S(1)}, bf16[4,256,384]{2,1,0:T(8,128)(2,1)S(1)}, u32[]{:S(2)}, u32[]{:S(2)}) collective-permute-start(bf16[4,256,384]{2,1,0:T(8,128)(2,1)S(1)} %dynamic-slice_bitcast_fusion), channel_id=1, source_target_pairs={{0,1},{1,0},{2,3},{3,2},{4,5},{5,4},{6,7},{7,6},{8,9},{9,8},{10,11... | collective-permute-start | bytes 2359304 | tf_op jit(solution)/shard_map/ppermute | solution.py:51
  134.4 1.9 %collective-permute-done.6 = bf16[4,256,384]{2,1,0:T(8,128)(2,1)S(1)} collective-permute-done((bf16[4,256,384]{2,1,0:T(8,128)(2,1)S(1)}, bf16[4,256,384]{2,1,0:T(8,128)(2,1)S(1)}, u32[]{:S(2)}, u32[]{:S(2)}) %collective-permute-start.6) | collective-permute-done | bytes 786464 | tf_op jit(solution)/shard_map/ppermute | solution.py:51
  136.3 1.1 fusion.10
  137.3 3.5 %all-to-all-start.4 = ((bf16[4,256,384]{2,1,0:T(8,128)(2,1)}), bf16[4,256,384]{2,1,0:T(8,128)(2,1)S(1)}, u32[]{:S(2)}, u32[]{:S(2)}) async-start(bf16[4,256,384]{2,1,0:T(8,128)(2,1)} %fusion.10), calls=%async_computation.4 | async-start | bytes 1572864 | tf_op jit(solution)/shard_map/all_to_all | solution.py:155
  140.9 11.9 %all-to-all-done.4 = bf16[4,256,384]{2,1,0:T(8,128)(2,1)S(1)} async-done(((bf16[4,256,384]{2,1,0:T(8,128)(2,1)}), bf16[4,256,384]{2,1,0:T(8,128)(2,1)S(1)}, u32[]{:S(2)}, u32[]{:S(2)}) %all-to-all-start.4) | async-done | bytes 786464 | tf_op jit(solution)/shard_map/all_to_all | solution.py:155
  153.7 4.5 %all-to-all-start.5 = ((f32[8,2,384]{2,1,0:T(2,128)}), f32[8,2,384]{2,1,0:T(2,128)S(1)}, u32[]{:S(2)}, u32[]{:S(2)}) async-start(f32[8,2,384]{2,1,0:T(2,128)} %broadcast_in_dim.17), calls=%async_computation.5 | async-start | bytes 49152 | tf_op jit(solution)/shard_map/all_to_all | solution.py:161
  158.2 0.8 dynamic_slice.23
  159.0 3.9 %all-to-all-done.5 = f32[8,2,384]{2,1,0:T(2,128)S(1)} async-done(((f32[8,2,384]{2,1,0:T(2,128)}), f32[8,2,384]{2,1,0:T(2,128)S(1)}, u32[]{:S(2)}, u32[]{:S(2)}) %all-to-all-start.5) | async-done | bytes 24608 | tf_op jit(solution)/shard_map/all_to_all | solution.py:161
  163.1 0.8 copy.73
  (61 shorter events, 10.0 us)
Async XLA Ops:
  6.5 117.3 %all-gather.2.cloned.1.call-start = ((), (), s32[]{:S(2)}) async-start(), calls=%async_computation.6 | async-start | bytes 9437184 | tf_op jit(solution)/shard_map/all_gather | solution.py:113
  42.2 7.0 %copy-start = (bf16[384,256]{1,0:T(8,128)(2,1)S(1)}, bf16[384,256]{1,0:T(8,128)(2,1)}, u32[]{:S(2)}) copy-start(bf16[384,256]{1,0:T(8,128)(2,1)} %param.12) | copy-start | bytes 589828
  42.2 38.9 %all-to-all-start.1 = ((bf16[8,256,384]{2,1,0:T(8,128)(2,1)}), bf16[8,256,384]{2,1,0:T(8,128)(2,1)S(1)}, u32[]{:S(2)}, u32[]{:S(2)}) async-start(bf16[8,256,384]{2,1,0:T(8,128)(2,1)} %broadcast_in_dim.14), calls=%async_computation.1 | async-start | bytes 3145728 | tf_op jit(solution)/shard_map/all_to_all | solution.py:39
  49.3 9.4 %collective-permute-start = (bf16[256,384]{1,0:T(8,128)(2,1)S(1)}, bf16[256,384]{1,0:T(8,128)(2,1)S(1)}, u32[]{:S(2)}, u32[]{:S(2)}) collective-permute-start(bf16[256,384]{1,0:T(8,128)(2,1)S(1)} %bitcast.257), channel_id=1, source_target_pairs={{0,6},{2,0},{4,2},{6,4},{1,7},{3,1},{5,3},{7,5},{8,14},{10,8},{12,... | collective-permute-start | bytes 589832 | tf_op jit(solution)/shard_map/ppermute | solution.py:47
  53.7 8.2 %collective-permute-start.1 = (bf16[256,384]{1,0:T(8,128)(2,1)S(1)}, bf16[256,384]{1,0:T(8,128)(2,1)S(1)}, u32[]{:S(2)}, u32[]{:S(2)}) collective-permute-start(bf16[256,384]{1,0:T(8,128)(2,1)S(1)} %bitcast.258), channel_id=1, source_target_pairs={{0,4},{2,6},{4,0},{6,2},{1,5},{3,7},{5,1},{7,3},{8,12},{10,14},{12... | collective-permute-start | bytes 589832 | tf_op jit(solution)/shard_map/ppermute | solution.py:47
  56.1 9.1 %collective-permute-start.2 = (bf16[256,384]{1,0:T(8,128)(2,1)S(1)}, bf16[256,384]{1,0:T(8,128)(2,1)S(1)}, u32[]{:S(2)}, u32[]{:S(2)}) collective-permute-start(bf16[256,384]{1,0:T(8,128)(2,1)S(1)} %bitcast.259), channel_id=1, source_target_pairs={{0,2},{2,4},{4,6},{6,0},{1,3},{3,5},{5,7},{7,1},{8,10},{10,12},{12... | collective-permute-start | bytes 589832 | tf_op jit(solution)/shard_map/ppermute | solution.py:47
  66.3 7.6 %collective-permute-start.3 = (bf16[4,256,384]{2,1,0:T(8,128)(2,1)}, bf16[4,256,384]{2,1,0:T(8,128)(2,1)S(1)}, u32[]{:S(2)}, u32[]{:S(2)}) collective-permute-start(bf16[4,256,384]{2,1,0:T(8,128)(2,1)} %pad_maximum_fusion.2), channel_id=1, source_target_pairs={{0,1},{1,0},{2,3},{3,2},{4,5},{5,4},{6,7},{7,6},{8,9},{9,8},{10,11... | collective-permute-start | bytes 2359304 | tf_op jit(solution)/shard_map/ppermute | solution.py:51
  92.7 7.7 %collective-permute-start.4 = (bf16[4,384,128]{2,1,0:T(8,128)(2,1)S(1)}, bf16[4,384,128]{2,1,0:T(8,128)(2,1)S(1)}, u32[]{:S(2)}, u32[]{:S(2)}) collective-permute-start(bf16[4,384,128]{2,1,0:T(8,128)(2,1)S(1)} %all_to_all.31), channel_id=1, source_target_pairs={{0,1},{1,0},{2,3},{3,2},{4,5},{5,4},{6,7},{7,6},{8,9},{9,8},{10,11... | collective-permute-start | bytes 1179656 | tf_op jit(solution)/shard_map/ppermute | solution.py:51
  99.7 1.2 copy-start.2
  102.4 17.9 %copy-start.1 = (f32[2048]{0:T(1024)S(1)}, f32[2048]{0:T(1024)}, u32[]{:S(2)}) copy-start(f32[2048]{0:T(1024)} %param.18) | copy-start | bytes 24580
  116.9 5.0 %collective-permute-start.5 = (bf16[4,256,384]{2,1,0:T(8,128)(2,1)S(1)}, bf16[4,256,384]{2,1,0:T(8,128)(2,1)S(1)}, u32[]{:S(2)}, u32[]{:S(2)}) collective-permute-start(bf16[4,256,384]{2,1,0:T(8,128)(2,1)S(1)} %all_to_all.32), channel_id=1, source_target_pairs={{0,1},{1,0},{2,3},{3,2},{4,5},{5,4},{6,7},{7,6},{8,9},{9,8},{10,11... | collective-permute-start | bytes 2359304 | tf_op jit(solution)/shard_map/ppermute | solution.py:51
  132.1 4.2 %collective-permute-start.6 = (bf16[4,256,384]{2,1,0:T(8,128)(2,1)S(1)}, bf16[4,256,384]{2,1,0:T(8,128)(2,1)S(1)}, u32[]{:S(2)}, u32[]{:S(2)}) collective-permute-start(bf16[4,256,384]{2,1,0:T(8,128)(2,1)S(1)} %dynamic-slice_bitcast_fusion), channel_id=1, source_target_pairs={{0,1},{1,0},{2,3},{3,2},{4,5},{5,4},{6,7},{7,6},{8,9},{9,8},{10,11... | collective-permute-start | bytes 2359304 | tf_op jit(solution)/shard_map/ppermute | solution.py:51
  137.3 15.5 %all-to-all-start.4 = ((bf16[4,256,384]{2,1,0:T(8,128)(2,1)}), bf16[4,256,384]{2,1,0:T(8,128)(2,1)S(1)}, u32[]{:S(2)}, u32[]{:S(2)}) async-start(bf16[4,256,384]{2,1,0:T(8,128)(2,1)} %fusion.10), calls=%async_computation.4 | async-start | bytes 1572864 | tf_op jit(solution)/shard_map/all_to_all | solution.py:155
  153.7 9.2 %all-to-all-start.5 = ((f32[8,2,384]{2,1,0:T(2,128)}), f32[8,2,384]{2,1,0:T(2,128)S(1)}, u32[]{:S(2)}, u32[]{:S(2)}) async-start(f32[8,2,384]{2,1,0:T(2,128)} %broadcast_in_dim.17), calls=%async_computation.5 | async-start | bytes 49152 | tf_op jit(solution)/shard_map/all_to_all | solution.py:161
Sparse Core Ops, SparseCore 0:
  40.9 68.9 all-gather.1

commit v9 on v8

--- a/solution.py
+++ b/solution.py
@@ -103,14 +103,14 @@
     own_xt = tokens.T
     mix_rows = w_mix_out.shape[0]
     halves = [w_mix_out[:, :channel_part], w_mix_out[:, channel_part:]]
-    wide = jnp.concatenate([w_up, w_down.T], 1)
-    small = jnp.concatenate([w_value, w_gate, jnp.concatenate(halves, 0)], 1)
-    wide, small = lax.optimization_barrier((wide, small))
+    wide = jnp.concatenate([w_up, w_down.T, w_value, w_gate], 1)
+    wide, small = lax.optimization_barrier((wide, jnp.concatenate(halves, 0)))
     copies = [jnp.broadcast_to(a, (SIDE, *a.shape)) for a in (wide, small)]
     shard = exchanged(jnp.concatenate(copies, 2), FIRST)
     shard = shard.reshape(-1, shard.shape[2])
     at = 2 * units_part
-    wide = lax.all_gather(shard[:, :at], ALL, axis=0, tiled=True, axis_index_groups=SECOND)
+    wide = shard[:, :at]
+    wide = lax.all_gather(wide, ALL, axis=0, tiled=True, axis_index_groups=SECOND)
     small = sent_to_group(shard[:, at:], SECOND)
     value_gate = small[:, :, : 2 * channel_part].reshape(WIDTH, 2 * channel_part)
     mix = small[:, :, 2 * channel_part :].reshape(SIDE, SIDE, 2, mix_rows, channel_part)
@@ -123,6 +123,7 @@
     mine, other = jnp.roll(mine, x_rank, 0), jnp.roll(other, x_rank, 0)
     ranks = jnp.stack([jnp.where(core == 0, mine, other), jnp.where(core == 0, other, mine)], 1)
     ranks = turned(core, ranks.reshape(SIDE, SIDE, -1, frames)).reshape(WIDTH, frames)
+    shift = residual_scale * jnp.mean(ranks.astype(f32), 0)
 
     both = lax.dot_general(ranks, value_gate, (((0,), (0,)), ((), ())), preferred_element_type=f32)
     values_proj, gate_proj = both[:, :channel_part], both[:, channel_part:]
@@ -133,7 +134,7 @@
     activated = jax.nn.silu((filtered_whole - average) * scale * conv_gain).astype(bf16)
 
     mixed = jnp.dot(activated, mix, preferred_element_type=f32)
-    combined = residual_scale * tokens.astype(f32) + mixed
+    combined = residual_scale * tokens.astype(f32) + mixed - shift[:, None]
     combined_whole = all_ranks(combined.astype(bf16).T, core).reshape(WIDTH, frames).astype(f32)
     average = jnp.sum(combined_whole, 0) / WIDTH
     spread = jnp.maximum(jnp.sum(combined_whole * combined_whole, 0) / WIDTH - average * average, 0.0)

time: 172 us -> 171 us (level)
  no operation moved by 1% of the time
where the time goes in v9:
time: 171 us; the launch traced here: 170 us
  blocking collectives  55 us (32%)
  starting transfers between devices  41.5 us (24%)
  waiting for transfers between devices  31.2 us (18%)
  between operations  13.8 us (8%)
  other arithmetic  12.1 us (7%)
  matrix products  9.11 us (5%)
  local copies, waits for them, and re-layouts  7.25 us (4%)
    all_to_all x1, blocking collectives, exchanged(): lax.all_to_all(copies, ALL, 0, 0, axis_index_groups=groups, tiled=True)  30.5 us
    all_to_all x2, blocking collectives, all_ranks(): mine = lax.all_to_all(copies, 'x', 0, 0, tiled=True)  24.5 us
    ppermute x4, starting transfers between devices, partner_of(): return lax.ppermute(a, 'core', [(0, 1), (1, 0)])  17.2 us
    all_to_all x1, waiting for transfers between devices, layer(): arrived = lax.all_to_all(pair, 'x', 0, 0, tiled=True)  11.9 us
    ppermute x3, starting transfers between devices, along_x(): return lax.ppermute(a, 'x', [(i, (i + by) % 4) for i in range(4)])  9.33 us
    dot_general x1, matrix products, layer(): terms = jnp.dot(wide[:, units_part:], hidden, preferred_element_type=f32)  8.01 us
    all_to_all x1, starting transfers between devices, exchanged(): lax.all_to_all(copies, ALL, 0, 0, axis_index_groups=groups, tiled=True)  6.95 us
    ppermute x3, waiting for transfers between devices, along_x(): return lax.ppermute(a, 'x', [(i, (i + by) % 4) for i in range(4)])  6.59 us
  transfers between devices with their start and end apart: 11, of which 8 were waited for; matrix products, arithmetic and copies ran while one was open for 8% of the time, Pallas kernels for 0%

profile of v9, /device:TPU:1, one launch (start us, length us, event | category | flops | bytes accessed | tf_op | source)
XLA Modules:
  0.0 170.0 jit_solution(9771013386393066988)
XLA Ops:
  7.2 0.9 pad_maximum_fusion.4
  8.4 30.5 %all_to_all.30 = bf16[8,32,2432]{2,1,0:T(8,128)(2,1)S(1)} all-to-all(bf16[8,32,2432]{2,1,0:T(8,128)(2,1)S(1)} %pad_maximum_fusion.1), channel_id=1, replica_groups={{0,8,16,24,32,40,48,56},{64,72,80,88,96,104,112,120},{128,136,144,152,1..., dimensions={0} | all-to-all | bytes 2490368 | tf_op jit(solution)/shard_map/all_to_all | solution.py:39
  38.9 1.1 slice.298
  40.1 1.4 broadcast_in_dim.14
  41.5 7.0 %all-to-all-start.1 = ((bf16[8,256,384]{2,1,0:T(8,128)(2,1)}), bf16[8,256,384]{2,1,0:T(8,128)(2,1)S(1)}, u32[]{:S(2)}, u32[]{:S(2)}) async-start(bf16[8,256,384]{2,1,0:T(8,128)(2,1)} %broadcast_in_dim.14), calls=%async_computation.1 | async-start | bytes 3145728 | tf_op jit(solution)/shard_map/all_to_all | solution.py:39
  48.6 4.4 %collective-permute-start = (bf16[256,384]{1,0:T(8,128)(2,1)S(1)}, bf16[256,384]{1,0:T(8,128)(2,1)S(1)}, u32[]{:S(2)}, u32[]{:S(2)}) collective-permute-start(bf16[256,384]{1,0:T(8,128)(2,1)S(1)} %bitcast.258), channel_id=1, source_target_pairs={{0,6},{2,0},{4,2},{6,4},{1,7},{3,1},{5,3},{7,5},{8,14},{10,8},{12,... | collective-permute-start | bytes 589832 | tf_op jit(solution)/shard_map/ppermute | solution.py:47
  53.0 2.4 %collective-permute-start.1 = (bf16[256,384]{1,0:T(8,128)(2,1)S(1)}, bf16[256,384]{1,0:T(8,128)(2,1)S(1)}, u32[]{:S(2)}, u32[]{:S(2)}) collective-permute-start(bf16[256,384]{1,0:T(8,128)(2,1)S(1)} %bitcast.259), channel_id=1, source_target_pairs={{0,4},{2,6},{4,0},{6,2},{1,5},{3,7},{5,1},{7,3},{8,12},{10,14},{12... | collective-permute-start | bytes 589832 | tf_op jit(solution)/shard_map/ppermute | solution.py:47
  55.4 2.5 %collective-permute-start.2 = (bf16[256,384]{1,0:T(8,128)(2,1)S(1)}, bf16[256,384]{1,0:T(8,128)(2,1)S(1)}, u32[]{:S(2)}, u32[]{:S(2)}) collective-permute-start(bf16[256,384]{1,0:T(8,128)(2,1)S(1)} %bitcast.260), channel_id=1, source_target_pairs={{0,2},{2,4},{4,6},{6,0},{1,3},{3,5},{5,7},{7,1},{8,10},{10,12},{12... | collective-permute-start | bytes 589832 | tf_op jit(solution)/shard_map/ppermute | solution.py:47
  57.9 3.2 %collective-permute-done.1 = bf16[256,384]{1,0:T(8,128)(2,1)S(1)} collective-permute-done((bf16[256,384]{1,0:T(8,128)(2,1)S(1)}, bf16[256,384]{1,0:T(8,128)(2,1)S(1)}, u32[]{:S(2)}, u32[]{:S(2)}) %collective-permute-start.1) | collective-permute-done | bytes 196640 | tf_op jit(solution)/shard_map/ppermute | solution.py:47
  61.2 3.3 %collective-permute-done.2 = bf16[256,384]{1,0:T(8,128)(2,1)S(1)} collective-permute-done((bf16[256,384]{1,0:T(8,128)(2,1)S(1)}, bf16[256,384]{1,0:T(8,128)(2,1)S(1)}, u32[]{:S(2)}, u32[]{:S(2)}) %collective-permute-start.2) | collective-permute-done | bytes 196640 | tf_op jit(solution)/shard_map/ppermute | solution.py:47
  64.5 1.0 pad_maximum_fusion.2
  65.6 5.3 %collective-permute-start.3 = (bf16[4,256,384]{2,1,0:T(8,128)(2,1)}, bf16[4,256,384]{2,1,0:T(8,128)(2,1)S(1)}, u32[]{:S(2)}, u32[]{:S(2)}) collective-permute-start(bf16[4,256,384]{2,1,0:T(8,128)(2,1)} %pad_maximum_fusion.2), channel_id=1, source_target_pairs={{0,1},{1,0},{2,3},{3,2},{4,5},{5,4},{6,7},{7,6},{8,9},{9,8},{10,11... | collective-permute-start | bytes 2359304 | tf_op jit(solution)/shard_map/ppermute | solution.py:51
  70.9 1.1 fusion.134
  72.0 1.1 fusion.104
  73.1 1.3 select_bitcast_fusion.3
  75.0 0.8 convert_reduce_fusion
  75.9 4.5 %all-to-all-done.1 = bf16[8,256,384]{2,1,0:T(8,128)(2,1)S(1)} async-done(((bf16[8,256,384]{2,1,0:T(8,128)(2,1)}), bf16[8,256,384]{2,1,0:T(8,128)(2,1)S(1)}, u32[]{:S(2)}, u32[]{:S(2)}) %all-to-all-start.1) | async-done | bytes 1572896 | tf_op jit(solution)/shard_map/all_to_all | solution.py:39
  81.9 10.1 %all_to_all.31 = bf16[4,384,128]{2,1,0:T(8,128)(2,1)S(1)} all-to-all(bf16[4,384,128]{2,1,0:T(8,128)(2,1)S(1)} %broadcast_in_dim.15), channel_id=1, replica_groups=mesh['z'=8,'y'=8,'x'=4,'core'=2] {'x'}, dimensions={0} | all-to-all | bytes 786432 | tf_op jit(solution)/shard_map/all_to_all | solution.py:60
  92.0 6.3 %collective-permute-start.4 = (bf16[4,384,128]{2,1,0:T(8,128)(2,1)S(1)}, bf16[4,384,128]{2,1,0:T(8,128)(2,1)S(1)}, u32[]{:S(2)}, u32[]{:S(2)}) collective-permute-start(bf16[4,384,128]{2,1,0:T(8,128)(2,1)S(1)} %all_to_all.31), channel_id=1, source_target_pairs={{0,1},{1,0},{2,3},{3,2},{4,5},{5,4},{6,7},{7,6},{8,9},{9,8},{10,11... | collective-permute-start | bytes 1179656 | tf_op jit(solution)/shard_map/ppermute | solution.py:51
  101.8 14.4 %all_to_all.32 = bf16[4,256,384]{2,1,0:T(8,128)(2,1)S(1)} all-to-all(bf16[4,256,384]{2,1,0:T(8,128)(2,1)S(1)} %broadcast_in_dim.16), channel_id=1, replica_groups=mesh['z'=8,'y'=8,'x'=4,'core'=2] {'x'}, dimensions={0} | all-to-all | bytes 1572864 | tf_op jit(solution)/shard_map/all_to_all | solution.py:60
  116.2 3.3 %collective-permute-start.5 = (bf16[4,256,384]{2,1,0:T(8,128)(2,1)S(1)}, bf16[4,256,384]{2,1,0:T(8,128)(2,1)S(1)}, u32[]{:S(2)}, u32[]{:S(2)}) collective-permute-start(bf16[4,256,384]{2,1,0:T(8,128)(2,1)S(1)} %all_to_all.32), channel_id=1, source_target_pairs={{0,1},{1,0},{2,3},{3,2},{4,5},{5,4},{6,7},{7,6},{8,9},{9,8},{10,11... | collective-permute-start | bytes 2359304 | tf_op jit(solution)/shard_map/ppermute | solution.py:51
  119.6 1.6 collective-permute-done.5
  123.1 8.0 %fusion.7 = bf16[2048,384]{1,0:T(8,128)(2,1)S(1)} fusion(bf16[2048,2048]{1,0:T(8,128)(2,1)} %all-gather.2.cloned.1.call-done, bf16[2048,384]{1,0:T(8,128)(2,1)S(1)} %bitcast.263), kind=kOutput, calls=%fused_computation.10 | convolution fusion | flops 3223191552 | bytes 11534336 | tf_op jit(solution)/shard_map/dot_general | solution.py:150
  131.4 2.3 %collective-permute-start.6 = (bf16[4,256,384]{2,1,0:T(8,128)(2,1)S(1)}, bf16[4,256,384]{2,1,0:T(8,128)(2,1)S(1)}, u32[]{:S(2)}, u32[]{:S(2)}) collective-permute-start(bf16[4,256,384]{2,1,0:T(8,128)(2,1)S(1)} %dynamic-slice_bitcast_fusion), channel_id=1, source_target_pairs={{0,1},{1,0},{2,3},{3,2},{4,5},{5,4},{6,7},{7,6},{8,9},{9,8},{10,11... | collective-permute-start | bytes 2359304 | tf_op jit(solution)/shard_map/ppermute | solution.py:51
  133.7 1.9 %collective-permute-done.6 = bf16[4,256,384]{2,1,0:T(8,128)(2,1)S(1)} collective-permute-done((bf16[4,256,384]{2,1,0:T(8,128)(2,1)S(1)}, bf16[4,256,384]{2,1,0:T(8,128)(2,1)S(1)}, u32[]{:S(2)}, u32[]{:S(2)}) %collective-permute-start.6) | collective-permute-done | bytes 786464 | tf_op jit(solution)/shard_map/ppermute | solution.py:51
  135.6 1.1 fusion.10
  136.6 3.5 %all-to-all-start.4 = ((bf16[4,256,384]{2,1,0:T(8,128)(2,1)}), bf16[4,256,384]{2,1,0:T(8,128)(2,1)S(1)}, u32[]{:S(2)}, u32[]{:S(2)}) async-start(bf16[4,256,384]{2,1,0:T(8,128)(2,1)} %fusion.10), calls=%async_computation.4 | async-start | bytes 1572864 | tf_op jit(solution)/shard_map/all_to_all | solution.py:156
  140.2 11.9 %all-to-all-done.4 = bf16[4,256,384]{2,1,0:T(8,128)(2,1)S(1)} async-done(((bf16[4,256,384]{2,1,0:T(8,128)(2,1)}), bf16[4,256,384]{2,1,0:T(8,128)(2,1)S(1)}, u32[]{:S(2)}, u32[]{:S(2)}) %all-to-all-start.4) | async-done | bytes 786464 | tf_op jit(solution)/shard_map/all_to_all | solution.py:156
  153.0 4.5 %all-to-all-start.5 = ((f32[8,2,384]{2,1,0:T(2,128)}), f32[8,2,384]{2,1,0:T(2,128)S(1)}, u32[]{:S(2)}, u32[]{:S(2)}) async-start(f32[8,2,384]{2,1,0:T(2,128)} %broadcast_in_dim.17), calls=%async_computation.5 | async-start | bytes 49152 | tf_op jit(solution)/shard_map/all_to_all | solution.py:162
  157.5 0.8 dynamic_slice.23
  158.3 3.9 %all-to-all-done.5 = f32[8,2,384]{2,1,0:T(2,128)S(1)} async-done(((f32[8,2,384]{2,1,0:T(2,128)}), f32[8,2,384]{2,1,0:T(2,128)S(1)}, u32[]{:S(2)}, u32[]{:S(2)}) %all-to-all-start.5) | async-done | bytes 24608 | tf_op jit(solution)/shard_map/all_to_all | solution.py:162
  162.4 0.8 copy.73
  (62 shorter events, 9.8 us)
Async XLA Ops:
  6.5 116.5 %all-gather.2.cloned.1.call-start = ((), (), s32[]{:S(2)}) async-start(), calls=%async_computation.6 | async-start | bytes 9437184 | tf_op jit(solution)/shard_map/all_gather | solution.py:113
  41.5 7.0 %copy-start = (bf16[384,256]{1,0:T(8,128)(2,1)S(1)}, bf16[384,256]{1,0:T(8,128)(2,1)}, u32[]{:S(2)}) copy-start(bf16[384,256]{1,0:T(8,128)(2,1)} %param.12) | copy-start | bytes 589828
  41.5 38.9 %all-to-all-start.1 = ((bf16[8,256,384]{2,1,0:T(8,128)(2,1)}), bf16[8,256,384]{2,1,0:T(8,128)(2,1)S(1)}, u32[]{:S(2)}, u32[]{:S(2)}) async-start(bf16[8,256,384]{2,1,0:T(8,128)(2,1)} %broadcast_in_dim.14), calls=%async_computation.1 | async-start | bytes 3145728 | tf_op jit(solution)/shard_map/all_to_all | solution.py:39
  48.6 9.4 %collective-permute-start = (bf16[256,384]{1,0:T(8,128)(2,1)S(1)}, bf16[256,384]{1,0:T(8,128)(2,1)S(1)}, u32[]{:S(2)}, u32[]{:S(2)}) collective-permute-start(bf16[256,384]{1,0:T(8,128)(2,1)S(1)} %bitcast.258), channel_id=1, source_target_pairs={{0,6},{2,0},{4,2},{6,4},{1,7},{3,1},{5,3},{7,5},{8,14},{10,8},{12,... | collective-permute-start | bytes 589832 | tf_op jit(solution)/shard_map/ppermute | solution.py:47
  53.0 8.2 %collective-permute-start.1 = (bf16[256,384]{1,0:T(8,128)(2,1)S(1)}, bf16[256,384]{1,0:T(8,128)(2,1)S(1)}, u32[]{:S(2)}, u32[]{:S(2)}) collective-permute-start(bf16[256,384]{1,0:T(8,128)(2,1)S(1)} %bitcast.259), channel_id=1, source_target_pairs={{0,4},{2,6},{4,0},{6,2},{1,5},{3,7},{5,1},{7,3},{8,12},{10,14},{12... | collective-permute-start | bytes 589832 | tf_op jit(solution)/shard_map/ppermute | solution.py:47
  55.4 9.1 %collective-permute-start.2 = (bf16[256,384]{1,0:T(8,128)(2,1)S(1)}, bf16[256,384]{1,0:T(8,128)(2,1)S(1)}, u32[]{:S(2)}, u32[]{:S(2)}) collective-permute-start(bf16[256,384]{1,0:T(8,128)(2,1)S(1)} %bitcast.260), channel_id=1, source_target_pairs={{0,2},{2,4},{4,6},{6,0},{1,3},{3,5},{5,7},{7,1},{8,10},{10,12},{12... | collective-permute-start | bytes 589832 | tf_op jit(solution)/shard_map/ppermute | solution.py:47
  65.6 7.6 %collective-permute-start.3 = (bf16[4,256,384]{2,1,0:T(8,128)(2,1)}, bf16[4,256,384]{2,1,0:T(8,128)(2,1)S(1)}, u32[]{:S(2)}, u32[]{:S(2)}) collective-permute-start(bf16[4,256,384]{2,1,0:T(8,128)(2,1)} %pad_maximum_fusion.2), channel_id=1, source_target_pairs={{0,1},{1,0},{2,3},{3,2},{4,5},{5,4},{6,7},{7,6},{8,9},{9,8},{10,11... | collective-permute-start | bytes 2359304 | tf_op jit(solution)/shard_map/ppermute | solution.py:51
  92.0 7.7 %collective-permute-start.4 = (bf16[4,384,128]{2,1,0:T(8,128)(2,1)S(1)}, bf16[4,384,128]{2,1,0:T(8,128)(2,1)S(1)}, u32[]{:S(2)}, u32[]{:S(2)}) collective-permute-start(bf16[4,384,128]{2,1,0:T(8,128)(2,1)S(1)} %all_to_all.31), channel_id=1, source_target_pairs={{0,1},{1,0},{2,3},{3,2},{4,5},{5,4},{6,7},{7,6},{8,9},{9,8},{10,11... | collective-permute-start | bytes 1179656 | tf_op jit(solution)/shard_map/ppermute | solution.py:51
  99.0 1.2 copy-start.2
  101.7 17.9 %copy-start.1 = (f32[2048]{0:T(1024)S(1)}, f32[2048]{0:T(1024)}, u32[]{:S(2)}) copy-start(f32[2048]{0:T(1024)} %param.18) | copy-start | bytes 24580
  116.2 5.0 %collective-permute-start.5 = (bf16[4,256,384]{2,1,0:T(8,128)(2,1)S(1)}, bf16[4,256,384]{2,1,0:T(8,128)(2,1)S(1)}, u32[]{:S(2)}, u32[]{:S(2)}) collective-permute-start(bf16[4,256,384]{2,1,0:T(8,128)(2,1)S(1)} %all_to_all.32), channel_id=1, source_target_pairs={{0,1},{1,0},{2,3},{3,2},{4,5},{5,4},{6,7},{7,6},{8,9},{9,8},{10,11... | collective-permute-start | bytes 2359304 | tf_op jit(solution)/shard_map/ppermute | solution.py:51
  131.4 4.2 %collective-permute-start.6 = (bf16[4,256,384]{2,1,0:T(8,128)(2,1)S(1)}, bf16[4,256,384]{2,1,0:T(8,128)(2,1)S(1)}, u32[]{:S(2)}, u32[]{:S(2)}) collective-permute-start(bf16[4,256,384]{2,1,0:T(8,128)(2,1)S(1)} %dynamic-slice_bitcast_fusion), channel_id=1, source_target_pairs={{0,1},{1,0},{2,3},{3,2},{4,5},{5,4},{6,7},{7,6},{8,9},{9,8},{10,11... | collective-permute-start | bytes 2359304 | tf_op jit(solution)/shard_map/ppermute | solution.py:51
  136.6 15.5 %all-to-all-start.4 = ((bf16[4,256,384]{2,1,0:T(8,128)(2,1)}), bf16[4,256,384]{2,1,0:T(8,128)(2,1)S(1)}, u32[]{:S(2)}, u32[]{:S(2)}) async-start(bf16[4,256,384]{2,1,0:T(8,128)(2,1)} %fusion.10), calls=%async_computation.4 | async-start | bytes 1572864 | tf_op jit(solution)/shard_map/all_to_all | solution.py:156
  153.0 9.2 %all-to-all-start.5 = ((f32[8,2,384]{2,1,0:T(2,128)}), f32[8,2,384]{2,1,0:T(2,128)S(1)}, u32[]{:S(2)}, u32[]{:S(2)}) async-start(f32[8,2,384]{2,1,0:T(2,128)} %broadcast_in_dim.17), calls=%async_computation.5 | async-start | bytes 49152 | tf_op jit(solution)/shard_map/all_to_all | solution.py:162
Sparse Core Ops, SparseCore 0:
  40.2 68.9 all-gather.1

commit v10 on v9

--- a/solution.py
+++ b/solution.py
@@ -61,6 +61,11 @@
     other = partner_of(mine)
     both = jnp.stack([jnp.where(core == 0, mine, other), jnp.where(core == 0, other, mine)], 1)
     return both.reshape(SIDE, *shard.shape)
+
+
+def all_at_once(shard):
+    copies = jnp.broadcast_to(shard, (SIDE, *shard.shape))
+    return lax.all_to_all(copies, TP, 0, 0, tiled=True)
 
 
 def joined_columns(parts):
@@ -129,7 +134,7 @@
     values_proj, gate_proj = both[:, :channel_part], both[:, channel_part:]
     gated = (values_proj * jax.nn.sigmoid(gate_proj)).astype(bf16)
     filtered = causal_filter(gated, mine_of(conv_kernel, channel_part))
-    filtered_whole = joined_columns(all_ranks(filtered.astype(bf16), core)).astype(f32)
+    filtered_whole = joined_columns(all_at_once(filtered.astype(bf16))).astype(f32)
     average, scale = row_norm_terms(filtered_whole, CHANNELS)
     activated = jax.nn.silu((filtered_whole - average) * scale * conv_gain).astype(bf16)
 

time: 171 us -> 173 us (1.012)
  waiting for transfers between devices: 31.2 us -> 42.1 us
  blocking collectives: 55 us -> 44.3 us
    all_to_all x0 -> x1, waiting for transfers between devices: none -> 11.5 us  [all_at_once(): return lax.all_to_all(copies, TP, 0, 0, tiled=True)]
    all_to_all x2 -> x1, blocking collectives: 24.5 us -> 13.8 us  [all_ranks(): mine = lax.all_to_all(copies, 'x', 0, 0, tiled=True)]
    all_to_all x0 -> x1, starting transfers between devices: none -> 7.36 us  [all_at_once(): return lax.all_to_all(copies, TP, 0, 0, tiled=True)]
    ppermute x4 -> x3, starting transfers between devices: 17.2 us -> 11.5 us  [partner_of(): return lax.ppermute(a, 'core', [(0, 1), (1, 0)])]
    ppermute x4 -> x3, waiting for transfers between devices: 4.19 us -> 3.51 us  [partner_of(): return lax.ppermute(a, 'core', [(0, 1), (1, 0)])]
  transfers between devices with their start and end apart: 11 -> 11, of which waited for: 8 -> 8; matrix products, arithmetic and copies ran while one was open for 8% -> 9% of each run, Pallas kernels for 0% -> 0%
where the time goes in v10:
time: 173 us; the launch traced here: 172 us
  blocking collectives  44.3 us (26%)
  starting transfers between devices  43.1 us (25%)
  waiting for transfers between devices  42.1 us (24%)
  between operations  13.8 us (8%)
  other arithmetic  11.9 us (7%)
  matrix products  9.11 us (5%)
  local copies, waits for them, and re-layouts  7.97 us (5%)
    all_to_all x1, blocking collectives, exchanged(): lax.all_to_all(copies, ALL, 0, 0, axis_index_groups=groups, tiled=True)  30.5 us
    all_to_all x1, blocking collectives, all_ranks(): mine = lax.all_to_all(copies, 'x', 0, 0, tiled=True)  13.8 us
    all_to_all x1, waiting for transfers between devices, layer(): arrived = lax.all_to_all(pair, 'x', 0, 0, tiled=True)  11.9 us
    all_to_all x1, waiting for transfers between devices, all_at_once(): return lax.all_to_all(copies, TP, 0, 0, tiled=True)  11.5 us
    ppermute x3, starting transfers between devices, partner_of(): return lax.ppermute(a, 'core', [(0, 1), (1, 0)])  11.5 us
    ppermute x3, starting transfers between devices, along_x(): return lax.ppermute(a, 'x', [(i, (i + by) % 4) for i in range(4)])  9.33 us
    dot_general x1, matrix products, layer(): terms = jnp.dot(wide[:, units_part:], hidden, preferred_element_type=f32)  8.01 us
    all_to_all x1, starting transfers between devices, all_at_once(): return lax.all_to_all(copies, TP, 0, 0, tiled=True)  7.36 us
  transfers between devices with their start and end apart: 11, of which 8 were waited for; matrix products, arithmetic and copies ran while one was open for 9% of the time, Pallas kernels for 0%

profile of v10, /device:TPU:1, one launch (start us, length us, event | category | flops | bytes accessed | tf_op | source)
XLA Modules:
  0.0 172.2 jit_solution(13323159668427317925)
XLA Ops:
  7.2 0.9 pad_maximum_fusion.3
  8.4 30.5 %all_to_all.30 = bf16[8,32,2432]{2,1,0:T(8,128)(2,1)S(1)} all-to-all(bf16[8,32,2432]{2,1,0:T(8,128)(2,1)S(1)} %pad_maximum_fusion.1), channel_id=1, replica_groups={{0,8,16,24,32,40,48,56},{64,72,80,88,96,104,112,120},{128,136,144,152,1..., dimensions={0} | all-to-all | bytes 2490368 | tf_op jit(solution)/shard_map/all_to_all | solution.py:39
  38.9 1.1 slice.298
  40.1 1.4 broadcast_in_dim.14
  41.5 7.0 %all-to-all-start.1 = ((bf16[8,256,384]{2,1,0:T(8,128)(2,1)}), bf16[8,256,384]{2,1,0:T(8,128)(2,1)S(1)}, u32[]{:S(2)}, u32[]{:S(2)}) async-start(bf16[8,256,384]{2,1,0:T(8,128)(2,1)} %broadcast_in_dim.14), calls=%async_computation.1 | async-start | bytes 3145728 | tf_op jit(solution)/shard_map/all_to_all | solution.py:39
  48.6 4.4 %collective-permute-start = (bf16[256,384]{1,0:T(8,128)(2,1)S(1)}, bf16[256,384]{1,0:T(8,128)(2,1)S(1)}, u32[]{:S(2)}, u32[]{:S(2)}) collective-permute-start(bf16[256,384]{1,0:T(8,128)(2,1)S(1)} %bitcast.242), channel_id=1, source_target_pairs={{0,6},{2,0},{4,2},{6,4},{1,7},{3,1},{5,3},{7,5},{8,14},{10,8},{12,... | collective-permute-start | bytes 589832 | tf_op jit(solution)/shard_map/ppermute | solution.py:47
  53.0 2.4 %collective-permute-start.1 = (bf16[256,384]{1,0:T(8,128)(2,1)S(1)}, bf16[256,384]{1,0:T(8,128)(2,1)S(1)}, u32[]{:S(2)}, u32[]{:S(2)}) collective-permute-start(bf16[256,384]{1,0:T(8,128)(2,1)S(1)} %bitcast.243), channel_id=1, source_target_pairs={{0,4},{2,6},{4,0},{6,2},{1,5},{3,7},{5,1},{7,3},{8,12},{10,14},{12... | collective-permute-start | bytes 589832 | tf_op jit(solution)/shard_map/ppermute | solution.py:47
  55.4 2.5 %collective-permute-start.2 = (bf16[256,384]{1,0:T(8,128)(2,1)S(1)}, bf16[256,384]{1,0:T(8,128)(2,1)S(1)}, u32[]{:S(2)}, u32[]{:S(2)}) collective-permute-start(bf16[256,384]{1,0:T(8,128)(2,1)S(1)} %bitcast.244), channel_id=1, source_target_pairs={{0,2},{2,4},{4,6},{6,0},{1,3},{3,5},{5,7},{7,1},{8,10},{10,12},{12... | collective-permute-start | bytes 589832 | tf_op jit(solution)/shard_map/ppermute | solution.py:47
  57.9 3.2 %collective-permute-done.1 = bf16[256,384]{1,0:T(8,128)(2,1)S(1)} collective-permute-done((bf16[256,384]{1,0:T(8,128)(2,1)S(1)}, bf16[256,384]{1,0:T(8,128)(2,1)S(1)}, u32[]{:S(2)}, u32[]{:S(2)}) %collective-permute-start.1) | collective-permute-done | bytes 196640 | tf_op jit(solution)/shard_map/ppermute | solution.py:47
  61.2 3.3 %collective-permute-done.2 = bf16[256,384]{1,0:T(8,128)(2,1)S(1)} collective-permute-done((bf16[256,384]{1,0:T(8,128)(2,1)S(1)}, bf16[256,384]{1,0:T(8,128)(2,1)S(1)}, u32[]{:S(2)}, u32[]{:S(2)}) %collective-permute-start.2) | collective-permute-done | bytes 196640 | tf_op jit(solution)/shard_map/ppermute | solution.py:47
  64.5 1.0 pad_maximum_fusion.2
  65.6 5.3 %collective-permute-start.3 = (bf16[4,256,384]{2,1,0:T(8,128)(2,1)}, bf16[4,256,384]{2,1,0:T(8,128)(2,1)S(1)}, u32[]{:S(2)}, u32[]{:S(2)}) collective-permute-start(bf16[4,256,384]{2,1,0:T(8,128)(2,1)} %pad_maximum_fusion.2), channel_id=1, source_target_pairs={{0,1},{1,0},{2,3},{3,2},{4,5},{5,4},{6,7},{7,6},{8,9},{9,8},{10,11... | collective-permute-start | bytes 2359304 | tf_op jit(solution)/shard_map/ppermute | solution.py:51
  70.9 1.1 fusion.137
  72.0 1.1 fusion.107
  73.1 1.3 select_bitcast_fusion.3
  75.0 0.8 convert_reduce_fusion
  75.9 4.5 %all-to-all-done.1 = bf16[8,256,384]{2,1,0:T(8,128)(2,1)S(1)} async-done(((bf16[8,256,384]{2,1,0:T(8,128)(2,1)}), bf16[8,256,384]{2,1,0:T(8,128)(2,1)S(1)}, u32[]{:S(2)}, u32[]{:S(2)}) %all-to-all-start.1) | async-done | bytes 1572896 | tf_op jit(solution)/shard_map/all_to_all | solution.py:39
  82.0 1.0 broadcast_in_dim.15
  83.0 7.4 %all-to-all-start.2 = ((bf16[8,384,128]{1,2,0:T(8,128)(2,1)}), bf16[8,384,128]{1,2,0:T(8,128)(2,1)S(1)}, u32[]{:S(2)}, u32[]{:S(2)}) async-start(bf16[8,384,128]{1,2,0:T(8,128)(2,1)} %broadcast_in_dim.15), calls=%async_computation.2 | async-start | bytes 1572864 | tf_op jit(solution)/shard_map/all_to_all | solution.py:68
  91.0 11.5 %all-to-all-done.2 = bf16[8,384,128]{1,2,0:T(8,128)(2,1)S(1)} async-done(((bf16[8,384,128]{1,2,0:T(8,128)(2,1)}), bf16[8,384,128]{1,2,0:T(8,128)(2,1)S(1)}, u32[]{:S(2)}, u32[]{:S(2)}) %all-to-all-start.2) | async-done | bytes 786464 | tf_op jit(solution)/shard_map/all_to_all | solution.py:68
  104.0 13.8 %all_to_all.31 = bf16[4,256,384]{2,1,0:T(8,128)(2,1)S(1)} all-to-all(bf16[4,256,384]{2,1,0:T(8,128)(2,1)S(1)} %broadcast_in_dim.16), channel_id=1, replica_groups=mesh['z'=8,'y'=8,'x'=4,'core'=2] {'x'}, dimensions={0} | all-to-all | bytes 1572864 | tf_op jit(solution)/shard_map/all_to_all | solution.py:60
  117.8 3.9 %collective-permute-start.4 = (bf16[4,256,384]{2,1,0:T(8,128)(2,1)S(1)}, bf16[4,256,384]{2,1,0:T(8,128)(2,1)S(1)}, u32[]{:S(2)}, u32[]{:S(2)}) collective-permute-start(bf16[4,256,384]{2,1,0:T(8,128)(2,1)S(1)} %all_to_all.31), channel_id=1, source_target_pairs={{0,1},{1,0},{2,3},{3,2},{4,5},{5,4},{6,7},{7,6},{8,9},{9,8},{10,11... | collective-permute-start | bytes 2359304 | tf_op jit(solution)/shard_map/ppermute | solution.py:51
  121.8 1.6 collective-permute-done.4
  125.3 8.0 %fusion.7 = bf16[2048,384]{1,0:T(8,128)(2,1)S(1)} fusion(bf16[2048,2048]{1,0:T(8,128)(2,1)} %all-gather.2.cloned.1.call-done, bf16[2048,384]{1,0:T(8,128)(2,1)S(1)} %bitcast.247), kind=kOutput, calls=%fused_computation.10 | convolution fusion | flops 3223191552 | bytes 11534336 | tf_op jit(solution)/shard_map/dot_general | solution.py:155
  133.6 2.3 %collective-permute-start.5 = (bf16[4,256,384]{2,1,0:T(8,128)(2,1)S(1)}, bf16[4,256,384]{2,1,0:T(8,128)(2,1)S(1)}, u32[]{:S(2)}, u32[]{:S(2)}) collective-permute-start(bf16[4,256,384]{2,1,0:T(8,128)(2,1)S(1)} %dynamic-slice_bitcast_fusion), channel_id=1, source_target_pairs={{0,1},{1,0},{2,3},{3,2},{4,5},{5,4},{6,7},{7,6},{8,9},{9,8},{10,11... | collective-permute-start | bytes 2359304 | tf_op jit(solution)/shard_map/ppermute | solution.py:51
  135.8 1.9 %collective-permute-done.5 = bf16[4,256,384]{2,1,0:T(8,128)(2,1)S(1)} collective-permute-done((bf16[4,256,384]{2,1,0:T(8,128)(2,1)S(1)}, bf16[4,256,384]{2,1,0:T(8,128)(2,1)S(1)}, u32[]{:S(2)}, u32[]{:S(2)}) %collective-permute-start.5) | collective-permute-done | bytes 786464 | tf_op jit(solution)/shard_map/ppermute | solution.py:51
  137.7 1.1 fusion.20
  138.8 3.5 %all-to-all-start.4 = ((bf16[4,256,384]{2,1,0:T(8,128)(2,1)}), bf16[4,256,384]{2,1,0:T(8,128)(2,1)S(1)}, u32[]{:S(2)}, u32[]{:S(2)}) async-start(bf16[4,256,384]{2,1,0:T(8,128)(2,1)} %fusion.20), calls=%async_computation.4 | async-start | bytes 1572864 | tf_op jit(solution)/shard_map/all_to_all | solution.py:161
  142.4 11.9 %all-to-all-done.4 = bf16[4,256,384]{2,1,0:T(8,128)(2,1)S(1)} async-done(((bf16[4,256,384]{2,1,0:T(8,128)(2,1)}), bf16[4,256,384]{2,1,0:T(8,128)(2,1)S(1)}, u32[]{:S(2)}, u32[]{:S(2)}) %all-to-all-start.4) | async-done | bytes 786464 | tf_op jit(solution)/shard_map/all_to_all | solution.py:161
  155.2 4.5 %all-to-all-start.5 = ((f32[8,2,384]{2,1,0:T(2,128)}), f32[8,2,384]{2,1,0:T(2,128)S(1)}, u32[]{:S(2)}, u32[]{:S(2)}) async-start(f32[8,2,384]{2,1,0:T(2,128)} %broadcast_in_dim.17), calls=%async_computation.5 | async-start | bytes 49152 | tf_op jit(solution)/shard_map/all_to_all | solution.py:167
  160.4 3.9 %all-to-all-done.5 = f32[8,2,384]{2,1,0:T(2,128)S(1)} async-done(((f32[8,2,384]{2,1,0:T(2,128)}), f32[8,2,384]{2,1,0:T(2,128)S(1)}, u32[]{:S(2)}, u32[]{:S(2)}) %all-to-all-start.5) | async-done | bytes 24608 | tf_op jit(solution)/shard_map/all_to_all | solution.py:167
  164.6 0.8 copy.69
  (59 shorter events, 9.3 us)
Async XLA Ops:
  6.5 118.7 %all-gather.2.cloned.1.call-start = ((), (), s32[]{:S(2)}) async-start(), calls=%async_computation.6 | async-start | bytes 9437184 | tf_op jit(solution)/shard_map/all_gather | solution.py:118
  41.5 7.0 %copy-start = (bf16[384,256]{1,0:T(8,128)(2,1)S(1)}, bf16[384,256]{1,0:T(8,128)(2,1)}, u32[]{:S(2)}) copy-start(bf16[384,256]{1,0:T(8,128)(2,1)} %param.12) | copy-start | bytes 589828
  41.5 38.9 %all-to-all-start.1 = ((bf16[8,256,384]{2,1,0:T(8,128)(2,1)}), bf16[8,256,384]{2,1,0:T(8,128)(2,1)S(1)}, u32[]{:S(2)}, u32[]{:S(2)}) async-start(bf16[8,256,384]{2,1,0:T(8,128)(2,1)} %broadcast_in_dim.14), calls=%async_computation.1 | async-start | bytes 3145728 | tf_op jit(solution)/shard_map/all_to_all | solution.py:39
  48.6 9.4 %collective-permute-start = (bf16[256,384]{1,0:T(8,128)(2,1)S(1)}, bf16[256,384]{1,0:T(8,128)(2,1)S(1)}, u32[]{:S(2)}, u32[]{:S(2)}) collective-permute-start(bf16[256,384]{1,0:T(8,128)(2,1)S(1)} %bitcast.242), channel_id=1, source_target_pairs={{0,6},{2,0},{4,2},{6,4},{1,7},{3,1},{5,3},{7,5},{8,14},{10,8},{12,... | collective-permute-start | bytes 589832 | tf_op jit(solution)/shard_map/ppermute | solution.py:47
  53.0 8.2 %collective-permute-start.1 = (bf16[256,384]{1,0:T(8,128)(2,1)S(1)}, bf16[256,384]{1,0:T(8,128)(2,1)S(1)}, u32[]{:S(2)}, u32[]{:S(2)}) collective-permute-start(bf16[256,384]{1,0:T(8,128)(2,1)S(1)} %bitcast.243), channel_id=1, source_target_pairs={{0,4},{2,6},{4,0},{6,2},{1,5},{3,7},{5,1},{7,3},{8,12},{10,14},{12... | collective-permute-start | bytes 589832 | tf_op jit(solution)/shard_map/ppermute | solution.py:47
  55.4 9.1 %collective-permute-start.2 = (bf16[256,384]{1,0:T(8,128)(2,1)S(1)}, bf16[256,384]{1,0:T(8,128)(2,1)S(1)}, u32[]{:S(2)}, u32[]{:S(2)}) collective-permute-start(bf16[256,384]{1,0:T(8,128)(2,1)S(1)} %bitcast.244), channel_id=1, source_target_pairs={{0,2},{2,4},{4,6},{6,0},{1,3},{3,5},{5,7},{7,1},{8,10},{10,12},{12... | collective-permute-start | bytes 589832 | tf_op jit(solution)/shard_map/ppermute | solution.py:47
  65.6 7.6 %collective-permute-start.3 = (bf16[4,256,384]{2,1,0:T(8,128)(2,1)}, bf16[4,256,384]{2,1,0:T(8,128)(2,1)S(1)}, u32[]{:S(2)}, u32[]{:S(2)}) collective-permute-start(bf16[4,256,384]{2,1,0:T(8,128)(2,1)} %pad_maximum_fusion.2), channel_id=1, source_target_pairs={{0,1},{1,0},{2,3},{3,2},{4,5},{5,4},{6,7},{7,6},{8,9},{9,8},{10,11... | collective-permute-start | bytes 2359304 | tf_op jit(solution)/shard_map/ppermute | solution.py:51
  83.0 19.5 %all-to-all-start.2 = ((bf16[8,384,128]{1,2,0:T(8,128)(2,1)}), bf16[8,384,128]{1,2,0:T(8,128)(2,1)S(1)}, u32[]{:S(2)}, u32[]{:S(2)}) async-start(bf16[8,384,128]{1,2,0:T(8,128)(2,1)} %broadcast_in_dim.15), calls=%async_computation.2 | async-start | bytes 1572864 | tf_op jit(solution)/shard_map/all_to_all | solution.py:68
  90.4 12.3 %copy-start.2 = (f32[1024]{0:T(1024)S(1)}, f32[1024]{0:T(1024)}, u32[]{:S(2)}) copy-start(f32[1024]{0:T(1024)} %param.16) | copy-start | bytes 12292
  103.9 17.9 %copy-start.1 = (f32[2048]{0:T(1024)S(1)}, f32[2048]{0:T(1024)}, u32[]{:S(2)}) copy-start(f32[2048]{0:T(1024)} %param.18) | copy-start | bytes 24580
  117.8 5.6 %collective-permute-start.4 = (bf16[4,256,384]{2,1,0:T(8,128)(2,1)S(1)}, bf16[4,256,384]{2,1,0:T(8,128)(2,1)S(1)}, u32[]{:S(2)}, u32[]{:S(2)}) collective-permute-start(bf16[4,256,384]{2,1,0:T(8,128)(2,1)S(1)} %all_to_all.31), channel_id=1, source_target_pairs={{0,1},{1,0},{2,3},{3,2},{4,5},{5,4},{6,7},{7,6},{8,9},{9,8},{10,11... | collective-permute-start | bytes 2359304 | tf_op jit(solution)/shard_map/ppermute | solution.py:51
  133.6 4.2 %collective-permute-start.5 = (bf16[4,256,384]{2,1,0:T(8,128)(2,1)S(1)}, bf16[4,256,384]{2,1,0:T(8,128)(2,1)S(1)}, u32[]{:S(2)}, u32[]{:S(2)}) collective-permute-start(bf16[4,256,384]{2,1,0:T(8,128)(2,1)S(1)} %dynamic-slice_bitcast_fusion), channel_id=1, source_target_pairs={{0,1},{1,0},{2,3},{3,2},{4,5},{5,4},{6,7},{7,6},{8,9},{9,8},{10,11... | collective-permute-start | bytes 2359304 | tf_op jit(solution)/shard_map/ppermute | solution.py:51
  138.8 15.5 %all-to-all-start.4 = ((bf16[4,256,384]{2,1,0:T(8,128)(2,1)}), bf16[4,256,384]{2,1,0:T(8,128)(2,1)S(1)}, u32[]{:S(2)}, u32[]{:S(2)}) async-start(bf16[4,256,384]{2,1,0:T(8,128)(2,1)} %fusion.20), calls=%async_computation.4 | async-start | bytes 1572864 | tf_op jit(solution)/shard_map/all_to_all | solution.py:161
  155.2 9.2 %all-to-all-start.5 = ((f32[8,2,384]{2,1,0:T(2,128)}), f32[8,2,384]{2,1,0:T(2,128)S(1)}, u32[]{:S(2)}, u32[]{:S(2)}) async-start(f32[8,2,384]{2,1,0:T(2,128)} %broadcast_in_dim.17), calls=%async_computation.5 | async-start | bytes 49152 | tf_op jit(solution)/shard_map/all_to_all | solution.py:167
Sparse Core Ops, SparseCore 0:
  40.2 68.9 all-gather.1
